TPU v7x, 512 devices: a whole 4x4x16 slice. The times are simulated.
512 devices in a mesh: ep: 128 (over z, x, core), tp: 4 (over y).
Axes of the slice: x: 4, y: 4, z: 16, core: 2. Of those that a mesh axis runs over, the one named last changes fastest.
Arguments:
- hidden_in: bfloat16 [2048, 256], P('ep'), may hold values from -24 to 24
- attn_gain: float32 [2048], replicated, may hold values from 0.1 to 1.9
- w_query: bfloat16 [2048, 1536], P('ep', 'tp'), may hold values from -32 to 32
- w_latent: bfloat16 [2048, 512], P('ep'), may hold values from -0.125 to 0.125
- w_rotkey: bfloat16 [32, 2048], replicated, may hold values from -32 to 32
- latent_gain: float32 [512], replicated, may hold values from 0.1 to 1.9
- w_key_up: bfloat16 [512, 1024], P(None, 'tp'), may hold values from -0.75 to 0.75
- w_value_up: bfloat16 [512, 1024], P(None, 'tp'), may hold values from -0.75 to 0.75
- w_attn_out: bfloat16 [2048, 1024], P('ep'), may hold values from -0.1875 to 0.1875
- cache_latent: bfloat16 [256, 1024, 512], P('ep'), may hold values from -6 to 6
- cache_rotkey: bfloat16 [256, 32, 1024], P('ep'), may hold values from -6 to 6
- lengths: int32 [256], P('ep'), may hold values from 128 to 1023
- ffn_gain: float32 [2048], replicated, may hold values from 0.1 to 1.9
- route_ids: int32 [256, 4], replicated, may hold values from 0 to 127, all different within a row; in each aligned block of 256 rows (0 to 255, 256 to 511, ...) at most 16 rows name the same one
- route_scores: float32 [256, 4], replicated, may hold values from 0.05 to 1
- w_exp_gate: bfloat16 [128, 2048, 512], P('ep', None, 'tp'), may hold values from -0.125 to 0.125
- w_exp_up: bfloat16 [128, 2048, 512], P('ep', None, 'tp'), may hold values from -0.125 to 0.125
- w_exp_down: bfloat16 [128, 512, 2048], P('ep', 'tp'), may hold values from -0.25 to 0.25
- w_shared_gate: bfloat16 [2048, 512], P('ep', 'tp'), may hold values from -0.125 to 0.125
- w_shared_up: bfloat16 [2048, 512], P('ep', 'tp'), may hold values from -0.125 to 0.125
- w_shared_out: bfloat16 [2048, 512], P('ep', 'tp'), may hold values from -0.25 to 0.25
Outputs:
- mixed_out: bfloat16 [2048, 256], P('ep', 'tp')
- new_latent: bfloat16 [256, 512], P('ep')
- new_rotkey: bfloat16 [256, 32], P('ep')
Inputs may be any that keep to these rules, and one draw needn't show every extreme that they name: `route_ids`: each row names 4 different experts; in the whole batch no expert is named by more than 16 rows, a bound that some block reaches.
All inputs are finite; a program needn't handle non-finite values.
Results may differ from a plain program's by a relative error of at most 0.015.
Values may be sent and summed in bfloat16 or wider, within the bound.
A program may use at most 64 MiB of HBM per device.

v0:
```python
import jax
import jax.numpy as jnp
from jax import lax
from jax.sharding import Mesh
from jax.sharding import PartitionSpec as P

HEAD_KEY = 64
HEAD_ROT = 32
HEAD_VAL = 64
SLOTS = 16
EP = ("ep_0", "ep_1", "ep_2")


EPSILON = 1e-06
THETA_BASE = 10000.0
ROUTED_SCALE = 2.5
HIGHEST = lax.Precision.HIGHEST


def in_blocks(value, dim, devices):
    lengths = value.shape
    pieces = value.reshape(*lengths[:dim], devices, lengths[dim] // devices, *lengths[dim + 1 :])
    return jnp.moveaxis(pieces, dim, 0)


def summed_on_arrival(value, axis, dim):
    pieces = in_blocks(value, dim, lax.axis_size(axis))
    arrived = lax.all_to_all(pieces, axis, split_axis=0, concat_axis=0, tiled=True)
    return arrived.sum(axis=0)


def summed_rows(value, axes, dim):
    far, near = axes
    own = summed_on_arrival(in_blocks(value, dim, lax.axis_size(far)), near, dim + 1)
    return jnp.sum(lax.all_to_all(own, far, 0, 0, tiled=True), axis=0)


def in_one_piece(arrays, axis, dim, along):
    widths = [a.shape[along] for a in arrays]
    both = jnp.concatenate(arrays, axis=along)
    out = summed_rows(both, axis, dim)
    return tuple(jnp.split(out, [sum(widths[:k]) for k in range(1, len(widths))], axis=along))


def copy_for_each(value, axis):
    devices = lax.axis_size(axis)
    return lax.all_to_all(
        jnp.broadcast_to(value[None], (devices, *value.shape)), axis, 0, 0, tiled=True
    )


def in_order(pieces, dim):
    pieces = jnp.moveaxis(pieces, 0, dim)
    lengths = pieces.shape
    return pieces.reshape(*lengths[:dim], lengths[dim] * lengths[dim + 1], *lengths[dim + 2 :])


def gathered_copies(value, axis, dim):
    pieces = copy_for_each(value, axis)
    return in_order(pieces, dim)


def whole_of(value, axes, dim):
    far, near = axes
    initial = copy_for_each(value, far)
    pieces = jnp.swapaxes(copy_for_each(initial, near), 0, 1)
    return in_order(pieces.reshape(-1, *value.shape), dim)


def rows_for(lines, devices):
    spare = -len(lines) % devices
    return jnp.pad(lines, [(0, spare)] + [(0, 0)] * (lines.ndim - 1))


def total_of(value, axes):
    own = summed_rows(rows_for(value, lax.axis_size(axes[0]) * lax.axis_size(axes[1])), axes, 0)
    whole = whole_of(own, axes, 0)
    return whole[: len(value)].reshape(value.shape)


def together(arrays, axis):
    ends = [0]
    for a in arrays:
        ends.append(ends[-1] + a.size)
    total = total_of(jnp.concatenate([a.ravel() for a in arrays]), axis)
    return tuple((total[b:e].reshape(a.shape) for a, b, e in zip(arrays, ends, ends[1:])))


def sum_at_owner(value, axis, dim):
    pieces = in_blocks(value, dim, lax.axis_size(axis))
    arrived = lax.all_to_all(pieces, axis, split_axis=0, concat_axis=0, tiled=True)
    return arrived.astype(jnp.float32).sum(axis=0)


def rotate(lower, upper, angles):
    cosine_part = jnp.cos(angles)
    sine_part = jnp.sin(angles)
    return (lower * cosine_part - upper * sine_part, lower * sine_part + upper * cosine_part)


def body(
    hidden_in,
    attn_gain,
    w_query,
    w_latent,
    w_rotkey,
    latent_gain,
    w_key_up,
    w_value_up,
    w_attn_out,
    cache_latent,
    cache_rotkey,
    lengths,
    ffn_gain,
    route_ids,
    route_scores,
    w_exp_gate,
    w_exp_up,
    w_exp_down,
    w_shared_gate,
    w_shared_up,
    w_shared_out,
):
    ep_count = lax.axis_size(EP)
    tp_count = lax.axis_size("tp")
    ep_index = lax.axis_index(EP)
    tp_index = lax.axis_index("tp")
    features, batch_rows = hidden_in.shape
    model_width = features * ep_count
    local_seqs, cache_len, latent = cache_latent.shape
    local_heads = w_key_up.shape[1] // HEAD_KEY
    contract_rows = (((0,), (0,)), ((), ()))
    input_rows = hidden_in.astype(jnp.float32)
    gain_block = lax.dynamic_slice_in_dim(attn_gain, ep_index * features, features)
    scaled_in = (input_rows * gain_block[:, None]).astype(jnp.bfloat16)
    query_part = lax.dot_general(
        w_query, scaled_in, contract_rows, preferred_element_type=jnp.float32
    )
    rot_weight = lax.dynamic_slice_in_dim(w_rotkey, ep_index * features, features, 1)
    rot_part = jnp.dot(rot_weight, scaled_in, preferred_element_type=jnp.float32)
    square_part = jnp.sum(input_rows * input_rows, axis=0, keepdims=True)
    query_count = query_part.shape[0]
    latent_cols = latent // tp_count
    latent_weight = lax.dynamic_slice_in_dim(w_latent, tp_index * latent_cols, latent_cols, 1)
    latent_part = lax.dot_general(
        latent_weight, scaled_in, contract_rows, preferred_element_type=jnp.float32
    )
    stacked = jnp.concatenate([query_part, latent_part, rot_part], axis=0)
    value_sum, square_sum = in_one_piece((stacked, square_part), (("ep_0", "ep_1"), "ep_2"), 1, 0)
    query_sum = value_sum[:query_count]
    latent_sum = value_sum[query_count : query_count + latent_cols]
    rot_sum = value_sum[query_count + latent_cols :]
    in_scale = lax.rsqrt(square_sum / model_width + EPSILON)
    latent_block = jnp.transpose((latent_sum * in_scale).astype(jnp.bfloat16))
    latent_raw = gathered_copies(latent_block, "tp", 1)
    query = jnp.transpose((query_sum * in_scale).astype(jnp.bfloat16))
    new_rotkey = jnp.transpose((rot_sum * in_scale).astype(jnp.bfloat16))
    raw_values = latent_raw.astype(jnp.float32)
    new_latent = (
        raw_values
        * lax.rsqrt(jnp.mean(raw_values * raw_values, axis=1, keepdims=True) + EPSILON)
        * latent_gain[None, :]
    ).astype(jnp.bfloat16)
    per_head = HEAD_KEY + HEAD_ROT
    query_heads = query.reshape(local_seqs, local_heads, per_head)
    key_up = w_key_up.reshape(latent, local_heads, HEAD_KEY)
    absorbed = jnp.einsum(
        "shn,chn->shc", query_heads[:, :, :HEAD_KEY], key_up, preferred_element_type=jnp.float32
    ).astype(jnp.bfloat16)
    half_rot = HEAD_ROT // 2
    frequency = THETA_BASE ** (-jnp.arange(half_rot, dtype=jnp.float32) / half_rot)
    new_angles = lengths.astype(jnp.float32)[:, None] * frequency[None, :]
    query_rot = query_heads[:, :, HEAD_KEY:].astype(jnp.float32)
    query_low, query_high = rotate(
        query_rot[..., :half_rot], query_rot[..., half_rot:], new_angles[:, None, :]
    )
    own_key = new_rotkey.astype(jnp.float32)
    own_low, own_high = rotate(own_key[:, :half_rot], own_key[:, half_rot:], new_angles)
    cache_angles = frequency[:, None] * jnp.arange(cache_len, dtype=jnp.float32)[None, :]
    rot_values = cache_rotkey.astype(jnp.float32)
    key_low, key_high = rotate(
        rot_values[:, :half_rot, :], rot_values[:, half_rot:, :], cache_angles[None]
    )
    score_scale = per_head ** (-0.5)
    latent_score = jnp.einsum(
        "shc,sjc->shj", absorbed, cache_latent, preferred_element_type=jnp.float32
    )
    rot_score = jnp.einsum("shr,srj->shj", query_low, key_low, precision=HIGHEST) + jnp.einsum(
        "shr,srj->shj", query_high, key_high, precision=HIGHEST
    )
    live = jnp.arange(cache_len)[None, None, :] < lengths[:, None, None]
    cache_score = jnp.where(live, score_scale * (latent_score + rot_score), -1e30)
    own_latent = jnp.einsum("shc,sc->sh", absorbed, new_latent, preferred_element_type=jnp.float32)
    own_score = score_scale * (
        own_latent
        + jnp.sum(query_low * own_low[:, None, :] + query_high * own_high[:, None, :], axis=2)
    )
    top_score = jnp.maximum(jnp.max(cache_score, axis=2), own_score)
    cache_weight = jnp.exp(cache_score - top_score[:, :, None])
    own_weight = jnp.exp(own_score - top_score)
    denominator = jnp.sum(cache_weight, axis=2) + own_weight
    cache_prob = (cache_weight / denominator[:, :, None]).astype(jnp.bfloat16)
    own_prob = (own_weight / denominator).astype(jnp.bfloat16)
    context = (
        jnp.einsum("shj,sjc->shc", cache_prob, cache_latent, preferred_element_type=jnp.float32)
        + own_prob.astype(jnp.float32)[:, :, None] * new_latent.astype(jnp.float32)[:, None, :]
    )
    value_up = w_value_up.reshape(latent, local_heads, HEAD_VAL)
    head_cols = local_heads * HEAD_VAL
    heads_out = (
        jnp.einsum(
            "shc,chv->shv",
            context.astype(jnp.bfloat16),
            value_up,
            preferred_element_type=jnp.float32,
        )
        .astype(jnp.bfloat16)
        .reshape(local_seqs, head_cols)
    )
    out_blocks = w_attn_out.reshape(features, tp_count, head_cols)
    piece = whole_of(
        heads_out.reshape(1, local_seqs * head_cols), (("ep_0", "ep_1"), ("ep_2", "tp")), 0
    )
    count = piece.shape[0]
    owners = jnp.arange(count, dtype=jnp.int32) % tp_count
    chosen = jnp.take(out_blocks, owners, axis=1)
    projected = jnp.einsum(
        "jsh,fjh->fjs",
        piece.reshape(count, local_seqs, head_cols),
        chosen,
        preferred_element_type=jnp.float32,
    )
    attn = jnp.sum(projected.reshape(features, ep_count, tp_count, local_seqs), axis=2)
    attn = attn.reshape(features, batch_rows).astype(jnp.bfloat16)
    mid = (input_rows + attn.astype(jnp.float32)).astype(jnp.bfloat16)
    mid_values = mid.astype(jnp.float32)
    ffn_block = lax.dynamic_slice_in_dim(ffn_gain, ep_index * features, features)
    ffn_in = (mid_values * ffn_block[:, None]).astype(jnp.bfloat16)
    gate_part = lax.dot_general(
        w_shared_gate, ffn_in, contract_rows, preferred_element_type=jnp.float32
    )
    up_part = lax.dot_general(
        w_shared_up, ffn_in, contract_rows, preferred_element_type=jnp.float32
    )
    mid_square_part = jnp.sum(mid_values * mid_values, axis=0, keepdims=True)
    mid_square, shared_gate, shared_up = together(
        (mid_square_part, gate_part, up_part), (("ep_0", "ep_1"), "ep_2")
    )
    scale_all = lax.rsqrt(mid_square / model_width + EPSILON)
    shared_act = (jax.nn.silu(scale_all * shared_gate) * (scale_all * shared_up)).astype(
        jnp.bfloat16
    )
    shared_block = jnp.dot(w_shared_out, shared_act, preferred_element_type=jnp.float32)
    top_count = route_ids.shape[1]
    flat_ids = route_ids.reshape(-1)
    hit_table = (flat_ids[:, None] == jnp.arange(ep_count, dtype=jnp.int32)[None, :]).astype(
        jnp.int32
    )
    earlier = jnp.cumsum(hit_table, axis=0) - hit_table
    slot_rank = jnp.sum(earlier * hit_table, axis=1)
    slot_of = flat_ids * SLOTS + slot_rank
    owners_flat = jnp.arange(batch_rows * top_count, dtype=jnp.int32) // top_count
    slot_row = jnp.full((ep_count * SLOTS,), batch_rows, jnp.int32).at[slot_of].set(owners_flat)
    padded_rows = jnp.concatenate(
        [jnp.transpose(mid), jnp.zeros((1, features), jnp.bfloat16)], axis=0
    )
    outbound = jnp.take(padded_rows, slot_row, axis=0).reshape(ep_count, SLOTS * features)
    arrived = lax.all_to_all(outbound, EP, split_axis=0, concat_axis=0, tiled=True).reshape(
        ep_count, SLOTS, features
    )
    arrived_values = arrived.astype(jnp.float32)
    slot_scale = lax.rsqrt(
        jnp.sum(arrived_values * arrived_values, axis=(0, 2)) / model_width + EPSILON
    )
    expert_in = (arrived_values * ffn_gain.reshape(ep_count, 1, features)).astype(jnp.bfloat16)
    gate_weight = w_exp_gate.reshape(ep_count, features, -1)
    up_weight = w_exp_up.reshape(ep_count, features, -1)
    gate_value = jnp.einsum(
        "gsf,gfh->sh", expert_in, gate_weight, preferred_element_type=jnp.float32
    )
    up_value = jnp.einsum("gsf,gfh->sh", expert_in, up_weight, preferred_element_type=jnp.float32)
    activation = (
        jax.nn.silu(slot_scale[:, None] * gate_value) * (slot_scale[:, None] * up_value)
    ).astype(jnp.bfloat16)
    down_weight = w_exp_down.reshape(activation.shape[1], ep_count, features)
    expert_out = jnp.einsum(
        "sh,hgf->gsf", activation, down_weight, preferred_element_type=jnp.float32
    )
    expert_out = expert_out.astype(jnp.bfloat16).reshape(ep_count, SLOTS * features)
    returned = lax.all_to_all(expert_out, EP, split_axis=0, concat_axis=0, tiled=True).reshape(
        ep_count * SLOTS, features
    )
    picked = (
        jnp.take(returned, slot_of, axis=0)
        .reshape(batch_rows, top_count, features)
        .astype(jnp.float32)
    )
    route_weight = ROUTED_SCALE * route_scores / jnp.sum(route_scores, axis=1, keepdims=True)
    routed = jnp.einsum("bkf,bk->fb", picked, route_weight, precision=HIGHEST)
    rows_tp = batch_rows // tp_count
    block_sum = sum_at_owner((shared_block + routed).astype(jnp.bfloat16), "tp", 1)
    mid_block = lax.dynamic_slice_in_dim(mid_values, tp_index * rows_tp, rows_tp, 1)
    mixed_out = (mid_block + block_sum).astype(jnp.bfloat16)
    return (mixed_out, new_latent, new_rotkey)


def solution(mesh):
    split = Mesh(mesh.devices.reshape(16, 4, 2, mesh.shape["tp"]), ("ep_0", "ep_1", "ep_2", "tp"))
    return jax.shard_map(
        body,
        mesh=split,
        in_specs=(
            P(EP, None),
            P(),
            P(EP, "tp"),
            P(EP, None),
            P(),
            P(),
            P(None, "tp"),
            P(None, "tp"),
            P(EP, None),
            P(EP, None, None),
            P(EP, None, None),
            P(EP),
            P(),
            P(),
            P(),
            P(EP, None, "tp"),
            P(EP, None, "tp"),
            P(EP, "tp", None),
            P(EP, "tp"),
            P(EP, "tp"),
            P(EP, "tp"),
        ),
        out_specs=(P(EP, "tp"), P(EP, None), P(EP, None)),
        check_vma=False,
    )
```

profile of v0, /device:TPU:1, one launch (start us, length us, event | category | flops | bytes accessed | tf_op | source)
XLA Modules:
  0.0 233.9 jit_solution(3346372376417153228)
XLA Ops:
  6.7 10.7 %all_to_all.70 = f32[2,64,545,2]{2,3,1,0:T(2,128)S(1)} all-to-all(f32[2,64,545,2]{2,3,1,0:T(2,128)S(1)} %copy.221), channel_id=1, replica_groups=mesh['ep_0'=16,'ep_1'=4,'ep_2'=2,'tp'=4] {'ep_2'}, dimensions={0} | all-to-all | bytes 1116160 | tf_op jit(solution)/shard_map/all_to_all | solution.py:28
  17.4 1.3 reduce_sum.138
  18.7 12.9 %all-to-all-start.1 = ((f32[64,545,2]{1,2,0:T(2,128)}), f32[64,545,2]{1,2,0:T(2,128)S(1)}, u32[]{:S(2)}, u32[]{:S(2)}) async-start(f32[64,545,2]{1,2,0:T(2,128)} %reduce_sum.138), calls=%async_computation.1 | async-start | bytes 655360 | tf_op jit(solution)/shard_map/all_to_all | solution.py:35
  32.6 1.1 copy.224
  34.6 1.8 copy.226
  43.0 11.4 %all-to-all-done.1 = f32[64,545,2]{1,2,0:T(2,128)S(1)} async-done(((f32[64,545,2]{1,2,0:T(2,128)}), f32[64,545,2]{1,2,0:T(2,128)S(1)}, u32[]{:S(2)}, u32[]{:S(2)}) %all-to-all-start.1) | async-done | bytes 279072 | tf_op jit(solution)/shard_map/all_to_all | solution.py:35
  56.2 4.2 %all-to-all-start.2 = ((bf16[4,2,128]{2,1,0:T(2,128)(2,1)}), bf16[4,2,128]{2,1,0:T(2,128)(2,1)S(1)}, u32[]{:S(2)}, u32[]{:S(2)}) async-start(bf16[4,2,128]{2,1,0:T(2,128)(2,1)} %broadcast_in_dim.114), calls=%async_computation.2 | async-start | bytes 4096 | tf_op jit(solution)/shard_map/all_to_all | solution.py:47
  62.7 1.7 all-to-all-done.2
  68.6 6.7 %all-to-all-start.3 = ((bf16[64,2,256]{2,1,0:T(2,128)(2,1)}), bf16[64,2,256]{2,1,0:T(2,128)(2,1)S(1)}, u32[]{:S(2)}, u32[]{:S(2)}) async-start(bf16[64,2,256]{2,1,0:T(2,128)(2,1)} %reshape.460), calls=%async_computation.3 | async-start | bytes 131072 | tf_op jit(solution)/shard_map/all_to_all | solution.py:47
  75.3 4.3 %scatter_custom_fusion = s32[2048]{0:T(1024)S(1)} fusion(s32[1024]{0:T(1024)S(1)} %bitcast.167, s32[1024]{0:T(1024)S(1)} %add_select_fusion, s32[]{:T(128)} %constant.145.clone.1), kind=kCustom, calls=%fused_computation.130 | custom fusion | bytes 8196 | tf_op jit(solution)/shard_map/scatter | solution.py:263
  79.7 9.7 %all-to-all-done.3 = bf16[64,2,256]{2,1,0:T(2,128)(2,1)S(1)} async-done(((bf16[64,2,256]{2,1,0:T(2,128)(2,1)}), bf16[64,2,256]{2,1,0:T(2,128)(2,1)S(1)}, u32[]{:S(2)}, u32[]{:S(2)}) %all-to-all-start.3) | async-done | bytes 65568 | tf_op jit(solution)/shard_map/all_to_all | solution.py:47
  90.3 7.8 %all-to-all-start.4 = ((bf16[8,64,1,512]{3,1,2,0:T(8,128)(2,1)}), bf16[8,64,1,512]{3,1,2,0:T(8,128)(2,1)S(1)}, u32[]{:S(2)}, u32[]{:S(2)}) async-start(bf16[8,64,1,512]{3,1,2,0:T(8,128)(2,1)} %broadcast_in_dim.118), calls=%async_computation.4 | async-start | bytes 1048576 | tf_op jit(solution)/shard_map/all_to_all | solution.py:47
  99.6 3.4 %gather_fusion = bf16[512,16,256]{2,1,0:T(8,128)(2,1)} fusion(bf16[16,4,256]{2,0,1:T(8,128)(2,1)S(1)} %bitcast.139, s32[1024]{0:T(1024)S(1)} %pad_clamp_fusion), kind=kCustom, calls=%fused_computation | custom fusion | bytes 8390656 | tf_op jit(solution)/shard_map/jit(_take)/gather | solution.py:226
  103.6 3.8 %all-to-all-done.4 = bf16[8,64,1,512]{3,1,2,0:T(8,128)(2,1)S(1)} async-done(((bf16[8,64,1,512]{3,1,2,0:T(8,128)(2,1)}), bf16[8,64,1,512]{3,1,2,0:T(8,128)(2,1)S(1)}, u32[]{:S(2)}, u32[]{:S(2)}) %all-to-all-start.4) | async-done | bytes 524320 | tf_op jit(solution)/shard_map/all_to_all | solution.py:47
  107.8 3.6 %bitcast_reduce_fusion = bf16[16,128,2]{0,2,1:T(2,128)(2,1)S(1)} fusion(bf16[512,2,256]{2,1,0:T(2,128)(2,1)S(1)} %reshape_reshape_reshape.3, bf16[512,16,256]{2,1,0:T(8,128)(2,1)} %gather_fusion, pred[512]{0:T(512)(128)(4,1)S(1)} %compare_and_fusion.2), kind=kOutput, calls=%fused_computation.38 | convolution fusion | flops 10498048 | bytes 4727296 | tf_op jit(solution)/shard_map/jsh,fjh->fjs/dot_general | solution.py:227
  114.1 3.7 %all-to-all-start.5 = ((f32[2,64,514]{2,1,0:T(8,128)}), f32[2,64,514]{2,1,0:T(8,128)S(1)}, u32[]{:S(2)}, u32[]{:S(2)}) async-start(f32[2,64,514]{2,1,0:T(8,128)} %copy.232), calls=%async_computation.5 | async-start | bytes 655360 | tf_op jit(solution)/shard_map/all_to_all | solution.py:28
  117.9 7.2 %gather_fusion.1 = bf16[2048,16]{1,0:T(8,128)(2,1)S(1)} fusion(bf16[257,16]{1,0:T(8,128)(2,1)S(1)} %concatenate.24, s32[2048]{0:T(1024)} %fusion.63), kind=kCustom, calls=%fused_computation.1 | custom fusion | bytes 139264 | tf_op jit(solution)/shard_map/jit(_take)/gather | solution.py:267
  127.8 6.3 %all-to-all-start.9 = ((bf16[128,2,128]{2,1,0:T(2,128)(2,1)}), bf16[128,2,128]{2,1,0:T(2,128)(2,1)}, u32[]{:S(2)}, u32[]{:S(2)}) async-start(bf16[128,2,128]{2,1,0:T(2,128)(2,1)} %reshape.462), calls=%async_computation.9 | async-start | bytes 131072 | tf_op jit(solution)/shard_map/all_to_all | solution.py:268
  136.7 11.7 %all-to-all-done.9 = bf16[128,2,128]{2,1,0:T(2,128)(2,1)} async-done(((bf16[128,2,128]{2,1,0:T(2,128)(2,1)}), bf16[128,2,128]{2,1,0:T(2,128)(2,1)}, u32[]{:S(2)}, u32[]{:S(2)}) %all-to-all-start.9) | async-done | bytes 65568 | tf_op jit(solution)/shard_map/all_to_all | solution.py:268
  148.4 4.6 %all-to-all-start.6 = ((f32[64,1,514]{2,1,0:T(1,128)}), f32[64,1,514]{2,1,0:T(1,128)S(1)}, u32[]{:S(2)}, u32[]{:S(2)}) async-start(f32[64,1,514]{2,1,0:T(1,128)} %all_to_all.50), calls=%async_computation.6 | async-start | bytes 327680 | tf_op jit(solution)/shard_map/all_to_all | solution.py:35
  155.6 1.4 fusion.15
  157.0 1.9 fusion.5
  160.4 9.3 %all-to-all-done.6 = f32[64,1,514]{2,1,0:T(1,128)S(1)} async-done(((f32[64,1,514]{2,1,0:T(1,128)}), f32[64,1,514]{2,1,0:T(1,128)S(1)}, u32[]{:S(2)}, u32[]{:S(2)}) %all-to-all-start.6) | async-done | bytes 131616 | tf_op jit(solution)/shard_map/all_to_all | solution.py:35
  169.7 8.6 %all-to-all-start.10 = ((bf16[128,2,128]{2,1,0:T(2,128)(2,1)}), bf16[128,2,128]{2,1,0:T(2,128)(2,1)S(1)}, u32[]{:S(2)}, u32[]{:S(2)}) async-start(bf16[128,2,128]{2,1,0:T(2,128)(2,1)} %reshape.464), calls=%async_computation.10 | async-start | bytes 131072 | tf_op jit(solution)/shard_map/all_to_all | solution.py:290
  178.7 14.8 %all-to-all-done.10 = bf16[128,2,128]{2,1,0:T(2,128)(2,1)S(1)} async-done(((bf16[128,2,128]{2,1,0:T(2,128)(2,1)}), bf16[128,2,128]{2,1,0:T(2,128)(2,1)S(1)}, u32[]{:S(2)}, u32[]{:S(2)}) %all-to-all-start.10) | async-done | bytes 65568 | tf_op jit(solution)/shard_map/all_to_all | solution.py:290
  194.2 4.8 %all-to-all-start.7 = ((f32[64,1,514]{2,1,0:T(1,128)}), f32[64,1,514]{2,1,0:T(1,128)S(1)}, u32[]{:S(2)}, u32[]{:S(2)}) async-start(f32[64,1,514]{2,1,0:T(1,128)} %broadcast_in_dim.119), calls=%async_computation.7 | async-start | bytes 327680 | tf_op jit(solution)/shard_map/all_to_all | solution.py:47
  200.2 3.2 %gather_fusion.2 = bf16[1024,16]{1,0:T(8,128)(2,1)S(1)} fusion(bf16[2048,16]{1,0:T(8,128)(2,1)S(1)} %reshape.411, s32[1024]{0:T(1024)S(1)} %broadcast_clamp_fusion), kind=kCustom, calls=%fused_computation.2 | custom fusion | bytes 69632 | tf_op jit(solution)/shard_map/jit(_take)/gather | solution.py:294
  203.4 1.5 multiply_reduce_fusion
  204.9 11.6 %all-to-all-done.7 = f32[64,1,514]{2,1,0:T(1,128)S(1)} async-done(((f32[64,1,514]{2,1,0:T(1,128)}), f32[64,1,514]{2,1,0:T(1,128)S(1)}, u32[]{:S(2)}, u32[]{:S(2)}) %all-to-all-start.7) | async-done | bytes 131616 | tf_op jit(solution)/shard_map/all_to_all | solution.py:47
  216.5 6.2 %all_to_all.71 = f32[2,64,514]{2,1,0:T(8,128)S(1)} all-to-all(f32[2,64,514]{2,1,0:T(8,128)S(1)} %broadcast_in_dim.121), channel_id=1, replica_groups=mesh['ep_0'=16,'ep_1'=4,'ep_2'=2,'tp'=4] {'ep_2'}, dimensions={0} | all-to-all | bytes 526336 | tf_op jit(solution)/shard_map/all_to_all | solution.py:47
  224.9 3.2 %all-to-all-start.11 = ((bf16[4,2,512]{2,1,0:T(2,128)(2,1)}), bf16[4,2,512]{2,1,0:T(2,128)(2,1)S(1)}, u32[]{:S(2)}, u32[]{:S(2)}) async-start(bf16[4,2,512]{2,1,0:T(2,128)(2,1)} %reshape.466), calls=%async_computation.11 | async-start | bytes 16384 | tf_op jit(solution)/shard_map/all_to_all | solution.py:91
  228.1 4.1 %all-to-all-done.11 = bf16[4,2,512]{2,1,0:T(2,128)(2,1)S(1)} async-done(((bf16[4,2,512]{2,1,0:T(2,128)(2,1)}), bf16[4,2,512]{2,1,0:T(2,128)(2,1)S(1)}, u32[]{:S(2)}, u32[]{:S(2)}) %all-to-all-start.11) | async-done | bytes 8224 | tf_op jit(solution)/shard_map/all_to_all | solution.py:91
  (168 shorter events, 43.8 us)
Async XLA Ops:
  0.6 60.6 %copy-start = (bf16[2,1024,512]{2,1,0:T(8,128)(2,1)S(1)}, bf16[2,1024,512]{2,1,0:T(8,128)(2,1)}, u32[]{:S(2)}) copy-start(bf16[2,1024,512]{2,1,0:T(8,128)(2,1)} %param.30) | copy-start | bytes 6291460
  3.4 28.2 %copy-start.3 = (s32[256,4]{0,1:T(4,128)S(1)}, s32[256,4]{0,1:T(4,128)}, u32[]{:S(2)}) copy-start(s32[256,4]{0,1:T(4,128)} %param.34) | copy-start | bytes 12292
  4.3 27.7 %copy-start.10 = (s32[2]{0:T(128)S(1)}, s32[2]{0:T(128)}, u32[]{:S(2)}) copy-start(s32[2]{0:T(128)} %param.32) | copy-start | bytes 28
  18.7 35.7 %all-to-all-start.1 = ((f32[64,545,2]{1,2,0:T(2,128)}), f32[64,545,2]{1,2,0:T(2,128)S(1)}, u32[]{:S(2)}, u32[]{:S(2)}) async-start(f32[64,545,2]{1,2,0:T(2,128)} %reduce_sum.138), calls=%async_computation.1 | async-start | bytes 655360 | tf_op jit(solution)/shard_map/all_to_all | solution.py:35
  41.5 1.2 copy-start.8
  41.8 24.2 %copy-start.2 = (bf16[512,256]{0,1:T(8,128)(2,1)S(1)}, bf16[512,256]{0,1:T(8,128)(2,1)}, u32[]{:S(2)}) copy-start(bf16[512,256]{0,1:T(8,128)(2,1)} %copy.226) | copy-start | bytes 786436
  54.5 43.5 %copy-start.4 = (bf16[16,1024]{1,0:T(8,128)(2,1)S(1)}, bf16[16,1024]{1,0:T(8,128)(2,1)}, u32[]{:S(2)}) copy-start(bf16[16,1024]{1,0:T(8,128)(2,1)} %param.29) | copy-start | bytes 98308
  56.2 8.2 %all-to-all-start.2 = ((bf16[4,2,128]{2,1,0:T(2,128)(2,1)}), bf16[4,2,128]{2,1,0:T(2,128)(2,1)S(1)}, u32[]{:S(2)}, u32[]{:S(2)}) async-start(bf16[4,2,128]{2,1,0:T(2,128)(2,1)} %broadcast_in_dim.114), calls=%async_computation.2 | async-start | bytes 4096 | tf_op jit(solution)/shard_map/all_to_all | solution.py:47
  65.3 25.0 %copy-start.9 = (bf16[2,512]{1,0:T(2,128)(2,1)}, bf16[2,512]{1,0:T(2,128)(2,1)S(1)}, u32[]{:S(2)}) copy-start(bf16[2,512]{1,0:T(2,128)(2,1)S(1)} %get-tuple-element.29) | copy-start | bytes 6148
  68.6 20.7 %all-to-all-start.3 = ((bf16[64,2,256]{2,1,0:T(2,128)(2,1)}), bf16[64,2,256]{2,1,0:T(2,128)(2,1)S(1)}, u32[]{:S(2)}, u32[]{:S(2)}) async-start(bf16[64,2,256]{2,1,0:T(2,128)(2,1)} %reshape.460), calls=%async_computation.3 | async-start | bytes 131072 | tf_op jit(solution)/shard_map/all_to_all | solution.py:47
  90.3 17.1 %all-to-all-start.4 = ((bf16[8,64,1,512]{3,1,2,0:T(8,128)(2,1)}), bf16[8,64,1,512]{3,1,2,0:T(8,128)(2,1)S(1)}, u32[]{:S(2)}, u32[]{:S(2)}) async-start(bf16[8,64,1,512]{3,1,2,0:T(8,128)(2,1)} %broadcast_in_dim.118), calls=%async_computation.4 | async-start | bytes 1048576 | tf_op jit(solution)/shard_map/all_to_all | solution.py:47
  107.8 4.5 %copy-start.6 = (bf16[16,128]{1,0:T(8,128)(2,1)S(1)}, bf16[16,128]{1,0:T(8,128)(2,1)}, u32[]{:S(2)}) copy-start(bf16[16,128]{1,0:T(8,128)(2,1)} %param.39) | copy-start | bytes 12292
  107.8 4.8 %copy-start.7 = (bf16[16,128]{1,0:T(8,128)(2,1)S(1)}, bf16[16,128]{1,0:T(8,128)(2,1)}, u32[]{:S(2)}) copy-start(bf16[16,128]{1,0:T(8,128)(2,1)} %param.40) | copy-start | bytes 12292
  113.0 22.6 %copy-start.1 = (bf16[1,128,2048]{2,1,0:T(8,128)(2,1)S(1)}, bf16[1,128,2048]{2,1,0:T(8,128)(2,1)}, u32[]{:S(2)}) copy-start(bf16[1,128,2048]{2,1,0:T(8,128)(2,1)} %param.38) | copy-start | bytes 1572868
  114.1 13.6 %all-to-all-start.5 = ((f32[2,64,514]{2,1,0:T(8,128)}), f32[2,64,514]{2,1,0:T(8,128)S(1)}, u32[]{:S(2)}, u32[]{:S(2)}) async-start(f32[2,64,514]{2,1,0:T(8,128)} %copy.232), calls=%async_computation.5 | async-start | bytes 655360 | tf_op jit(solution)/shard_map/all_to_all | solution.py:28
  127.8 20.6 %all-to-all-start.9 = ((bf16[128,2,128]{2,1,0:T(2,128)(2,1)}), bf16[128,2,128]{2,1,0:T(2,128)(2,1)}, u32[]{:S(2)}, u32[]{:S(2)}) async-start(bf16[128,2,128]{2,1,0:T(2,128)(2,1)} %reshape.462), calls=%async_computation.9 | async-start | bytes 131072 | tf_op jit(solution)/shard_map/all_to_all | solution.py:268
  135.9 42.6 %copy-start.5 = (f32[256,4]{0,1:T(4,128)S(1)}, f32[256,4]{0,1:T(4,128)}, u32[]{:S(2)}) copy-start(f32[256,4]{0,1:T(4,128)} %param.35) | copy-start | bytes 12292
  148.4 21.3 %all-to-all-start.6 = ((f32[64,1,514]{2,1,0:T(1,128)}), f32[64,1,514]{2,1,0:T(1,128)S(1)}, u32[]{:S(2)}, u32[]{:S(2)}) async-start(f32[64,1,514]{2,1,0:T(1,128)} %all_to_all.50), calls=%async_computation.6 | async-start | bytes 327680 | tf_op jit(solution)/shard_map/all_to_all | solution.py:35
  169.7 23.7 %all-to-all-start.10 = ((bf16[128,2,128]{2,1,0:T(2,128)(2,1)}), bf16[128,2,128]{2,1,0:T(2,128)(2,1)S(1)}, u32[]{:S(2)}, u32[]{:S(2)}) async-start(bf16[128,2,128]{2,1,0:T(2,128)(2,1)} %reshape.464), calls=%async_computation.10 | async-start | bytes 131072 | tf_op jit(solution)/shard_map/all_to_all | solution.py:290
  178.4 45.5 %copy-start.11 = (bf16[16,128]{1,0:T(8,128)(2,1)S(1)}, bf16[16,128]{1,0:T(8,128)(2,1)}, u32[]{:S(2)}) copy-start(bf16[16,128]{1,0:T(8,128)(2,1)} %param.41) | copy-start | bytes 12292
  194.2 22.3 %all-to-all-start.7 = ((f32[64,1,514]{2,1,0:T(1,128)}), f32[64,1,514]{2,1,0:T(1,128)S(1)}, u32[]{:S(2)}, u32[]{:S(2)}) async-start(f32[64,1,514]{2,1,0:T(1,128)} %broadcast_in_dim.119), calls=%async_computation.7 | async-start | bytes 327680 | tf_op jit(solution)/shard_map/all_to_all | solution.py:47
  224.9 7.4 %all-to-all-start.11 = ((bf16[4,2,512]{2,1,0:T(2,128)(2,1)}), bf16[4,2,512]{2,1,0:T(2,128)(2,1)S(1)}, u32[]{:S(2)}, u32[]{:S(2)}) async-start(bf16[4,2,512]{2,1,0:T(2,128)(2,1)} %reshape.466), calls=%async_computation.11 | async-start | bytes 16384 | tf_op jit(solution)/shard_map/all_to_all | solution.py:91
where the time goes:
time: 236 us; the launch traced here: 234 us
  waiting for transfers between devices  78 us (33%)
  starting transfers between devices  63 us (27%)
  local copies, waits for them, and re-layouts  45.4 us (19%)
  blocking collectives  17 us (7%)
  other arithmetic  16.9 us (7%)
  matrix products  12.3 us (5%)
    all_to_all x4, waiting for transfers between devices, copy_for_each(): lax.all_to_all(jnp.broadcast_to(value[None], (devices, *value.shape)), ax...  26.7 us
    all_to_all x4, starting transfers between devices, copy_for_each(): lax.all_to_all(jnp.broadcast_to(value[None], (devices, *value.shape)), ax...  23.5 us
    all_to_all x2, waiting for transfers between devices, summed_rows(): return jnp.sum(lax.all_to_all(own, far, 0, 0, tiled=True), axis=0)  20.7 us
    all_to_all x2, starting transfers between devices, summed_rows(): return jnp.sum(lax.all_to_all(own, far, 0, 0, tiled=True), axis=0)  17.6 us
    all_to_all x1, waiting for transfers between devices, body(): lax.all_to_all(expert_out, EP, split_axis=0, concat_axis=0, tiled=True)  14.8 us
    all_to_all x1, waiting for transfers between devices, body(): lax.all_to_all(outbound, EP, split_axis=0, concat_axis=0, tiled=True)  11.7 us
    all_to_all x1, blocking collectives, summed_on_arrival(): lax.all_to_all(pieces, axis, split_axis=0, concat_axis=0, tiled=True)  10.7 us
    unnamed x45, local copies, waits for them, and re-layouts  9.14 us
  transfers between devices with their start and end apart: 10, of which 9 were waited for; matrix products, arithmetic and copies ran while one was open for 21% of the time, Pallas kernels for 0%

commit v1 on v0

v1 whole, which is shorter than its diff:
```python
import functools

import jax
import jax.numpy as jnp
import numpy as np
from jax import lax
from jax.experimental import pallas as pl
from jax.experimental.pallas import tpu as pltpu
from jax.sharding import Mesh
from jax.sharding import PartitionSpec as P

MESH = pl.DeviceIdType.MESH
F32 = jnp.float32
BF16 = jnp.bfloat16
HIGHEST = lax.Precision.HIGHEST
NN = (((1,), (0,)), ((), ()))
NT = (((1,), (1,)), ((), ()))
TN = (((0,), (0,)), ((), ()))

LOCAL_HEADS = 4
HEAD_KEY = 64
HEAD_ROT = 32
HEAD_VAL = 64
PER_HEAD = HEAD_KEY + HEAD_ROT
LATENT = 512
CACHE = 1024
HIDDEN = 128
SLOTS = 16
FEATS = 16
SEQS = 2
EPSILON = 1e-06
THETA_BASE = 10000.0
ROUTED_SCALE = 2.5
QW = LOCAL_HEADS * PER_HEAD
HV = LOCAL_HEADS * HEAD_VAL


def dot(a, b, dims=NN, precision=None):
    return lax.dot_general(a, b, dims, precision=precision, preferred_element_type=F32)


def iota(shape, axis):
    return lax.broadcasted_iota(jnp.int32, shape, axis)


def ones_where(mask, dtype=BF16):
    return jnp.where(mask, 1.0, 0.0).astype(dtype)


def rounded(v):
    return v.astype(BF16).astype(F32)


def log2(n):
    return n.bit_length() - 1


def kernel(nz, nx, nc, nt, *refs):
    (
        hidden, attn_gain, w_query, w_latent, w_rotkey, latent_gain, w_key_up, w_value_up, w_attn_out, cache_latent, cache_rotkey,
        lengths, ffn_gain, route_ids, route_scores, w_exp_gate, w_exp_up, w_exp_down, w_shared_gate, w_shared_up, w_shared_out,
        trig, freq,
        o_mixed, o_latent, o_rotkey,
        crit, back, rotw, again, fgain, lgain, fr, keyup, valup, cache, crot, lens, ids, scores, wgu, wd, trg,
        za_s, za_r, yb, zd, ye, midx, zf_s, zf_r, zg_s, zg_r, zh_s, zh_r, zs, xr_s, xr_r, yo_s, yo_r,
        ka, krot, sel_p, wt, ht, h32, s32, pall, shf,
        lsem, ssem, rsem,
    ) = refs
    ncol = nx * nc
    pf = FEATS * ncol
    rows = SEQS * nz
    batch = rows * ncol
    width = pf * nz
    lq = LATENT // nt
    nslot = nz * SLOTS
    ob = batch // nt
    hl = 2 * ob
    z, x, c, y = (lax.axis_index(a) for a in ("z", "x", "c", "y"))
    col = x * nc + c

    z_order = sorted(range(1, nz), key=lambda d: -min(d, nz - d))
    z_peers = [(lax.rem(z + d, nz),) for d in z_order]

    def zdev(p):
        return {"z": p}

    def xdev(p):
        return {"x": lax.div(p, nc), "c": lax.rem(p, nc)}

    def ydev(p):
        return {"y": p}

    x_peers = [lax.rem(col + d, ncol) for d in range(1, ncol)]
    y_peers = [lax.rem(y + d, nt) for d in range(1, nt)]
    z_peers = [p for (p,) in z_peers]

    bar = pltpu.get_barrier_semaphore()
    for p in z_peers:
        pl.semaphore_signal(bar, inc=1, device_id=zdev(p), device_id_type=MESH)
    for p in x_peers:
        pl.semaphore_signal(bar, inc=1, device_id=xdev(p), device_id_type=MESH)
    for p in y_peers:
        pl.semaphore_signal(bar, inc=1, device_id=ydev(p), device_id_type=MESH)

    def loads(sem, pairs):
        copies = [pltpu.make_async_copy(s, d, lsem.at[sem + i]) for i, (s, d) in enumerate(pairs)]
        for cp in copies:
            cp.start()
        return copies

    def done(copies):
        for cp in copies:
            cp.wait()

    own_lq = pl.ds(pl.multiple_of(y * lq, lq), lq)
    own_hv = pl.ds(pl.multiple_of(y * HV, HV), HV)
    own_pf = pl.ds(pl.multiple_of(z * pf, pf), pf)
    half = HEAD_ROT // 2
    l_crit = loads(0, [
        (w_query, crit.at[col, :, pl.ds(0, QW)]),
        (w_latent.at[:, own_lq], crit.at[col, :, pl.ds(QW, lq)]),
        (hidden, crit.at[col, :, pl.ds(QW + lq, batch)]),
    ])
    l_rot = loads(3, [
        (w_rotkey.at[:, own_pf], rotw.at[pl.ds(0, HEAD_ROT)]),
        (w_rotkey.at[pl.ds(half, half), own_pf], rotw.at[pl.ds(64, half)]),
        (w_rotkey.at[pl.ds(0, half), own_pf], rotw.at[pl.ds(64 + half, half)]),
        (attn_gain, again),
        (ffn_gain, fgain),
        (latent_gain, lgain),
        (freq, fr),
        (lengths, lens),
    ])
    l_back = loads(11, [
        (w_attn_out.at[:, own_hv], back.at[col, :, pl.ds(0, HV)]),
        (w_shared_gate, back.at[col, :, pl.ds(HV, HIDDEN)]),
        (w_shared_up, back.at[col, :, pl.ds(HV + HIDDEN, HIDDEN)]),
        (w_shared_out, back.at[col, :, pl.ds(HV + 2 * HIDDEN, HIDDEN)]),
    ])
    l_tab = loads(15, [
        (w_key_up, keyup), (cache_rotkey, crot), (trig, trg), (route_ids, ids), (route_scores, scores),
    ])
    l_att = loads(20, [(cache_latent, cache), (w_value_up, valup)])
    l_exp = loads(22, [
        (w_exp_gate.at[0], wgu.at[:, pl.ds(0, HIDDEN)]),
        (w_exp_up.at[0], wgu.at[:, pl.ds(HIDDEN, HIDDEN)]),
        (w_exp_down.at[0], wd),
    ])

    def send(src, dst, k, dev):
        cp = pltpu.make_async_remote_copy(
            src_ref=src, dst_ref=dst, send_sem=ssem.at[k], recv_sem=rsem.at[k], device_id=dev, device_id_type=MESH
        )
        cp.start()

    def arrived(buf, n, k):
        part = buf.at[pl.ds(0, n)]
        pltpu.make_async_copy(part, part, rsem.at[k]).wait()

    pending = []

    def sent(buf, n, k):
        pending.append((buf, n, k))

    done(l_crit)
    pl.semaphore_wait(bar, len(z_peers) + len(x_peers) + len(y_peers))
    for p in x_peers:
        send(crit.at[col], crit.at[col], 0, xdev(p))
    sent(crit, ncol - 1, 0)
    done(l_back)
    for p in x_peers:
        send(back.at[col], back.at[col], 1, xdev(p))
    sent(back, ncol - 1, 1)

    done(l_rot)
    done(l_tab)
    cos_t, sin_t = trg[0], trg[1]
    for s in range(SEQS):
        low = crot[s, pl.ds(0, half), :].astype(F32)
        high = crot[s, pl.ds(half, half), :].astype(F32)
        krot[s, pl.ds(0, half), :] = low * cos_t - high * sin_t
        krot[s, pl.ds(half, half), :] = low * sin_t + high * cos_t
    spread_r = iota((LOCAL_HEADS * HEAD_KEY, QW), 0)
    spread = ones_where(iota((LOCAL_HEADS * HEAD_KEY, QW), 1) == spread_r + HEAD_ROT * (spread_r >> log2(HEAD_KEY)))
    ka[pl.ds(0, LATENT), :] = dot(keyup[...], spread).astype(BF16)
    lane_q = iota((256, QW), 1)
    head_q = ones_where(lane_q >= PER_HEAD, jnp.int32)
    for h in range(2, LOCAL_HEADS):
        head_q = head_q + ones_where(lane_q >= h * PER_HEAD, jnp.int32)
    within = lane_q - PER_HEAD * head_q - HEAD_KEY
    row_q = iota((256, QW), 0)
    want = jnp.where(row_q < 128, row_q, (row_q - 128) ^ half)
    limit = jnp.where(row_q < 128, row_q, row_q - 128)
    ka[pl.ds(LATENT, 256), :] = ones_where((within == want) & (limit < HEAD_ROT))
    rot_rows = iota((128, pf), 0)
    rot_w = jnp.where((rot_rows & 63) < HEAD_ROT, rotw[...].astype(F32), 0.0).astype(BF16)

    arrived(crit, ncol - 1, 0)
    r_i, b_i = iota((rows, batch), 0), iota((rows, batch), 1)
    sel_a = ones_where(b_i == (r_i >> 1) * (ncol * SEQS) + col * SEQS + (r_i & 1))
    hid = crit[:, :, pl.ds(QW + lq, batch)].reshape(pf, batch)
    h_t = dot(sel_a, hid, NT)
    ht[...] = h_t
    scaled = (h_t * again[pl.ds(z, 1), :]).astype(BF16)
    main = dot(scaled, crit[:, :, pl.ds(0, QW + lq)].reshape(pf, QW + lq))
    rot = dot(scaled, rot_w, NT)
    square = jnp.sum(h_t * h_t, axis=1, keepdims=True)
    rot = jnp.where(iota((rows, 128), 1) == HEAD_ROT, square, rot)
    aw = QW + lq + 128
    pall[:, pl.ds(0, QW + lq)] = main
    pall[:, pl.ds(QW + lq, 128)] = rot
    for i in range(nz):
        za_s[i] = pall[pl.ds(SEQS * i, SEQS), :]
    for p in z_peers:
        send(za_s.at[p], za_r.at[z], 2, zdev(p))
    sent(za_s, nz - 1, 2)
    za_r[pl.ds(z, 1)] = za_s[pl.ds(z, 1)]

    rs = scores[...]
    rw = ROUTED_SCALE * rs / jnp.sum(rs, axis=1, keepdims=True)
    idv = ids[...]
    target = iota((batch, 128), 1) * ncol + col
    hit = jnp.zeros((batch, 128), F32)
    wgt = jnp.zeros((batch, 128), F32)
    for k in range(4):
        same = idv[:, k : k + 1] == target
        hit = jnp.where(same, 1.0, hit)
        wgt = jnp.where(same, rw[:, k : k + 1], wgt)
    before = ones_where(iota((batch, batch), 1) < iota((batch, batch), 0))
    rank = dot(before, hit.astype(BF16))
    val = jnp.where(hit > 0.0, rank, -1.0).astype(BF16)
    expand = ones_where(iota((nslot, 128), 1) == (iota((nslot, 128), 0) >> log2(SLOTS)))
    slot_i = (iota((nslot, batch), 0) & (SLOTS - 1)).astype(F32)
    in_slot = dot(expand, val, NT) == slot_i
    w_hi = wgt.astype(BF16)
    w_lo = (wgt - w_hi.astype(F32)).astype(BF16)
    wt[pl.ds(0, nslot), :] = jnp.where(in_slot, dot(expand, w_hi, NT), 0.0).astype(BF16)
    wt[pl.ds(nslot, nslot), :] = jnp.where(in_slot, dot(expand, w_lo, NT), 0.0).astype(BF16)

    def natural(p):
        return ((p >> 1) & (nz - 1)) * (ncol * SEQS) + (p >> log2(rows)) * SEQS + (p & 1)

    perm = ones_where(iota((batch, batch), 0) == natural(iota((batch, batch), 1)))
    sel_p[...] = dot(ones_where(in_slot), perm).astype(BF16)

    arrived(za_r, nz - 1, 2)
    tot = za_r[0]
    for i in range(1, nz):
        tot = tot + za_r[i]
    lane2 = iota((SEQS, 128), 1)
    tail = tot[:, QW + lq : aw]
    sq = jnp.sum(jnp.where(lane2 == HEAD_ROT, tail, 0.0), axis=1, keepdims=True)
    scale = lax.rsqrt(sq / width + EPSILON)
    yb[pl.ds(y, 1)] = rounded(tot[:, QW : QW + lq] * scale).reshape(1, SEQS, lq)
    for p in y_peers:
        send(yb.at[y], yb.at[y], 3, ydev(p))
    sent(yb, nt - 1, 3)
    q = rounded(tot[:, :QW] * scale)
    nrows = SEQS * LOCAL_HEADS
    r8 = iota((nrows, 128), 0)
    first8 = r8 < LOCAL_HEADS

    def per_row(v):
        top = iota((nrows, v.shape[1]), 0) < LOCAL_HEADS
        return jnp.where(top, v[0:1, :], v[1:2, :])

    lane_8 = iota((nrows, QW), 1)
    first = (iota((nrows, QW), 0) & (LOCAL_HEADS - 1)) * PER_HEAD
    q8 = jnp.where((lane_8 >= first) & (lane_8 < first + PER_HEAD), per_row(q), 0.0).astype(BF16)
    qa = dot(q8, ka[...], NT)
    absorbed = qa[:, :LATENT].astype(BF16)
    len8 = jnp.where(first8, lens[0], lens[1])
    angle = len8.astype(F32) * fr[...]
    cos8 = jnp.cos(angle)
    lane8 = iota((nrows, 128), 1)
    sin8 = jnp.where((lane8 & half) == 0, -jnp.sin(angle), jnp.sin(angle))
    q_rot = qa[:, LATENT : LATENT + 128] * cos8 + qa[:, LATENT + 128 : LATENT + 256] * sin8

    done(l_att)
    q32 = q_rot[:, :HEAD_ROT]
    per_seq = [dot(absorbed, cache[s], NT) + dot(q32, krot[s], NN, HIGHEST) for s in range(SEQS)]
    top_rows = iota((nrows, CACHE), 0) < LOCAL_HEADS
    score_scale = PER_HEAD**-0.5
    live = iota((nrows, CACHE), 1) < jnp.where(top_rows, lens[0], lens[1])
    cache_score = jnp.where(live, score_scale * jnp.where(top_rows, per_seq[0], per_seq[1]), -1e30)
    best = jnp.max(cache_score, axis=1, keepdims=True)

    new_rot = rounded(tail * scale)
    o_rotkey[...] = new_rot[:, :HEAD_ROT].astype(BF16)
    new_swap = pltpu.roll(new_rot, 64, 1)
    own_rot = jnp.where(lane8 < HEAD_ROT, per_row(new_rot) * cos8 + per_row(new_swap) * sin8, 0.0)

    arrived(yb, nt - 1, 3)
    raw = jnp.concatenate([yb[i] for i in range(nt)], axis=1)
    new_latent = (
        raw * lax.rsqrt(jnp.mean(raw * raw, axis=1, keepdims=True) + EPSILON) * lgain[...]
    ).astype(BF16)
    o_latent[...] = new_latent
    lat8 = per_row(new_latent.astype(F32))
    own_score = score_scale * (
        jnp.sum(absorbed.astype(F32) * lat8, axis=1, keepdims=True)
        + jnp.sum(q_rot * own_rot, axis=1, keepdims=True)
    )
    top_score = jnp.maximum(best, own_score)
    cache_weight = jnp.exp(cache_score - top_score)
    own_weight = jnp.exp(own_score - top_score)
    denominator = jnp.sum(cache_weight, axis=1, keepdims=True) + own_weight
    prob = (cache_weight / denominator).astype(BF16)
    own_prob = rounded(own_weight / denominator)
    ctx = [dot(prob, cache[s]) for s in range(SEQS)]
    top_rows = iota((nrows, LATENT), 0) < LOCAL_HEADS
    context = jnp.where(top_rows, ctx[0], ctx[1]) + own_prob * lat8
    ho = dot(context.astype(BF16), valup[...])
    r_h = iota((nrows, HV), 0)
    ho = jnp.where((iota((nrows, HV), 1) >> log2(HEAD_VAL)) == (r_h & (LOCAL_HEADS - 1)), ho, 0.0)
    h0 = jnp.sum(jnp.where(r_h < LOCAL_HEADS, ho, 0.0), axis=0, keepdims=True)
    h1 = jnp.sum(jnp.where(r_h < LOCAL_HEADS, 0.0, ho), axis=0, keepdims=True)
    heads = rounded(jnp.where(iota((SEQS, HV), 0) == 0, h0, h1))
    zd[pl.ds(z, 1)] = heads.reshape(1, SEQS, HV)
    for p in z_peers:
        send(zd.at[z], zd.at[z], 4, zdev(p))
    sent(zd, nz - 1, 4)

    arrived(back, ncol - 1, 1)
    arrived(zd, nz - 1, 4)
    for i in range(nz):
        h32[pl.ds(SEQS * i, SEQS), :] = zd[i]
    part = dot(h32[...].astype(BF16), back[:, :, pl.ds(0, HV)].reshape(pf, HV), NT)
    ye[pl.ds(y, 1)] = part.reshape(1, rows, pf)
    for p in y_peers:
        send(ye.at[y], ye.at[y], 5, ydev(p))
    sent(ye, nt - 1, 5)
    arrived(ye, nt - 1, 5)
    attn = ye[0]
    for i in range(1, nt):
        attn = attn + ye[i]
    mid = (ht[...] + rounded(attn)).astype(BF16)
    midx[pl.ds(col, 1)] = mid.reshape(1, rows, pf)
    for p in x_peers:
        send(midx.at[col], midx.at[col], 6, xdev(p))
    sent(midx, ncol - 1, 6)
    mid_v = mid.astype(F32)
    ffn = (mid_v * fgain[pl.ds(z, 1), :]).astype(BF16)
    shf[:, pl.ds(0, 2 * HIDDEN)] = dot(ffn, back[:, :, pl.ds(HV, 2 * HIDDEN)].reshape(pf, 2 * HIDDEN))
    shf[:, pl.ds(2 * HIDDEN, 128)] = jnp.broadcast_to(jnp.sum(mid_v * mid_v, axis=1, keepdims=True), (rows, 128))
    for i in range(nz):
        zf_s[i] = shf[pl.ds(SEQS * i, SEQS), :]
    for p in z_peers:
        send(zf_s.at[p], zf_r.at[z], 7, zdev(p))
    sent(zf_s, nz - 1, 7)
    zf_r[pl.ds(z, 1)] = zf_s[pl.ds(z, 1)]

    arrived(midx, ncol - 1, 6)
    mid_all = midx[...].reshape(batch, pf)
    zg_s[...] = dot(sel_p[...], mid_all).astype(BF16).reshape(nz, SLOTS, pf)
    for p in z_peers:
        send(zg_s.at[p], zg_r.at[z], 8, zdev(p))
    sent(zg_s, nz - 1, 8)
    zg_r[pl.ds(z, 1)] = zg_s[pl.ds(z, 1)]
    own_f = ones_where(iota((FEATS, pf), 1) == iota((FEATS, pf), 0) + col * FEATS)
    mid_t = dot(own_f, mid_all, NT).astype(BF16)
    to_half = ones_where(natural(iota((batch, hl), 0)) == iota((batch, hl), 1) + (y >> 1) * hl)
    mid_own = dot(mid_t, to_half)

    arrived(zf_r, nz - 1, 7)
    tot = zf_r[0]
    for i in range(1, nz):
        tot = tot + zf_r[i]
    scale = lax.rsqrt(tot[:, 2 * HIDDEN : 2 * HIDDEN + 1] / width + EPSILON)
    gate = scale * tot[:, :HIDDEN]
    act = rounded(gate / (1.0 + jnp.exp(-gate)) * (scale * tot[:, HIDDEN : 2 * HIDDEN]))
    zs[pl.ds(z, 1)] = act.reshape(1, SEQS, HIDDEN)
    for p in z_peers:
        send(zs.at[z], zs.at[z], 9, zdev(p))
    sent(zs, nz - 1, 9)

    done(l_exp)
    arrived(zg_r, nz - 1, 8)
    pieces = []
    sq = jnp.zeros((SLOTS, 1), F32)
    for i in range(nz):
        v = zg_r[i].astype(F32)
        sq = sq + jnp.sum(v * v, axis=1, keepdims=True)
        pieces.append((v * fgain[pl.ds(i, 1), :]).astype(BF16))
    gu = dot(jnp.concatenate(pieces, axis=1), wgu[...])
    scale = lax.rsqrt(sq / width + EPSILON)
    gate = scale * gu[:, :HIDDEN]
    act = (gate / (1.0 + jnp.exp(-gate)) * (scale * gu[:, HIDDEN:])).astype(BF16)
    out = dot(act, wd[...])
    for i in range(nz):
        zh_s[i] = out[:, pf * i : pf * (i + 1)].astype(BF16)
    for p in z_peers:
        send(zh_s.at[p], zh_r.at[z], 10, zdev(p))
    sent(zh_s, nz - 1, 10)
    zh_r[pl.ds(z, 1)] = zh_s[pl.ds(z, 1)]

    arrived(zs, nz - 1, 9)
    for i in range(nz):
        s32[pl.ds(SEQS * i, SEQS), :] = zs[i]
    place = ones_where(
        iota((batch, rows), 0) == (iota((batch, rows), 1) >> 1) * (ncol * SEQS) + col * SEQS + (iota((batch, rows), 1) & 1)
    )
    spread_act = dot(place, s32[...].astype(BF16)).astype(BF16)
    total = dot(back[:, :, pl.ds(HV + 2 * HIDDEN, HIDDEN)].reshape(pf, HIDDEN), spread_act, NT)
    arrived(zh_r, nz - 1, 10)
    parts = zh_r[...].reshape(nslot, pf)
    total = total + dot(parts, wt[pl.ds(0, nslot), :], TN) + dot(parts, wt[pl.ds(nslot, nslot), :], TN)
    xr_s[...] = total.reshape(ncol, FEATS, batch)
    for p in x_peers:
        send(xr_s.at[p], xr_r.at[col], 11, xdev(p))
    sent(xr_s, ncol - 1, 11)
    xr_r[pl.ds(col, 1)] = xr_s[pl.ds(col, 1)]
    arrived(xr_r, ncol - 1, 11)
    tot = xr_r[0]
    for i in range(1, ncol):
        tot = tot + xr_r[i]
    for i in range(nt // 2):
        yo_s[i] = tot[:, hl * i : hl * (i + 1)].astype(BF16)
    for p in y_peers:
        send(yo_s.at[p >> 1], yo_r.at[y], 12, ydev(p))
    sent(yo_r, nt - 1, 12)
    yo_r[pl.ds(y, 1)] = yo_s[pl.ds(y >> 1, 1)]
    arrived(yo_r, nt - 1, 12)
    tot = yo_r[0].astype(F32)
    for i in range(1, nt):
        tot = tot + yo_r[i].astype(F32)
    res = mid_own + tot
    res = jnp.where((y & 1) == 1, pltpu.roll(res, ob, 1), res)
    o_mixed[...] = res[:, :ob].astype(BF16)

    for buf, n, k in pending:
        part = buf.at[pl.ds(0, n)]
        pltpu.make_async_copy(part, part, ssem.at[k]).wait()


def body(nz, nx, nc, nt, *args):
    args = list(args)
    ncol = nx * nc
    pf = FEATS * ncol
    rows = SEQS * nz
    batch = rows * ncol
    lq = LATENT // nt
    nslot = nz * SLOTS
    hl = 2 * (batch // nt)
    aw = QW + lq + 128
    for i in (1, 12):
        args[i] = args[i].reshape(nz, pf)
    args[5] = args[5].reshape(1, LATENT)
    half = HEAD_ROT // 2
    frequency = THETA_BASE ** (-np.arange(half, dtype=np.float64) / half)
    angles = frequency.astype(np.float32)[:, None] * np.arange(CACHE, dtype=np.float32)[None, :]
    trig = jnp.asarray(np.stack([np.cos(angles.astype(np.float64)), np.sin(angles.astype(np.float64))]).astype(np.float32))
    freq = jnp.asarray(np.tile(frequency.astype(np.float32), 128 // half)[None, :])
    vm = pltpu.VMEM
    scratch = [
        vm((ncol, FEATS, QW + lq + batch), BF16),
        vm((ncol, FEATS, HV + 3 * HIDDEN), BF16),
        vm((128, pf), BF16),
        vm((nz, pf), F32), vm((nz, pf), F32), vm((1, LATENT), F32), vm((1, 128), F32),
        vm((LATENT, LOCAL_HEADS * HEAD_KEY), BF16), vm((LATENT, HV), BF16),
        vm((SEQS, CACHE, LATENT), BF16), vm((SEQS, HEAD_ROT, CACHE), BF16),
        pltpu.SMEM((SEQS,), jnp.int32),
        vm((batch, 4), jnp.int32), vm((batch, 4), F32),
        vm((pf * nz, 2 * HIDDEN), BF16), vm((HIDDEN, pf * nz), BF16),
        vm((2, half, CACHE), F32),
        vm((nz, SEQS, aw), F32), vm((nz, SEQS, aw), F32),
        vm((nt, SEQS, lq), F32),
        vm((nz, SEQS, HV), F32),
        vm((nt, rows, pf), F32),
        vm((ncol, rows, pf), BF16),
        vm((nz, SEQS, 2 * HIDDEN + 128), F32), vm((nz, SEQS, 2 * HIDDEN + 128), F32),
        vm((nz, SLOTS, pf), BF16), vm((nz, SLOTS, pf), BF16),
        vm((nz, SLOTS, pf), BF16), vm((nz, SLOTS, pf), BF16),
        vm((nz, SEQS, HIDDEN), F32),
        vm((ncol, FEATS, batch), F32), vm((ncol, FEATS, batch), F32),
        vm((nt // 2, FEATS, hl), BF16), vm((nt, FEATS, hl), BF16),
        vm((LATENT + 256, QW), BF16),
        vm((SEQS, HEAD_ROT, CACHE), F32),
        vm((nslot, batch), BF16),
        vm((2 * nslot, batch), BF16),
        vm((rows, pf), F32),
        vm((rows, HV), F32),
        vm((rows, HIDDEN), F32),
        vm((rows, aw), F32),
        vm((rows, 2 * HIDDEN + 128), F32),
        pltpu.SemaphoreType.DMA((25,)),
        pltpu.SemaphoreType.DMA((13,)),
        pltpu.SemaphoreType.DMA((13,)),
    ]
    anywhere = pl.BlockSpec(memory_space=pl.ANY)
    return pl.pallas_call(
        functools.partial(kernel, nz, nx, nc, nt),
        out_shape=(
            jax.ShapeDtypeStruct((FEATS, batch // nt), BF16),
            jax.ShapeDtypeStruct((SEQS, LATENT), BF16),
            jax.ShapeDtypeStruct((SEQS, HEAD_ROT), BF16),
        ),
        in_specs=[anywhere] * 23,
        out_specs=(pl.BlockSpec(memory_space=pltpu.VMEM),) * 3,
        scratch_shapes=scratch,
        compiler_params=pltpu.CompilerParams(collective_id=0, has_side_effects=True, vmem_limit_bytes=40 * 2**20),
        name="layer",
    )(*args, trig, freq)


EP = ("z", "x", "c")


def build(devices):
    split = Mesh(devices, ("z", "x", "c", "y"))
    return jax.shard_map(
        functools.partial(body, *devices.shape),
        mesh=split,
        in_specs=(
            P(EP, None),
            P(),
            P(EP, "y"),
            P(EP, None),
            P(),
            P(),
            P(None, "y"),
            P(None, "y"),
            P(EP, None),
            P(EP, None, None),
            P(EP, None, None),
            P(EP),
            P(),
            P(),
            P(),
            P(EP, None, "y"),
            P(EP, None, "y"),
            P(EP, "y", None),
            P(EP, "y"),
            P(EP, "y"),
            P(EP, "y"),
        ),
        out_specs=(P(EP, "y"), P(EP, None), P(EP, None)),
        check_vma=False,
    )


def solution(mesh):
    return build(mesh.devices.reshape(16, 4, 2, mesh.shape["tp"]))
```

time: 236 us -> 94.5 us (0.40)
  waiting for transfers between devices: 78 us -> 0 us
  Pallas kernels: 0 us -> 72 us
  starting transfers between devices: 63 us -> 0 us
  local copies, waits for them, and re-layouts: 45.4 us -> 21 us
  blocking collectives: 17 us -> 0 us
  other arithmetic: 16.9 us -> 0 us
  matrix products: 12.3 us -> 0 us
    all_to_all x10 -> x0, waiting for transfers between devices: 78 us -> none  [the longest x4 26.7 us: copy_for_each(): lax.all_to_all(jnp.broadcast_to(value[None], (devices, *value.shape)), ax...]
    pallas_call x0 -> x1, Pallas kernels: none -> 72 us  [body(): pl.pallas_call(functools.partial(kernel, nz, nx, nc, nt), out_shape=(jax....]
    all_to_all x10 -> x0, starting transfers between devices: 63 us -> none  [the longest x4 23.5 us: copy_for_each(): lax.all_to_all(jnp.broadcast_to(value[None], (devices, *value.shape)), ax...]
    all_to_all x2 -> x0, blocking collectives: 17 us -> none  [the longest x1 10.7 us: summed_on_arrival(): lax.all_to_all(pieces, axis, split_axis=0, concat_axis=0, tiled=True)]
    gather x5 -> x0, local copies, waits for them, and re-layouts: 14.4 us -> none  [the longest x3 7.73 us: body(): jnp.take(padded_rows, slot_row, axis=0).reshape(ep_count, SLOTS * features)]
    dot_general x16 -> x0, matrix products: 12.3 us -> none  [the longest x1 3.64 us: body(): jnp.einsum('jsh,fjh->fjs', piece.reshape(count, local_seqs, head_cols), c...]
    unnamed x45 -> x47, local copies, waits for them, and re-layouts: 9.14 us -> 21 us
    convert_element_type x9 -> x0, other arithmetic: 5.07 us -> none  [the longest x1 0.93 us: body(): rot_values = cache_rotkey.astype(jnp.float32)]
  transfers between devices with their start and end apart: 10 -> 0, of which waited for: 9 -> 0; matrix products, arithmetic and copies ran while one was open for 21% -> 0% of each run, Pallas kernels for 0% -> 0%
where the time goes in v1:
time: 94.5 us; the launch traced here: 93.6 us
  Pallas kernels  72 us (76%)
  local copies, waits for them, and re-layouts  21 us (22%)
    pallas_call x1, Pallas kernels, body(): pl.pallas_call(functools.partial(kernel, nz, nx, nc, nt), out_shape=(jax....  72 us
    unnamed x47, local copies, waits for them, and re-layouts  21 us

profile of v1, /device:TPU:1, one launch (start us, length us, event | category | flops | bytes accessed | tf_op | source)
XLA Modules:
  0.0 93.6 jit_solution(3260742597144325321)
XLA Ops:
  0.6 0.8 copy.26.refs_13_
  1.5 0.8 copy.27.refs_14_
  2.3 0.0 copy-start
  2.3 1.6 %copy-done = bf16[2,1024,512]{2,1,0:T(8,128)(2,1)S(1)} copy-done((bf16[2,1024,512]{2,1,0:T(8,128)(2,1)S(1)}, bf16[2,1024,512]{2,1,0:T(8,128)(2,1)}, u32[]{:S(2)}) %copy-start) | copy-done | bytes 2097176
  3.9 0.0 copy-start.1
  3.9 1.0 %copy-done.1 = bf16[1,2048,128]{2,1,0:T(8,128)(2,1)S(1)} copy-done((bf16[1,2048,128]{2,1,0:T(8,128)(2,1)S(1)}, bf16[1,2048,128]{2,1,0:T(8,128)(2,1)}, u32[]{:S(2)}) %copy-start.1) | copy-done | bytes 524312
  4.9 0.0 copy-start.2
  4.9 1.0 %copy-done.2 = bf16[1,2048,128]{2,1,0:T(8,128)(2,1)S(1)} copy-done((bf16[1,2048,128]{2,1,0:T(8,128)(2,1)S(1)}, bf16[1,2048,128]{2,1,0:T(8,128)(2,1)}, u32[]{:S(2)}) %copy-start.2) | copy-done | bytes 524312
  6.0 0.0 copy-start.3
  6.0 1.0 %copy-done.3 = bf16[1,128,2048]{2,1,0:T(8,128)(2,1)S(1)} copy-done((bf16[1,128,2048]{2,1,0:T(8,128)(2,1)S(1)}, bf16[1,128,2048]{2,1,0:T(8,128)(2,1)}, u32[]{:S(2)}) %copy-start.3) | copy-done | bytes 524312
  7.0 0.0 copy-start.4
  7.0 0.9 %copy-done.4 = bf16[512,256]{1,0:T(8,128)(2,1)S(1)} copy-done((bf16[512,256]{1,0:T(8,128)(2,1)S(1)}, bf16[512,256]{1,0:T(8,128)(2,1)}, u32[]{:S(2)}) %copy-start.4) | copy-done | bytes 262168
  8.0 0.9 %copy-done.5 = bf16[512,256]{1,0:T(8,128)(2,1)S(1)} copy-done((bf16[512,256]{1,0:T(8,128)(2,1)S(1)}, bf16[512,256]{1,0:T(8,128)(2,1)}, u32[]{:S(2)}) %copy-start.5) | copy-done | bytes 262168
  8.9 0.9 copy-done.6
  9.8 0.9 copy-done.7
  10.7 0.9 copy-done.8
  11.6 0.8 copy-done.9
  12.4 0.7 copy-done.10
  13.1 0.7 copy-done.11
  13.8 0.7 copy-done.12
  14.5 0.7 copy-done.13
  15.2 0.7 copy-done.14
  15.9 0.7 copy-done.15
  16.6 0.7 copy-done.16
  17.3 0.7 copy-done.17
  18.0 0.7 copy-done.18
  18.6 0.7 copy-done.19
  19.3 0.7 copy-done.20
  19.9 72.0 %layer.1 = (bf16[16,64]{1,0:T(8,128)(2,1)S(1)}, bf16[2,512]{1,0:T(2,128)(2,1)S(1)}, bf16[2,32]{1,0:T(2,128)(2,1)S(1)}) custom-call(bf16[16,256]{1,0:T(8,128)(2,1)S(1)} %copy-done.12, f32[16,128]{1,0:T(8,128)S(1)} %bitcast.3, bf16[16,384]{1,0:T(8,128)(2,1)S(1)} %copy-done.11, bf16[16,512]{1,0:T(8,128)(2,1)S(1)} %copy-done.10, bf16[32,2048]{1,0:T(8,128)(2,1)S(1)} %copy-done.6, ...), custom_call_target="tpu_custom_call" | custom-call | tf_op jit(solution)/shard_map/layer/pallas_call | solution.py:491
  91.9 0.6 copy.31
  92.5 0.6 copy.32
  93.1 0.5 copy.33
  (16 shorter events, 0.0 us)
Async XLA Ops:
  2.3 1.6 %copy-start = (bf16[2,1024,512]{2,1,0:T(8,128)(2,1)S(1)}, bf16[2,1024,512]{2,1,0:T(8,128)(2,1)}, u32[]{:S(2)}) copy-start(bf16[2,1024,512]{2,1,0:T(8,128)(2,1)} %refs_9_.1) | copy-start | bytes 6291460
  3.9 1.0 %copy-start.1 = (bf16[1,2048,128]{2,1,0:T(8,128)(2,1)S(1)}, bf16[1,2048,128]{2,1,0:T(8,128)(2,1)}, u32[]{:S(2)}) copy-start(bf16[1,2048,128]{2,1,0:T(8,128)(2,1)} %refs_15_.1) | copy-start | bytes 1572868
  4.9 1.0 %copy-start.2 = (bf16[1,2048,128]{2,1,0:T(8,128)(2,1)S(1)}, bf16[1,2048,128]{2,1,0:T(8,128)(2,1)}, u32[]{:S(2)}) copy-start(bf16[1,2048,128]{2,1,0:T(8,128)(2,1)} %refs_16_.1) | copy-start | bytes 1572868
  6.0 1.0 %copy-start.3 = (bf16[1,128,2048]{2,1,0:T(8,128)(2,1)S(1)}, bf16[1,128,2048]{2,1,0:T(8,128)(2,1)}, u32[]{:S(2)}) copy-start(bf16[1,128,2048]{2,1,0:T(8,128)(2,1)} %refs_17_.1) | copy-start | bytes 1572868
  7.0 0.9 %copy-start.4 = (bf16[512,256]{1,0:T(8,128)(2,1)S(1)}, bf16[512,256]{1,0:T(8,128)(2,1)}, u32[]{:S(2)}) copy-start(bf16[512,256]{1,0:T(8,128)(2,1)} %refs_6_.1) | copy-start | bytes 786436
  8.0 0.9 %copy-start.5 = (bf16[512,256]{1,0:T(8,128)(2,1)S(1)}, bf16[512,256]{1,0:T(8,128)(2,1)}, u32[]{:S(2)}) copy-start(bf16[512,256]{1,0:T(8,128)(2,1)} %refs_7_.1) | copy-start | bytes 786436
  8.9 0.9 copy-start.6
  9.8 0.9 copy-start.7
  10.7 0.9 copy-start.8
  11.6 0.8 copy-start.9
  12.4 0.7 copy-start.10
  13.1 0.7 copy-start.11
  13.8 0.7 copy-start.12
  14.5 0.7 copy-start.13
  15.2 0.7 copy-start.14
  15.9 0.7 copy-start.15
  16.6 0.7 copy-start.16
  17.3 0.7 copy-start.17
  18.0 0.7 copy-start.18
  18.6 0.7 copy-start.19
  19.3 0.7 copy-start.20

commit v2 on v1

--- a/solution.py
+++ b/solution.py
@@ -217,25 +217,25 @@
     za_r[pl.ds(z, 1)] = za_s[pl.ds(z, 1)]
 
     rs = scores[...]
-    rw = ROUTED_SCALE * rs / jnp.sum(rs, axis=1, keepdims=True)
+    rw = ROUTED_SCALE * rs / jnp.sum(rs, axis=0, keepdims=True)
     idv = ids[...]
-    target = iota((batch, 128), 1) * ncol + col
-    hit = jnp.zeros((batch, 128), F32)
-    wgt = jnp.zeros((batch, 128), F32)
+    target = iota((nz, batch), 0) * ncol + col
+    hit = jnp.zeros((nz, batch), F32)
+    wgt = jnp.zeros((nz, batch), F32)
     for k in range(4):
-        same = idv[:, k : k + 1] == target
+        same = idv[k : k + 1, :] == target
         hit = jnp.where(same, 1.0, hit)
-        wgt = jnp.where(same, rw[:, k : k + 1], wgt)
-    before = ones_where(iota((batch, batch), 1) < iota((batch, batch), 0))
-    rank = dot(before, hit.astype(BF16))
+        wgt = jnp.where(same, rw[k : k + 1, :], wgt)
+    before = ones_where(iota((batch, batch), 0) < iota((batch, batch), 1))
+    rank = dot(hit.astype(BF16), before)
     val = jnp.where(hit > 0.0, rank, -1.0).astype(BF16)
-    expand = ones_where(iota((nslot, 128), 1) == (iota((nslot, 128), 0) >> log2(SLOTS)))
+    expand = ones_where(iota((nslot, nz), 1) == (iota((nslot, nz), 0) >> log2(SLOTS)))
     slot_i = (iota((nslot, batch), 0) & (SLOTS - 1)).astype(F32)
-    in_slot = dot(expand, val, NT) == slot_i
+    in_slot = dot(expand, val) == slot_i
     w_hi = wgt.astype(BF16)
     w_lo = (wgt - w_hi.astype(F32)).astype(BF16)
-    wt[pl.ds(0, nslot), :] = jnp.where(in_slot, dot(expand, w_hi, NT), 0.0).astype(BF16)
-    wt[pl.ds(nslot, nslot), :] = jnp.where(in_slot, dot(expand, w_lo, NT), 0.0).astype(BF16)
+    wt[pl.ds(0, nslot), :] = jnp.where(in_slot, dot(expand, w_hi), 0.0).astype(BF16)
+    wt[pl.ds(nslot, nslot), :] = jnp.where(in_slot, dot(expand, w_lo), 0.0).astype(BF16)
 
     def natural(p):
         return ((p >> 1) & (nz - 1)) * (ncol * SEQS) + (p >> log2(rows)) * SEQS + (p & 1)
@@ -446,6 +446,7 @@
     for i in (1, 12):
         args[i] = args[i].reshape(nz, pf)
     args[5] = args[5].reshape(1, LATENT)
+    args[13], args[14] = args[13].T, args[14].T
     half = HEAD_ROT // 2
     frequency = THETA_BASE ** (-np.arange(half, dtype=np.float64) / half)
     angles = frequency.astype(np.float32)[:, None] * np.arange(CACHE, dtype=np.float32)[None, :]
@@ -460,7 +461,7 @@
         vm((LATENT, LOCAL_HEADS * HEAD_KEY), BF16), vm((LATENT, HV), BF16),
         vm((SEQS, CACHE, LATENT), BF16), vm((SEQS, HEAD_ROT, CACHE), BF16),
         pltpu.SMEM((SEQS,), jnp.int32),
-        vm((batch, 4), jnp.int32), vm((batch, 4), F32),
+        vm((4, batch), jnp.int32), vm((4, batch), F32),
         vm((pf * nz, 2 * HIDDEN), BF16), vm((HIDDEN, pf * nz), BF16),
         vm((2, half, CACHE), F32),
         vm((nz, SEQS, aw), F32), vm((nz, SEQS, aw), F32),
@@ -487,7 +488,7 @@
         pltpu.SemaphoreType.DMA((13,)),
         pltpu.SemaphoreType.DMA((13,)),
     ]
-    anywhere = pl.BlockSpec(memory_space=pl.ANY)
+    anywhere = pl.BlockSpec(memory_space=pltpu.HBM)
     return pl.pallas_call(
         functools.partial(kernel, nz, nx, nc, nt),
         out_shape=(
@@ -498,7 +499,7 @@
         in_specs=[anywhere] * 23,
         out_specs=(pl.BlockSpec(memory_space=pltpu.VMEM),) * 3,
         scratch_shapes=scratch,
-        compiler_params=pltpu.CompilerParams(collective_id=0, has_side_effects=True, vmem_limit_bytes=40 * 2**20),
+        compiler_params=pltpu.CompilerParams(collective_id=0, has_side_effects=True, vmem_limit_bytes=67043328),
         name="layer",
     )(*args, trig, freq)
 

time: 94.5 us -> 77.2 us (0.82)
  local copies, waits for them, and re-layouts: 21 us -> 3.67 us
    unnamed x47 -> x3, local copies, waits for them, and re-layouts: 21 us -> 3.67 us
where the time goes in v2:
time: 77.2 us; the launch traced here: 77 us
  Pallas kernels  72.7 us (94%)
  local copies, waits for them, and re-layouts  3.67 us (5%)
    pallas_call x1, Pallas kernels, body(): pl.pallas_call(functools.partial(kernel, nz, nx, nc, nt), out_shape=(jax....  72.7 us
    unnamed x3, local copies, waits for them, and re-layouts  3.67 us

profile of v2, /device:TPU:1, one launch (start us, length us, event | category | flops | bytes accessed | tf_op | source)
XLA Modules:
  0.0 77.0 jit_solution(2868180292532472123)
XLA Ops:
  0.6 72.7 %layer.1 = (bf16[16,64]{1,0:T(8,128)(2,1)}, bf16[2,512]{1,0:T(2,128)(2,1)}, bf16[2,32]{1,0:T(2,128)(2,1)}) custom-call(bf16[16,256]{1,0:T(8,128)(2,1)} %refs_0_.1, f32[16,128]{1,0:T(8,128)} %bitcast.5, bf16[16,384]{1,0:T(8,128)(2,1)} %refs_2_.1, bf16[16,512]{1,0:T(8,128)(2,1)} %refs_3_.1, bf16[32,2048]{1,0:T(8,128)(2,1)} %refs_4_.1, f32[1,512]{1,0:T(1,128)} %bitcast.9, ...), custom_call_target="tpu_custom_call" | custom-call | tf_op jit(solution)/shard_map/layer/pallas_call | solution.py:492
  73.3 1.3 %copy.29 = bf16[16,64]{1,0:T(8,128)(2,1)} copy(bf16[16,64]{1,0:T(8,128)(2,1)} %get-tuple-element.6) | data formatting | bytes 4096
  74.6 1.2 %copy.30 = bf16[2,512]{1,0:T(2,128)(2,1)} copy(bf16[2,512]{1,0:T(2,128)(2,1)} %get-tuple-element.7) | data formatting | bytes 4096
  75.8 1.2 %copy.31 = bf16[2,32]{1,0:T(2,128)(2,1)} copy(bf16[2,32]{1,0:T(2,128)(2,1)} %get-tuple-element.8) | data formatting | bytes 256

commit v3 on v2

--- a/solution.py
+++ b/solution.py
@@ -62,9 +62,9 @@
         trig, freq,
         o_mixed, o_latent, o_rotkey,
         crit, back, rotw, again, fgain, lgain, fr, keyup, valup, cache, crot, lens, ids, scores, wgu, wd, trg,
-        za_s, za_r, yb, zd, ye, midx, zf_s, zf_r, zg_s, zg_r, zh_s, zh_r, zs, xr_s, xr_r, yo_s, yo_r,
+        za_s, za_r, yb, hs, zd, midx, zf_s, zf_r, zg_s, zg_r, zh_s, zh_r, zs, pd_s, pd_r,
         ka, krot, sel_p, wt, ht, h32, s32, pall, shf,
-        lsem, ssem, rsem,
+        lsem, ssem, rsem, ok,
     ) = refs
     ncol = nx * nc
     pf = FEATS * ncol
@@ -75,6 +75,8 @@
     nslot = nz * SLOTS
     ob = batch // nt
     hl = 2 * ob
+    aow = nt * HV
+    zy = nz // nt
     z, x, c, y = (lax.axis_index(a) for a in ("z", "x", "c", "y"))
     col = x * nc + c
 
@@ -90,17 +92,34 @@
     def ydev(p):
         return {"y": p}
 
-    x_peers = [lax.rem(col + d, ncol) for d in range(1, ncol)]
+    x_order = sorted(range(1, ncol), key=lambda d: -min(d, ncol - d))
+    x_peers = [lax.rem(col + d, ncol) for d in x_order]
     y_peers = [lax.rem(y + d, nt) for d in range(1, nt)]
     z_peers = [p for (p,) in z_peers]
+    plane_order = sorted(
+        [(dx, dc, dy) for dx in range(nx) for dc in range(nc) for dy in range(nt) if dx or dc or dy],
+        key=lambda t: -(min(t[0], nx - t[0]) + min(t[2], nt - t[2])),
+    )
+    plane_peers = [
+        {"x": lax.rem(x + dx, nx), "c": lax.rem(c + dc, nc), "y": lax.rem(y + dy, nt)} for dx, dc, dy in plane_order
+    ]
 
     bar = pltpu.get_barrier_semaphore()
+
+    def signal(sem, dev):
+        pl.semaphore_signal(sem, inc=1, device_id=dev, device_id_type=MESH)
+
+    for d in range(nx - 1, 0, -1):
+        signal(bar, {"x": lax.rem(x + d, nx), "c": 0})
+
+    @pl.when(c == 1)
+    def _():
+        signal(bar, {"c": 0})
+
     for p in z_peers:
-        pl.semaphore_signal(bar, inc=1, device_id=zdev(p), device_id_type=MESH)
-    for p in x_peers:
-        pl.semaphore_signal(bar, inc=1, device_id=xdev(p), device_id_type=MESH)
+        signal(bar, {"z": p, "c": 1})
     for p in y_peers:
-        pl.semaphore_signal(bar, inc=1, device_id=ydev(p), device_id_type=MESH)
+        signal(bar, {"y": p, "c": 1})
 
     def loads(sem, pairs):
         copies = [pltpu.make_async_copy(s, d, lsem.at[sem + i]) for i, (s, d) in enumerate(pairs)]
@@ -113,7 +132,6 @@
             cp.wait()
 
     own_lq = pl.ds(pl.multiple_of(y * lq, lq), lq)
-    own_hv = pl.ds(pl.multiple_of(y * HV, HV), HV)
     own_pf = pl.ds(pl.multiple_of(z * pf, pf), pf)
     half = HEAD_ROT // 2
     l_crit = loads(0, [
@@ -132,10 +150,10 @@
         (lengths, lens),
     ])
     l_back = loads(11, [
-        (w_attn_out.at[:, own_hv], back.at[col, :, pl.ds(0, HV)]),
-        (w_shared_gate, back.at[col, :, pl.ds(HV, HIDDEN)]),
-        (w_shared_up, back.at[col, :, pl.ds(HV + HIDDEN, HIDDEN)]),
-        (w_shared_out, back.at[col, :, pl.ds(HV + 2 * HIDDEN, HIDDEN)]),
+        (w_attn_out, back.at[col, :, pl.ds(0, aow)]),
+        (w_shared_gate, back.at[col, :, pl.ds(aow, HIDDEN)]),
+        (w_shared_up, back.at[col, :, pl.ds(aow + HIDDEN, HIDDEN)]),
+        (w_shared_out, back.at[col, :, pl.ds(aow + 2 * HIDDEN, HIDDEN)]),
     ])
     l_tab = loads(15, [
         (w_key_up, keyup), (cache_rotkey, crot), (trig, trg), (route_ids, ids), (route_scores, scores),
@@ -157,20 +175,25 @@
         part = buf.at[pl.ds(0, n)]
         pltpu.make_async_copy(part, part, rsem.at[k]).wait()
 
-    pending = []
+    pending, late = [], []
 
     def sent(buf, n, k):
         pending.append((buf, n, k))
 
     done(l_crit)
-    pl.semaphore_wait(bar, len(z_peers) + len(x_peers) + len(y_peers))
+
+    @pl.when(c == 0)
+    def _():
+        pl.semaphore_wait(bar, nc * nx - 1)
+        signal(ok.at[0], {"c": 1})
+
+    @pl.when(c == 1)
+    def _():
+        pl.semaphore_wait(ok.at[0], 1)
+
     for p in x_peers:
         send(crit.at[col], crit.at[col], 0, xdev(p))
     sent(crit, ncol - 1, 0)
-    done(l_back)
-    for p in x_peers:
-        send(back.at[col], back.at[col], 1, xdev(p))
-    sent(back, ncol - 1, 1)
 
     done(l_rot)
     done(l_tab)
@@ -211,10 +234,24 @@
     pall[:, pl.ds(QW + lq, 128)] = rot
     for i in range(nz):
         za_s[i] = pall[pl.ds(SEQS * i, SEQS), :]
+
+    @pl.when(c == 1)
+    def _():
+        pl.semaphore_wait(bar, nc * (nz - 1) + nc * (nt - 1))
+        signal(ok.at[1], {"c": 0})
+
+    @pl.when(c == 0)
+    def _():
+        pl.semaphore_wait(ok.at[1], 1)
+
     for p in z_peers:
         send(za_s.at[p], za_r.at[z], 2, zdev(p))
     sent(za_s, nz - 1, 2)
     za_r[pl.ds(z, 1)] = za_s[pl.ds(z, 1)]
+    done(l_back)
+    for p in x_peers:
+        send(back.at[col], back.at[col], 1, xdev(p))
+    sent(back, ncol - 1, 1)
 
     rs = scores[...]
     rw = ROUTED_SCALE * rs / jnp.sum(rs, axis=0, keepdims=True)
@@ -316,32 +353,54 @@
     h0 = jnp.sum(jnp.where(r_h < LOCAL_HEADS, ho, 0.0), axis=0, keepdims=True)
     h1 = jnp.sum(jnp.where(r_h < LOCAL_HEADS, 0.0, ho), axis=0, keepdims=True)
     heads = rounded(jnp.where(iota((SEQS, HV), 0) == 0, h0, h1))
-    zd[pl.ds(z, 1)] = heads.reshape(1, SEQS, HV)
+    hs[...] = heads
+    y_to = lax.div(z, zy)
+    spot = lax.rem(z, zy) * nt + y
+    to = zd.at[spot]
     for p in z_peers:
-        send(zd.at[z], zd.at[z], 4, zdev(p))
-    sent(zd, nz - 1, 4)
-
+        send(hs, to, 4, {"z": p, "y": y_to})
+
+    @pl.when(y_to == y)
+    def _():
+        zd[pl.ds(spot, 1)] = heads.reshape(1, SEQS, HV)
+
+    @pl.when(y_to != y)
+    def _():
+        send(hs, to, 4, {"y": y_to})
+
+    def heads_wait(sems):
+        for remote in (True, False):
+
+            @pl.when((y_to != y) if remote else (y_to == y))
+            def _():
+                part = zd.at[pl.ds(0, nz if remote else nz - 1)]
+                pltpu.make_async_copy(part, part, sems.at[4]).wait()
+
+    late.append(lambda: heads_wait(ssem))
     arrived(back, ncol - 1, 1)
-    arrived(zd, nz - 1, 4)
-    for i in range(nz):
-        h32[pl.ds(SEQS * i, SEQS), :] = zd[i]
-    part = dot(h32[...].astype(BF16), back[:, :, pl.ds(0, HV)].reshape(pf, HV), NT)
-    ye[pl.ds(y, 1)] = part.reshape(1, rows, pf)
-    for p in y_peers:
-        send(ye.at[y], ye.at[y], 5, ydev(p))
-    sent(ye, nt - 1, 5)
-    arrived(ye, nt - 1, 5)
-    attn = ye[0]
-    for i in range(1, nt):
-        attn = attn + ye[i]
-    mid = (ht[...] + rounded(attn)).astype(BF16)
-    midx[pl.ds(col, 1)] = mid.reshape(1, rows, pf)
-    for p in x_peers:
-        send(midx.at[col], midx.at[col], 6, xdev(p))
-    sent(midx, ncol - 1, 6)
-    mid_v = mid.astype(F32)
+    heads_wait(rsem)
+    for j in range(zy):
+        for i in range(nt):
+            h32[pl.ds(SEQS * j, SEQS), pl.ds(HV * i, HV)] = zd[j * nt + i]
+    group = SEQS * zy
+    attn = dot(h32[...].astype(BF16), back[:, :, pl.ds(0, aow)].reshape(pf, aow), NT)
+    mid = rounded(ht[pl.ds(pl.multiple_of(group * y, group), group), :] + rounded(attn))
+    place_of = col * nt + y
+    midx[pl.ds(place_of, 1)] = mid.reshape(1, group, pf)
+    for dev in plane_peers:
+        send(midx.at[place_of], midx.at[place_of], 6, dev)
+    sent(midx, ncol * nt - 1, 6)
+
+    arrived(midx, ncol * nt - 1, 6)
+    mid_all = midx[...].reshape(batch, pf).astype(BF16)
+    zg_s[...] = dot(sel_p[...], mid_all).astype(BF16).reshape(nz, SLOTS, pf)
+    for p in z_peers:
+        send(zg_s.at[p], zg_r.at[z], 8, zdev(p))
+    sent(zg_s, nz - 1, 8)
+    zg_r[pl.ds(z, 1)] = zg_s[pl.ds(z, 1)]
+    mid_v = midx[pl.ds(pl.multiple_of(col * nt, nt), nt)].reshape(rows, pf)
     ffn = (mid_v * fgain[pl.ds(z, 1), :]).astype(BF16)
-    shf[:, pl.ds(0, 2 * HIDDEN)] = dot(ffn, back[:, :, pl.ds(HV, 2 * HIDDEN)].reshape(pf, 2 * HIDDEN))
+    shf[:, pl.ds(0, 2 * HIDDEN)] = dot(ffn, back[:, :, pl.ds(aow, 2 * HIDDEN)].reshape(pf, 2 * HIDDEN))
     shf[:, pl.ds(2 * HIDDEN, 128)] = jnp.broadcast_to(jnp.sum(mid_v * mid_v, axis=1, keepdims=True), (rows, 128))
     for i in range(nz):
         zf_s[i] = shf[pl.ds(SEQS * i, SEQS), :]
@@ -349,19 +408,13 @@
         send(zf_s.at[p], zf_r.at[z], 7, zdev(p))
     sent(zf_s, nz - 1, 7)
     zf_r[pl.ds(z, 1)] = zf_s[pl.ds(z, 1)]
-
-    arrived(midx, ncol - 1, 6)
-    mid_all = midx[...].reshape(batch, pf)
-    zg_s[...] = dot(sel_p[...], mid_all).astype(BF16).reshape(nz, SLOTS, pf)
-    for p in z_peers:
-        send(zg_s.at[p], zg_r.at[z], 8, zdev(p))
-    sent(zg_s, nz - 1, 8)
-    zg_r[pl.ds(z, 1)] = zg_s[pl.ds(z, 1)]
     own_f = ones_where(iota((FEATS, pf), 1) == iota((FEATS, pf), 0) + col * FEATS)
     mid_t = dot(own_f, mid_all, NT).astype(BF16)
-    to_half = ones_where(natural(iota((batch, hl), 0)) == iota((batch, hl), 1) + (y >> 1) * hl)
-    mid_own = dot(mid_t, to_half)
-
+    to_own = ones_where(natural(iota((batch, hl), 0)) == (iota((batch, hl), 1) & (ob - 1)) + y * ob)
+    mid_own = dot(mid_t, to_own)
+    mid_own = jnp.where(iota((FEATS // 2, hl), 1) < ob, mid_own[: FEATS // 2], mid_own[FEATS // 2 :])
+
+    arrived(zg_r, nz - 1, 8)
     arrived(zf_r, nz - 1, 7)
     tot = zf_r[0]
     for i in range(1, nz):
@@ -375,7 +428,6 @@
     sent(zs, nz - 1, 9)
 
     done(l_exp)
-    arrived(zg_r, nz - 1, 8)
     pieces = []
     sq = jnp.zeros((SLOTS, 1), F32)
     for i in range(nz):
@@ -401,36 +453,42 @@
         iota((batch, rows), 0) == (iota((batch, rows), 1) >> 1) * (ncol * SEQS) + col * SEQS + (iota((batch, rows), 1) & 1)
     )
     spread_act = dot(place, s32[...].astype(BF16)).astype(BF16)
-    total = dot(back[:, :, pl.ds(HV + 2 * HIDDEN, HIDDEN)].reshape(pf, HIDDEN), spread_act, NT)
+    total = dot(back[:, :, pl.ds(aow + 2 * HIDDEN, HIDDEN)].reshape(pf, HIDDEN), spread_act, NT)
     arrived(zh_r, nz - 1, 10)
     parts = zh_r[...].reshape(nslot, pf)
     total = total + dot(parts, wt[pl.ds(0, nslot), :], TN) + dot(parts, wt[pl.ds(nslot, nslot), :], TN)
-    xr_s[...] = total.reshape(ncol, FEATS, batch)
-    for p in x_peers:
-        send(xr_s.at[p], xr_r.at[col], 11, xdev(p))
-    sent(xr_s, ncol - 1, 11)
-    xr_r[pl.ds(col, 1)] = xr_s[pl.ds(col, 1)]
-    arrived(xr_r, ncol - 1, 11)
-    tot = xr_r[0]
-    for i in range(1, ncol):
-        tot = tot + xr_r[i]
-    for i in range(nt // 2):
-        yo_s[i] = tot[:, hl * i : hl * (i + 1)].astype(BF16)
-    for p in y_peers:
-        send(yo_s.at[p >> 1], yo_r.at[y], 12, ydev(p))
-    sent(yo_r, nt - 1, 12)
-    yo_r[pl.ds(y, 1)] = yo_s[pl.ds(y >> 1, 1)]
-    arrived(yo_r, nt - 1, 12)
-    tot = yo_r[0].astype(F32)
-    for i in range(1, nt):
-        tot = tot + yo_r[i].astype(F32)
-    res = mid_own + tot
-    res = jnp.where((y & 1) == 1, pltpu.roll(res, ob, 1), res)
-    o_mixed[...] = res[:, :ob].astype(BF16)
-
+    total = total.reshape(ncol, 2, FEATS // 2, batch)
+    low_lane = iota((ncol, FEATS // 2, hl), 2) < ob
+    for k in range(nt // 2):
+        ta = total[:, 0, :, hl * k : hl * (k + 1)]
+        tb = total[:, 1, :, hl * k : hl * (k + 1)]
+        flat = (ncol * FEATS // 2, hl)
+        ra = pltpu.roll(ta.reshape(flat), ob, 1).reshape(ta.shape)
+        rb = pltpu.roll(tb.reshape(flat), ob, 1).reshape(tb.shape)
+        pd_s[:, 2 * k] = jnp.where(low_lane, ta, rb)
+        pd_s[:, 2 * k + 1] = jnp.where(low_lane, ra, tb)
+    for dev in plane_peers:
+        send(pd_s.at[dev["x"] * nc + dev["c"], dev["y"]], pd_r.at[place_of], 11, dev)
+    sent(pd_r, ncol * nt - 1, 11)
+    pd_r[pl.ds(place_of, 1)] = pd_s[pl.ds(col, 1), pl.ds(y, 1)].reshape(1, FEATS // 2, hl)
+    arrived(pd_r, ncol * nt - 1, 11)
+    tot = pd_r[0]
+    for i in range(1, ncol * nt):
+        tot = tot + pd_r[i]
+    o_mixed[...] = mid_own + tot
+
+    late.pop()()
     for buf, n, k in pending:
         part = buf.at[pl.ds(0, n)]
         pltpu.make_async_copy(part, part, ssem.at[k]).wait()
+
+
+def finish(ob, packed, latent, rotkey, o_mixed, o_latent, o_rotkey):
+    v = packed[...]
+    both = jnp.concatenate([v, pltpu.roll(v, ob, 1)], axis=0)
+    o_mixed[...] = both[:, :ob].astype(BF16)
+    o_latent[...] = latent[...]
+    o_rotkey[...] = rotkey[...]
 
 
 def body(nz, nx, nc, nt, *args):
@@ -455,7 +513,7 @@
     vm = pltpu.VMEM
     scratch = [
         vm((ncol, FEATS, QW + lq + batch), BF16),
-        vm((ncol, FEATS, HV + 3 * HIDDEN), BF16),
+        vm((ncol, FEATS, nt * HV + 3 * HIDDEN), BF16),
         vm((128, pf), BF16),
         vm((nz, pf), F32), vm((nz, pf), F32), vm((1, LATENT), F32), vm((1, 128), F32),
         vm((LATENT, LOCAL_HEADS * HEAD_KEY), BF16), vm((LATENT, HV), BF16),
@@ -466,33 +524,33 @@
         vm((2, half, CACHE), F32),
         vm((nz, SEQS, aw), F32), vm((nz, SEQS, aw), F32),
         vm((nt, SEQS, lq), F32),
+        vm((SEQS, HV), F32),
         vm((nz, SEQS, HV), F32),
-        vm((nt, rows, pf), F32),
-        vm((ncol, rows, pf), BF16),
+        vm((ncol * nt, SEQS * nz // nt, pf), F32),
         vm((nz, SEQS, 2 * HIDDEN + 128), F32), vm((nz, SEQS, 2 * HIDDEN + 128), F32),
         vm((nz, SLOTS, pf), BF16), vm((nz, SLOTS, pf), BF16),
         vm((nz, SLOTS, pf), BF16), vm((nz, SLOTS, pf), BF16),
         vm((nz, SEQS, HIDDEN), F32),
-        vm((ncol, FEATS, batch), F32), vm((ncol, FEATS, batch), F32),
-        vm((nt // 2, FEATS, hl), BF16), vm((nt, FEATS, hl), BF16),
+        vm((ncol, nt, FEATS // 2, hl), F32), vm((ncol * nt, FEATS // 2, hl), F32),
         vm((LATENT + 256, QW), BF16),
         vm((SEQS, HEAD_ROT, CACHE), F32),
         vm((nslot, batch), BF16),
         vm((2 * nslot, batch), BF16),
         vm((rows, pf), F32),
-        vm((rows, HV), F32),
+        vm((SEQS * nz // nt, nt * HV), F32),
         vm((rows, HIDDEN), F32),
         vm((rows, aw), F32),
         vm((rows, 2 * HIDDEN + 128), F32),
         pltpu.SemaphoreType.DMA((25,)),
         pltpu.SemaphoreType.DMA((13,)),
         pltpu.SemaphoreType.DMA((13,)),
+        pltpu.SemaphoreType.REGULAR((2,)),
     ]
     anywhere = pl.BlockSpec(memory_space=pltpu.HBM)
-    return pl.pallas_call(
+    packed, latent, rotkey = pl.pallas_call(
         functools.partial(kernel, nz, nx, nc, nt),
         out_shape=(
-            jax.ShapeDtypeStruct((FEATS, batch // nt), BF16),
+            jax.ShapeDtypeStruct((FEATS // 2, hl), F32),
             jax.ShapeDtypeStruct((SEQS, LATENT), BF16),
             jax.ShapeDtypeStruct((SEQS, HEAD_ROT), BF16),
         ),
@@ -502,6 +560,18 @@
         compiler_params=pltpu.CompilerParams(collective_id=0, has_side_effects=True, vmem_limit_bytes=67043328),
         name="layer",
     )(*args, trig, freq)
+    vmem = pl.BlockSpec(memory_space=pltpu.VMEM)
+    return pl.pallas_call(
+        functools.partial(finish, hl // 2),
+        out_shape=(
+            jax.ShapeDtypeStruct((FEATS, hl // 2), BF16),
+            jax.ShapeDtypeStruct((SEQS, LATENT), BF16),
+            jax.ShapeDtypeStruct((SEQS, HEAD_ROT), BF16),
+        ),
+        in_specs=[vmem] * 3,
+        out_specs=(vmem,) * 3,
+        name="finish",
+    )(packed, latent, rotkey)
 
 
 EP = ("z", "x", "c")

time: 77.2 us -> 69.9 us (0.905)
  Pallas kernels: 72.7 us -> 69 us
  local copies, waits for them, and re-layouts: 3.67 us -> 0 us
    pallas_call x1, Pallas kernels: 72.7 us -> 67.7 us  [body(): pl.pallas_call(functools.partial(kernel, nz, nx, nc, nt), out_shape=(jax....]
    unnamed x3 -> x0, local copies, waits for them, and re-layouts: 3.67 us -> none
    pallas_call x0 -> x1, Pallas kernels: none -> 1.34 us  [body(): pl.pallas_call(functools.partial(finish, hl // 2), out_shape=(jax.ShapeDt...]
where the time goes in v3:
time: 69.9 us; the launch traced here: 69.7 us
  Pallas kernels  69 us (99%)
    pallas_call x1, Pallas kernels, body(): pl.pallas_call(functools.partial(kernel, nz, nx, nc, nt), out_shape=(jax....  67.7 us

profile of v3, /device:TPU:1, one launch (start us, length us, event | category | flops | bytes accessed | tf_op | source)
XLA Modules:
  0.0 69.7 jit_solution(9352115941067037616)
XLA Ops:
  0.6 67.7 %layer.1 = (f32[8,128]{1,0:T(8,128)}, bf16[2,512]{1,0:T(2,128)(2,1)}, bf16[2,32]{1,0:T(2,128)(2,1)}) custom-call(bf16[16,256]{1,0:T(8,128)(2,1)} %refs_0_.1, f32[16,128]{1,0:T(8,128)} %bitcast.5, bf16[16,384]{1,0:T(8,128)(2,1)} %refs_2_.1, bf16[16,512]{1,0:T(8,128)(2,1)} %refs_3_.1, bf16[32,2048]{1,0:T(8,128)(2,1)} %refs_4_.1, f32[1,512]{1,0:T(1,128)} %bitcast.9, ...), custom_call_target="tpu_custom_call" | custom-call | tf_op jit(solution)/shard_map/layer/pallas_call | solution.py:550
  68.3 1.3 %finish.1 = (bf16[16,64]{1,0:T(8,128)(2,1)}, bf16[2,512]{1,0:T(2,128)(2,1)}, bf16[2,32]{1,0:T(2,128)(2,1)}) custom-call(f32[8,128]{1,0:T(8,128)} %get-tuple-element.6.packed, bf16[2,512]{1,0:T(2,128)(2,1)} %get-tuple-element.7.latent, bf16[2,32]{1,0:T(2,128)(2,1)} %get-tuple-element.8.rotkey), custom_call_target="tpu_custom_call" | custom-call | tf_op jit(solution)/shard_map/finish/pallas_call | solution.py:564

commit v4 on v3

v4 whole, which is shorter than its diff:
```python
import functools

import jax
import jax.numpy as jnp
import numpy as np
from jax import lax
from jax.experimental import pallas as pl
from jax.experimental.pallas import tpu as pltpu
from jax.sharding import Mesh
from jax.sharding import PartitionSpec as P

MESH = pl.DeviceIdType.MESH
F32 = jnp.float32
BF16 = jnp.bfloat16
HIGHEST = lax.Precision.HIGHEST
NN = (((1,), (0,)), ((), ()))
NT = (((1,), (1,)), ((), ()))
TN = (((0,), (0,)), ((), ()))

LOCAL_HEADS = 4
HEAD_KEY = 64
HEAD_ROT = 32
HEAD_VAL = 64
PER_HEAD = HEAD_KEY + HEAD_ROT
LATENT = 512
CACHE = 1024
HIDDEN = 128
SLOTS = 16
FEATS = 16
SEQS = 2
EPSILON = 1e-06
THETA_BASE = 10000.0
ROUTED_SCALE = 2.5
QW = LOCAL_HEADS * PER_HEAD
HV = LOCAL_HEADS * HEAD_VAL


def dot(a, b, dims=NN, precision=None):
    return lax.dot_general(a, b, dims, precision=precision, preferred_element_type=F32)


def iota(shape, axis):
    return lax.broadcasted_iota(jnp.int32, shape, axis)


def ones_where(mask, dtype=BF16):
    return jnp.where(mask, 1.0, 0.0).astype(dtype)


def rounded(v):
    return v.astype(BF16).astype(F32)


def log2(n):
    return n.bit_length() - 1


def kernel(nz, nx, nc, nt, *refs):
    (
        hidden, attn_gain, w_query, w_latent, w_rotkey, latent_gain, w_key_up, w_value_up, w_attn_out, cache_latent, cache_rotkey,
        lengths, ffn_gain, route_ids, route_scores, w_exp_gate, w_exp_up, w_exp_down, w_shared_gate, w_shared_up, w_shared_out,
        trig, freq,
        o_mixed, o_latent, o_rotkey,
        crit, so, bgs, aoc, sgc, hc, rotw, again, fgain, lgain, fr, keyup, valup, cache, crot, lens, ids, scores, wgu, wd, trg,
        za_s, za_r, yb, ha, mz, sh_s, sh_r, tk_s, tk_r, zh_s, zh_r, zs, pd_s, pd_r,
        ka, krot, sel_p, wt, h16, s32, pall, sp, gp, tot0,
        lsem, ssem, rsem, ok,
    ) = refs
    ncol = nx * nc
    pf = FEATS * ncol
    rows = SEQS * nz
    batch = rows * ncol
    width = pf * nz
    lq = LATENT // nt
    nslot = nz * SLOTS
    ob = batch // nt
    hl = 2 * ob
    hb = batch // 2
    zy = nz // nt
    tok = ncol * SEQS
    cf = FEATS * zy
    npl = ncol * nt
    z, x, c, y = (lax.axis_index(a) for a in ("z", "x", "c", "y"))
    col = x * nc + c
    place_of = col * nt + y
    y_to = lax.div(z, zy)
    spot = lax.rem(z, zy) * nt + y

    def xdev(p):
        return {"x": lax.div(p, nc), "c": lax.rem(p, nc)}

    z_order = sorted(range(1, nz), key=lambda d: -min(d, nz - d))
    z_peers = [lax.rem(z + d, nz) for d in z_order]
    x_order = sorted(range(1, ncol), key=lambda d: -min(d, ncol - d))
    x_peers = [lax.rem(col + d, ncol) for d in x_order]
    y_peers = [lax.rem(y + d, nt) for d in range(1, nt)]
    plane_order = sorted(
        [(dx, dc, dy) for dx in range(nx) for dc in range(nc) for dy in range(nt) if dx or dc or dy],
        key=lambda t: -(min(t[0], nx - t[0]) + min(t[2], nt - t[2])),
    )
    plane_peers = [
        {"x": lax.rem(x + dx, nx), "c": lax.rem(c + dc, nc), "y": lax.rem(y + dy, nt)} for dx, dc, dy in plane_order
    ]

    bar = pltpu.get_barrier_semaphore()

    def signal(sem, dev):
        pl.semaphore_signal(sem, inc=1, device_id=dev, device_id_type=MESH)

    for d in range(nx - 1, 0, -1):
        signal(bar, {"x": lax.rem(x + d, nx), "c": 0})

    @pl.when(c == 1)
    def _():
        signal(bar, {"c": 0})

    def loads(sem, pairs):
        copies = [pltpu.make_async_copy(s, d, lsem.at[sem + i]) for i, (s, d) in enumerate(pairs)]
        for cp in copies:
            cp.start()
        return copies

    def done(copies):
        for cp in copies:
            cp.wait()

    own_lq = pl.ds(pl.multiple_of(y * lq, lq), lq)
    own_hv = pl.ds(pl.multiple_of(y * HV, HV), HV)
    own_pf = pl.ds(pl.multiple_of(z * pf, pf), pf)
    half = HEAD_ROT // 2
    l_crit = loads(0, [
        (w_query, crit.at[col, :, pl.ds(0, QW)]),
        (w_latent.at[:, own_lq], crit.at[col, :, pl.ds(QW, lq)]),
        (hidden, crit.at[col, :, pl.ds(QW + lq, batch)]),
    ])

    for p in z_peers:
        signal(bar, {"z": p, "c": 1})
    for p in y_peers:
        signal(bar, {"y": p, "c": 1})

    def send(src, dst, k, dev):
        cp = pltpu.make_async_remote_copy(
            src_ref=src, dst_ref=dst, send_sem=ssem.at[k], recv_sem=rsem.at[k], device_id=dev, device_id_type=MESH
        )
        cp.start()

    def take(part, sem):
        pltpu.make_async_copy(part, part, sem).wait()

    def arrived(buf, n, k):
        take(buf.at[pl.ds(0, n)], rsem.at[k])

    pending, late = [], []

    def sent(buf, n, k):
        pending.append((buf, n, k))

    done(l_crit)

    @pl.when(c == 0)
    def _():
        pl.semaphore_wait(bar, nc * nx - 1)
        signal(ok.at[0], {"c": 1})

    @pl.when(c == 1)
    def _():
        pl.semaphore_wait(ok.at[0], 1)

    for p in x_peers:
        send(crit.at[col], crit.at[col], 0, xdev(p))
    sent(crit, ncol - 1, 0)
    l_rot = loads(3, [
        (w_rotkey.at[:, own_pf], rotw.at[pl.ds(0, HEAD_ROT)]),
        (w_rotkey.at[pl.ds(half, half), own_pf], rotw.at[pl.ds(64, half)]),
        (w_rotkey.at[pl.ds(0, half), own_pf], rotw.at[pl.ds(64 + half, half)]),
        (attn_gain, again),
        (ffn_gain, fgain),
        (latent_gain, lgain),
        (freq, fr),
        (lengths, lens),
    ])
    l_tab = loads(11, [
        (w_key_up, keyup), (cache_rotkey, crot), (trig, trg), (route_ids, ids), (route_scores, scores),
    ])
    l_att = loads(16, [(cache_latent, cache), (w_value_up, valup)])
    l_bg = loads(18, [
        (w_attn_out.at[:, own_hv], bgs.at[:, pl.ds(0, HV)]),
        (w_shared_gate, bgs.at[:, pl.ds(HV, HIDDEN)]),
        (w_shared_up, bgs.at[:, pl.ds(HV + HIDDEN, HIDDEN)]),
        (w_shared_out, so.at[col]),
    ])
    l_exp = loads(22, [(w_exp_down.at[0], wd)])
    for i in range(ncol):
        pltpu.make_async_copy(w_exp_gate.at[:, i], wgu.at[i, :, :, pl.ds(0, HIDDEN)], lsem.at[23]).start()
        pltpu.make_async_copy(w_exp_up.at[:, i], wgu.at[i, :, :, pl.ds(HIDDEN, HIDDEN)], lsem.at[23]).start()
    l_gu = pltpu.make_async_copy(wgu, wgu, lsem.at[23])

    done(l_rot)
    done(l_tab)
    cos_t, sin_t = trg[0], trg[1]
    for s in range(SEQS):
        low = crot[s, pl.ds(0, half), :].astype(F32)
        high = crot[s, pl.ds(half, half), :].astype(F32)
        krot[s, pl.ds(0, half), :] = low * cos_t - high * sin_t
        krot[s, pl.ds(half, half), :] = low * sin_t + high * cos_t
    spread_r = iota((LOCAL_HEADS * HEAD_KEY, QW), 0)
    spread = ones_where(iota((LOCAL_HEADS * HEAD_KEY, QW), 1) == spread_r + HEAD_ROT * (spread_r >> log2(HEAD_KEY)))
    ka[pl.ds(0, LATENT), :] = dot(keyup[...], spread).astype(BF16)
    lane_q = iota((256, QW), 1)
    head_q = ones_where(lane_q >= PER_HEAD, jnp.int32)
    for h in range(2, LOCAL_HEADS):
        head_q = head_q + ones_where(lane_q >= h * PER_HEAD, jnp.int32)
    within = lane_q - PER_HEAD * head_q - HEAD_KEY
    row_q = iota((256, QW), 0)
    want = jnp.where(row_q < 128, row_q, (row_q - 128) ^ half)
    limit = jnp.where(row_q < 128, row_q, row_q - 128)
    ka[pl.ds(LATENT, 256), :] = ones_where((within == want) & (limit < HEAD_ROT))
    rot_rows = iota((128, pf), 0)
    rot_w = jnp.where((rot_rows & 63) < HEAD_ROT, rotw[...].astype(F32), 0.0).astype(BF16)

    @pl.when(c == 1)
    def _():
        pl.semaphore_wait(bar, nc * (nz - 1) + nc * (nt - 1))
        signal(ok.at[1], {"c": 0})
        for p in y_peers:
            for core in range(nc):
                signal(ok.at[2], {"y": p, "c": core})

    arrived(crit, ncol - 1, 0)
    r_i, b_i = iota((rows, batch), 0), iota((rows, batch), 1)
    sel_a = ones_where(b_i == (r_i >> 1) * tok + col * SEQS + (r_i & 1))
    hid = crit[:, :, pl.ds(QW + lq, batch)].reshape(pf, batch)
    h_t = dot(sel_a, hid, NT)
    scaled = (h_t * again[pl.ds(z, 1), :]).astype(BF16)
    main = dot(scaled, crit[:, :, pl.ds(0, QW + lq)].reshape(pf, QW + lq))
    rot = dot(scaled, rot_w, NT)
    square = jnp.sum(h_t * h_t, axis=1, keepdims=True)
    rot = jnp.where(iota((rows, 128), 1) == HEAD_ROT, square, rot)
    aw = QW + lq + 128
    pall[:, pl.ds(0, QW + lq)] = main
    pall[:, pl.ds(QW + lq, 128)] = rot
    for i in range(nz):
        za_s[i] = pall[pl.ds(SEQS * i, SEQS), :]

    @pl.when(c == 0)
    def _():
        pl.semaphore_wait(ok.at[1], 1)

    for p in z_peers:
        send(za_s.at[p], za_r.at[z], 2, {"z": p})
    sent(za_s, nz - 1, 2)
    za_r[pl.ds(z, 1)] = za_s[pl.ds(z, 1)]
    pl.semaphore_wait(ok.at[2], nt - 1)
    done(l_bg)

    def chunk_send(src, dst, k):
        for p in z_peers:
            send(src, dst.at[spot], k, {"z": p, "y": y_to})

        @pl.when(y_to == y)
        def _():
            dst[pl.ds(spot, 1)] = src[...].reshape(1, FEATS, HV)

        @pl.when(y_to != y)
        def _():
            send(src, dst.at[spot], k, {"y": y_to})

        def wait(sems, _):
            @pl.when(y_to == y)
            def _():
                take(dst.at[pl.ds(0, nz - 1)], sems.at[k])

            @pl.when(y_to != y)
            def _():
                take(dst.at[pl.ds(0, nz)], sems.at[k])

        late.append((k, wait))
        return wait

    wait_ao = chunk_send(bgs.at[:, pl.ds(0, HV)], aoc, 1)
    hzs = nz // 2

    @pl.when(y_to == y)
    def _():
        for p in z_peers:
            lanes = pl.ds(pl.multiple_of(QW + lq + lax.div(p, hzs) * hb, hb), hb)
            send(crit.at[col, :, lanes], hc.at[lax.rem(z, zy)], 3, {"z": p})
        own = pl.ds(pl.multiple_of(QW + lq + lax.div(z, hzs) * hb, hb), hb)
        hc[pl.ds(lax.rem(z, zy), 1)] = crit[pl.ds(col, 1), :, own]

    def wait_hc(sems, receive):
        @pl.when(y_to == y)
        def _():
            if receive:
                if zy > 1:
                    take(hc.at[pl.ds(0, zy - 1)], sems.at[3])
            else:
                take(aoc.at[pl.ds(0, nz - 1), :, pl.ds(0, hb)], sems.at[3])

        if receive:

            @pl.when(y_to != y)
            def _():
                take(hc.at[pl.ds(0, zy)], sems.at[3])

    late.append((3, wait_hc))
    for p in x_peers:
        send(so.at[col], so.at[col], 4, xdev(p))
    sent(so, ncol - 1, 4)

    arrived(za_r, nz - 1, 2)
    tot = za_r[0]
    for i in range(1, nz):
        tot = tot + za_r[i]
    lane2 = iota((SEQS, 128), 1)
    tail = tot[:, QW + lq : aw]
    sq = jnp.sum(jnp.where(lane2 == HEAD_ROT, tail, 0.0), axis=1, keepdims=True)
    scale = lax.rsqrt(sq / width + EPSILON)
    yb[pl.ds(y, 1)] = rounded(tot[:, QW : QW + lq] * scale).reshape(1, SEQS, lq)
    for p in y_peers:
        send(yb.at[y], yb.at[y], 5, {"y": p})
    sent(yb, nt - 1, 5)
    wait_sg = chunk_send(bgs.at[:, pl.ds(HV, HV)], sgc, 6)
    q = rounded(tot[:, :QW] * scale)
    nrows = SEQS * LOCAL_HEADS
    r8 = iota((nrows, 128), 0)
    first8 = r8 < LOCAL_HEADS

    def per_row(v):
        top = iota((nrows, v.shape[1]), 0) < LOCAL_HEADS
        return jnp.where(top, v[0:1, :], v[1:2, :])

    lane_8 = iota((nrows, QW), 1)
    first = (iota((nrows, QW), 0) & (LOCAL_HEADS - 1)) * PER_HEAD
    q8 = jnp.where((lane_8 >= first) & (lane_8 < first + PER_HEAD), per_row(q), 0.0).astype(BF16)
    qa = dot(q8, ka[...], NT)
    absorbed = qa[:, :LATENT].astype(BF16)
    len8 = jnp.where(first8, lens[0], lens[1])
    angle = len8.astype(F32) * fr[...]
    cos8 = jnp.cos(angle)
    lane8 = iota((nrows, 128), 1)
    sin8 = jnp.where((lane8 & half) == 0, -jnp.sin(angle), jnp.sin(angle))
    q_rot = qa[:, LATENT : LATENT + 128] * cos8 + qa[:, LATENT + 128 : LATENT + 256] * sin8

    done(l_att)
    q32 = q_rot[:, :HEAD_ROT]
    per_seq = [dot(absorbed, cache[s], NT) + dot(q32, krot[s], NN, HIGHEST) for s in range(SEQS)]
    top_rows = iota((nrows, CACHE), 0) < LOCAL_HEADS
    score_scale = PER_HEAD**-0.5
    live = iota((nrows, CACHE), 1) < jnp.where(top_rows, lens[0], lens[1])
    cache_score = jnp.where(live, score_scale * jnp.where(top_rows, per_seq[0], per_seq[1]), -1e30)
    best = jnp.max(cache_score, axis=1, keepdims=True)

    new_rot = rounded(tail * scale)
    o_rotkey[...] = new_rot[:, :HEAD_ROT].astype(BF16)
    new_swap = pltpu.roll(new_rot, 64, 1)
    own_rot = jnp.where(lane8 < HEAD_ROT, per_row(new_rot) * cos8 + per_row(new_swap) * sin8, 0.0)

    arrived(yb, nt - 1, 5)
    raw = jnp.concatenate([yb[i] for i in range(nt)], axis=1)
    new_latent = (
        raw * lax.rsqrt(jnp.mean(raw * raw, axis=1, keepdims=True) + EPSILON) * lgain[...]
    ).astype(BF16)
    o_latent[...] = new_latent
    lat8 = per_row(new_latent.astype(F32))
    own_score = score_scale * (
        jnp.sum(absorbed.astype(F32) * lat8, axis=1, keepdims=True)
        + jnp.sum(q_rot * own_rot, axis=1, keepdims=True)
    )
    top_score = jnp.maximum(best, own_score)
    cache_weight = jnp.exp(cache_score - top_score)
    own_weight = jnp.exp(own_score - top_score)
    denominator = jnp.sum(cache_weight, axis=1, keepdims=True) + own_weight
    prob = (cache_weight / denominator).astype(BF16)
    own_prob = rounded(own_weight / denominator)
    ctx = [dot(prob, cache[s]) for s in range(SEQS)]
    top_rows = iota((nrows, LATENT), 0) < LOCAL_HEADS
    context = jnp.where(top_rows, ctx[0], ctx[1]) + own_prob * lat8
    ho = dot(context.astype(BF16), valup[...])
    r_h = iota((nrows, HV), 0)
    ho = jnp.where((iota((nrows, HV), 1) >> log2(HEAD_VAL)) == (r_h & (LOCAL_HEADS - 1)), ho, 0.0)
    h0 = jnp.sum(jnp.where(r_h < LOCAL_HEADS, ho, 0.0), axis=0, keepdims=True)
    h1 = jnp.sum(jnp.where(r_h < LOCAL_HEADS, 0.0, ho), axis=0, keepdims=True)
    heads = rounded(jnp.where(iota((SEQS, HV), 0) == 0, h0, h1))
    ha[pl.ds(place_of, 1)] = heads.reshape(1, SEQS, HV)
    for dev in plane_peers:
        send(ha.at[place_of], ha.at[place_of], 7, dev)
    sent(ha, npl - 1, 7)

    wait_hc(rsem, True)
    t_i, l_i = iota((tok, hb), 0), iota((tok, hb), 1)
    sel_h = ones_where(l_i == lax.rem(z, hzs) * tok + t_i)
    hcv = hc[...].reshape(cf, hb)
    hid_c = dot(sel_h, jnp.concatenate([hcv, hcv], axis=0), NT)
    rs = scores[...]
    rw = ROUTED_SCALE * rs / jnp.sum(rs, axis=0, keepdims=True)
    idv = ids[...]
    nex = nz + ncol
    which = iota((nex, batch), 0)
    target = jnp.where(which < nz, which * ncol + col, z * ncol + which - nz)
    hit = jnp.zeros((nex, batch), F32)
    wgt = jnp.zeros((nex, batch), F32)
    for k in range(4):
        same = idv[k : k + 1, :] == target
        hit = jnp.where(same, 1.0, hit)
        wgt = jnp.where(same, rw[k : k + 1, :], wgt)
    before = ones_where(iota((batch, batch), 0) < iota((batch, batch), 1))
    rank = dot(hit.astype(BF16), before)
    val = jnp.where(hit > 0.0, rank, -1.0).astype(BF16)
    pslot = ncol * SLOTS
    expand_p = ones_where(iota((pslot, nex), 1) == nz + (iota((pslot, nex), 0) >> log2(SLOTS)))
    sel_p[...] = ones_where(dot(expand_p, val) == (iota((pslot, batch), 0) & (SLOTS - 1)).astype(F32))

    gain_rows = jnp.broadcast_to(fgain[...][:, None, :], (nz, ncol, pf)).reshape(nz * ncol, pf)
    gr = iota((nz * ncol, pf), 0)
    gain_rows = jnp.where((iota((nz * ncol, pf), 1) >> log2(FEATS)) == (gr & (ncol - 1)), gain_rows, 0.0)
    tile_f = jnp.where(
        (iota((pf, 2 * cf), 0) & (FEATS - 1)) == (iota((pf, 2 * cf), 1) & (FEATS - 1)), 1.0, 0.0
    )
    tiled = dot(gain_rows, tile_f, NN, HIGHEST).reshape(nz, ncol, 2 * cf)
    lane_z = iota((ncol, 2 * cf), 1) >> log2(FEATS)
    for k in range(nt // 2):
        g = jnp.zeros((ncol, 2 * cf), F32)
        for i in range(2 * zy):
            g = jnp.where(lane_z == i, tiled[2 * zy * k + i], g)
        gp[k] = g

    wait_ao(rsem, True)
    arrived(ha, npl - 1, 7)
    for i in range(ncol):
        for j in range(nt):
            h16[pl.ds(SEQS * i, SEQS), pl.ds(HV * j, HV)] = ha[i * nt + j]
    attn = jnp.zeros((tok, 2 * cf), F32)
    for j in range(nt):
        w = jnp.concatenate([aoc[i * nt + j] for i in range(zy)] * 2, axis=0)
        attn = attn + dot(h16[:, pl.ds(HV * j, HV)].astype(BF16), w, NT)
    mine = (iota((tok, 2 * cf), 1) >> log2(cf)) == (y & 1)
    mid = jnp.where(mine, rounded(hid_c + rounded(attn)), 0.0)
    mz[pl.ds(z, 1)] = mid.astype(BF16).reshape(1, tok, 2 * cf)
    for p in z_peers:
        send(mz.at[z], mz.at[z], 8, {"z": p})
    sent(mz, nz - 1, 8)

    ffn = (mid * gp[pl.ds(y >> 1, 1), pl.ds(col, 1)].reshape(1, 2 * cf)).astype(BF16)
    square = jnp.broadcast_to(jnp.sum(mid * mid, axis=1, keepdims=True), (tok, 128))
    wait_sg(rsem, True)
    for j in range(nt):
        w = jnp.concatenate([sgc[i * nt + j] for i in range(zy)] * 2, axis=0)
        sp[:, pl.ds(0, 2 * HIDDEN)] = dot(ffn, w)
        sp[:, pl.ds(2 * HIDDEN, 128)] = square
        for i in range(ncol):
            sh_s[i * nt + j] = sp[pl.ds(SEQS * i, SEQS), :]
    for dev in plane_peers:
        send(sh_s.at[(dev["x"] * nc + dev["c"]) * nt + dev["y"]], sh_r.at[place_of], 9, dev)
    sent(sh_s, npl - 1, 9)
    sh_r[pl.ds(place_of, 1)] = sh_s[pl.ds(place_of, 1)]

    expand = ones_where(iota((nslot, nex), 1) == (iota((nslot, nex), 0) >> log2(SLOTS)))
    slot_i = (iota((nslot, batch), 0) & (SLOTS - 1)).astype(F32)
    in_slot = dot(expand, val) == slot_i
    w_hi = wgt.astype(BF16)
    w_lo = (wgt - w_hi.astype(F32)).astype(BF16)
    wt[pl.ds(0, nslot), :] = jnp.where(in_slot, dot(expand, w_hi), 0.0).astype(BF16)
    wt[pl.ds(nslot, nslot), :] = jnp.where(in_slot, dot(expand, w_lo), 0.0).astype(BF16)
    arrived(mz, nz - 1, 8)
    mid_all = mz[...].reshape(batch, 2 * cf)
    tk_s[...] = dot(sel_p[...], mid_all).astype(BF16).reshape(ncol, SLOTS, 2 * cf)
    for dev in plane_peers:
        send(tk_s.at[dev["x"] * nc + dev["c"]], tk_r.at[place_of], 10, dev)
    sent(tk_r, npl - 1, 10)
    tk_r[pl.ds(place_of, 1)] = tk_s[pl.ds(col, 1)]
    f_i, l_i = iota((pf, 2 * cf), 0), iota((pf, 2 * cf), 1)
    own_f = (f_i >> log2(FEATS) == col) & (l_i == (z & (2 * zy - 1)) * FEATS + (f_i & (FEATS - 1))) & (y_to == y)
    tot0[...] = dot(ones_where(own_f), mid_all, NT)

    arrived(sh_r, npl - 1, 9)
    tot = sh_r[0]
    for i in range(1, npl):
        tot = tot + sh_r[i]
    scale = lax.rsqrt(tot[:, 2 * HIDDEN : 2 * HIDDEN + 1] / width + EPSILON)
    gate = scale * tot[:, :HIDDEN]
    act = rounded(gate / (1.0 + jnp.exp(-gate)) * (scale * tot[:, HIDDEN : 2 * HIDDEN]))
    zs[pl.ds(z, 1)] = act.reshape(1, SEQS, HIDDEN)
    for p in z_peers:
        send(zs.at[z], zs.at[z], 11, {"z": p})
    sent(zs, nz - 1, 11)

    done(l_exp)
    done([l_gu])
    arrived(tk_r, npl - 1, 10)
    pieces = []
    sq = jnp.zeros((SLOTS, 2 * cf), F32)
    for i in range(ncol):
        for k in range(nt // 2):
            v = tk_r[i * nt + 2 * k].astype(F32) + tk_r[i * nt + 2 * k + 1].astype(F32)
            sq = sq + v * v
            pieces.append((v * gp[k, pl.ds(i, 1), :]).astype(BF16))
    gu = dot(jnp.concatenate(pieces, axis=1), wgu[...].reshape(width, 2 * HIDDEN))
    scale = lax.rsqrt(jnp.sum(sq, axis=1, keepdims=True) / width + EPSILON)
    gate = scale * gu[:, :HIDDEN]
    act = (gate / (1.0 + jnp.exp(-gate)) * (scale * gu[:, HIDDEN:])).astype(BF16)
    out = dot(act, wd[...])
    for i in range(nz):
        zh_s[i] = out[:, pf * i : pf * (i + 1)].astype(BF16)
    for p in z_peers:
        send(zh_s.at[p], zh_r.at[z], 12, {"z": p})
    sent(zh_s, nz - 1, 12)
    zh_r[pl.ds(z, 1)] = zh_s[pl.ds(z, 1)]

    arrived(so, ncol - 1, 4)
    arrived(zs, nz - 1, 11)
    for i in range(nz):
        s32[pl.ds(SEQS * i, SEQS), :] = zs[i]
    b_i, r_i = iota((batch, rows), 0), iota((batch, rows), 1)
    place = ones_where(b_i == (r_i >> 1) * tok + col * SEQS + (r_i & 1))
    spread_act = dot(place, s32[...].astype(BF16)).astype(BF16)
    total = tot0[...] + dot(so[...].reshape(pf, HIDDEN), spread_act, NT)
    arrived(zh_r, nz - 1, 12)
    parts = zh_r[...].reshape(nslot, pf)
    total = total + dot(parts, wt[pl.ds(0, nslot), :], TN) + dot(parts, wt[pl.ds(nslot, nslot), :], TN)
    total = total.reshape(ncol, 2, FEATS // 2, batch)
    low_lane = iota((ncol, FEATS // 2, hl), 2) < ob
    for k in range(nt // 2):
        ta = total[:, 0, :, hl * k : hl * (k + 1)]
        tb = total[:, 1, :, hl * k : hl * (k + 1)]
        flat = (ncol * FEATS // 2, hl)
        ra = pltpu.roll(ta.reshape(flat), ob, 1).reshape(ta.shape)
        rb = pltpu.roll(tb.reshape(flat), ob, 1).reshape(tb.shape)
        pd_s[:, 2 * k] = jnp.where(low_lane, ta, rb)
        pd_s[:, 2 * k + 1] = jnp.where(low_lane, ra, tb)
    for dev in plane_peers:
        send(pd_s.at[dev["x"] * nc + dev["c"], dev["y"]], pd_r.at[place_of], 13, dev)
    sent(pd_r, npl - 1, 13)
    pd_r[pl.ds(place_of, 1)] = pd_s[pl.ds(col, 1), pl.ds(y, 1)].reshape(1, FEATS // 2, hl)
    arrived(pd_r, npl - 1, 13)
    tot = pd_r[0]
    for i in range(1, npl):
        tot = tot + pd_r[i]
    both = jnp.concatenate([tot, pltpu.roll(tot, ob, 1)], axis=0)
    o_mixed[...] = both[:, :ob].astype(BF16)

    for k, f in late:
        f(ssem, False)
    for buf, n, k in pending:
        take(buf.at[pl.ds(0, n)], ssem.at[k])


def finish(*refs):
    copies = [pltpu.make_async_copy(refs[i], refs[3 + i], refs[6].at[i]) for i in range(3)]
    for cp in copies:
        cp.start()
    for cp in copies:
        cp.wait()


def body(nz, nx, nc, nt, *args):
    args = list(args)
    ncol = nx * nc
    pf = FEATS * ncol
    rows = SEQS * nz
    batch = rows * ncol
    lq = LATENT // nt
    nslot = nz * SLOTS
    hl = 2 * (batch // nt)
    aw = QW + lq + 128
    for i in (1, 12):
        args[i] = args[i].reshape(nz, pf)
    args[5] = args[5].reshape(1, LATENT)
    args[13], args[14] = args[13].T, args[14].T
    for i in (15, 16):
        args[i] = args[i].reshape(nz, ncol, FEATS, HIDDEN)
    half = HEAD_ROT // 2
    frequency = THETA_BASE ** (-np.arange(half, dtype=np.float64) / half)
    angles = frequency.astype(np.float32)[:, None] * np.arange(CACHE, dtype=np.float32)[None, :]
    trig = jnp.asarray(np.stack([np.cos(angles.astype(np.float64)), np.sin(angles.astype(np.float64))]).astype(np.float32))
    freq = jnp.asarray(np.tile(frequency.astype(np.float32), 128 // half)[None, :])
    vm = pltpu.VMEM
    tok = ncol * SEQS
    cf = FEATS * nz // nt
    npl = ncol * nt
    scratch = [
        vm((ncol, FEATS, QW + lq + batch), BF16),
        vm((ncol, FEATS, HIDDEN), BF16),
        vm((FEATS, 2 * HV), BF16),
        vm((nz, FEATS, HV), BF16), vm((nz, FEATS, HV), BF16),
        vm((nz // nt, FEATS, batch // 2), BF16),
        vm((128, pf), BF16),
        vm((nz, pf), F32), vm((nz, pf), F32), vm((1, LATENT), F32), vm((1, 128), F32),
        vm((LATENT, LOCAL_HEADS * HEAD_KEY), BF16), vm((LATENT, HV), BF16),
        vm((SEQS, CACHE, LATENT), BF16), vm((SEQS, HEAD_ROT, CACHE), BF16),
        pltpu.SMEM((SEQS,), jnp.int32),
        vm((4, batch), jnp.int32), vm((4, batch), F32),
        vm((ncol, nz, FEATS, 2 * HIDDEN), BF16), vm((HIDDEN, pf * nz), BF16),
        vm((2, half, CACHE), F32),
        vm((nz, SEQS, aw), F32), vm((nz, SEQS, aw), F32),
        vm((nt, SEQS, lq), F32),
        vm((npl, SEQS, HV), F32),
        vm((nz, tok, 2 * cf), BF16),
        vm((npl, SEQS, 2 * HIDDEN + 128), F32), vm((npl, SEQS, 2 * HIDDEN + 128), F32),
        vm((ncol, SLOTS, 2 * cf), BF16), vm((npl, SLOTS, 2 * cf), BF16),
        vm((nz, SLOTS, pf), BF16), vm((nz, SLOTS, pf), BF16),
        vm((nz, SEQS, HIDDEN), F32),
        vm((ncol, nt, FEATS // 2, hl), F32), vm((npl, FEATS // 2, hl), F32),
        vm((LATENT + 256, QW), BF16),
        vm((SEQS, HEAD_ROT, CACHE), F32),
        vm((ncol * SLOTS, batch), BF16),
        vm((2 * nslot, batch), BF16),
        vm((tok, nt * HV), F32),
        vm((rows, HIDDEN), F32),
        vm((rows, aw), F32),
        vm((tok, 2 * HIDDEN + 128), F32),
        vm((nt // 2, ncol, 2 * cf), F32),
        vm((pf, batch), F32),
        pltpu.SemaphoreType.DMA((24,)),
        pltpu.SemaphoreType.DMA((14,)),
        pltpu.SemaphoreType.DMA((14,)),
        pltpu.SemaphoreType.REGULAR((3,)),
    ]
    anywhere = pl.BlockSpec(memory_space=pltpu.HBM)
    results = pl.pallas_call(
        functools.partial(kernel, nz, nx, nc, nt),
        out_shape=(
            pltpu.VMEM((FEATS, hl // 2), BF16),
            pltpu.VMEM((SEQS, LATENT), BF16),
            pltpu.VMEM((SEQS, HEAD_ROT), BF16),
        ),
        in_specs=[anywhere] * 23,
        out_specs=(pl.BlockSpec(memory_space=pltpu.VMEM),) * 3,
        scratch_shapes=scratch,
        compiler_params=pltpu.CompilerParams(collective_id=0, has_side_effects=True, vmem_limit_bytes=66977792),
        name="layer",
    )(*args, trig, freq)
    results = [pltpu.with_memory_space_constraint(r, pltpu.VMEM) for r in results]
    return pl.pallas_call(
        finish,
        out_shape=(
            jax.ShapeDtypeStruct((FEATS, hl // 2), BF16),
            jax.ShapeDtypeStruct((SEQS, LATENT), BF16),
            jax.ShapeDtypeStruct((SEQS, HEAD_ROT), BF16),
        ),
        in_specs=[pl.BlockSpec(memory_space=pltpu.VMEM)] * 3,
        out_specs=(anywhere,) * 3,
        scratch_shapes=[pltpu.SemaphoreType.DMA((3,))],
        name="finish",
    )(*results)


EP = ("z", "x", "c")


def build(devices):
    split = Mesh(devices, ("z", "x", "c", "y"))
    return jax.shard_map(
        functools.partial(body, *devices.shape),
        mesh=split,
        in_specs=(
            P(EP, None),
            P(),
            P(EP, "y"),
            P(EP, None),
            P(),
            P(),
            P(None, "y"),
            P(None, "y"),
            P(EP, None),
            P(EP, None, None),
            P(EP, None, None),
            P(EP),
            P(),
            P(),
            P(),
            P(EP, None, "y"),
            P(EP, None, "y"),
            P(EP, "y", None),
            P(EP, "y"),
            P(EP, "y"),
            P(EP, "y"),
        ),
        out_specs=(P(EP, "y"), P(EP, None), P(EP, None)),
        check_vma=False,
    )


def solution(mesh):
    return build(mesh.devices.reshape(16, 4, 2, mesh.shape["tp"]))
```

time: 69.9 us -> 65.1 us (0.931)
  Pallas kernels: 69 us -> 64.2 us
    pallas_call x2, Pallas kernels: 69 us -> 64.2 us  [the longest x1 63.6 us: body(): pl.pallas_call(functools.partial(kernel, nz, nx, nc, nt), out_shape=(pltp...]
where the time goes in v4:
time: 65.1 us; the launch traced here: 64.8 us
  Pallas kernels  64.2 us (99%)
    pallas_call x1, Pallas kernels, body(): pl.pallas_call(functools.partial(kernel, nz, nx, nc, nt), out_shape=(pltp...  63.6 us

profile of v4, /device:TPU:1, one launch (start us, length us, event | category | flops | bytes accessed | tf_op | source)
XLA Modules:
  0.0 64.8 jit_solution(16925377573661680373)
XLA Ops:
  0.6 63.6 %layer.1 = (bf16[16,64]{1,0:T(8,128)(2,1)S(1)}, bf16[2,512]{1,0:T(2,128)(2,1)S(1)}, bf16[2,32]{1,0:T(2,128)(2,1)S(1)}) custom-call(bf16[16,256]{1,0:T(8,128)(2,1)} %refs_0_.1, f32[16,128]{1,0:T(8,128)} %bitcast.9, bf16[16,384]{1,0:T(8,128)(2,1)} %refs_2_.1, bf16[16,512]{1,0:T(8,128)(2,1)} %refs_3_.1, bf16[32,2048]{1,0:T(8,128)(2,1)} %refs_4_.1, ...), custom_call_target="tpu_custom_call" | custom-call | tf_op jit(solution)/shard_map/layer/pallas_call | solution.py:621
  64.2 0.6 finish.1

commit v5 on v4

--- a/solution.py
+++ b/solution.py
@@ -1,4 +1,5 @@
 import functools
+import math
 
 import jax
 import jax.numpy as jnp
@@ -33,6 +34,7 @@
 ROUTED_SCALE = 2.5
 QW = LOCAL_HEADS * PER_HEAD
 HV = LOCAL_HEADS * HEAD_VAL
+UNIT = 1024
 
 
 def dot(a, b, dims=NN, precision=None):
@@ -61,10 +63,10 @@
         lengths, ffn_gain, route_ids, route_scores, w_exp_gate, w_exp_up, w_exp_down, w_shared_gate, w_shared_up, w_shared_out,
         trig, freq,
         o_mixed, o_latent, o_rotkey,
-        crit, so, bgs, aoc, sgc, hc, rotw, again, fgain, lgain, fr, keyup, valup, cache, crot, lens, ids, scores, wgu, wd, trg,
-        za_s, za_r, yb, ha, mz, sh_s, sh_r, tk_s, tk_r, zh_s, zh_r, zs, pd_s, pd_r,
+        pack, crit, so, bgs, aoc, sgc, hc, rotw, again, fgain, lgain, fr, keyup, valup, cache, crot, lens, ids, scores, wgu, wd, trg,
+        za_s, za_r, zb_r, yb, ha, mz, sh_s, sh_r, tk_s, tk_r, zh_s, zh_r, zs, pd_s, pd_r,
         ka, krot, sel_p, wt, h16, s32, pall, sp, gp, tot0,
-        lsem, ssem, rsem, ok,
+        lsem, ssem, rsem, ok, ruler,
     ) = refs
     ncol = nx * nc
     pf = FEATS * ncol
@@ -75,7 +77,8 @@
     nslot = nz * SLOTS
     ob = batch // nt
     hl = 2 * ob
-    hb = batch // 2
+    wa = 2 * 128
+    wb = QW - wa + lq
     zy = nz // nt
     tok = ncol * SEQS
     cf = FEATS * zy
@@ -83,23 +86,23 @@
     z, x, c, y = (lax.axis_index(a) for a in ("z", "x", "c", "y"))
     col = x * nc + c
     place_of = col * nt + y
-    y_to = lax.div(z, zy)
-    spot = lax.rem(z, zy) * nt + y
+    y_to = ((z) >> log2(zy))
+    ring = ((z) & (zy - 1))
 
     def xdev(p):
-        return {"x": lax.div(p, nc), "c": lax.rem(p, nc)}
+        return {"x": ((p) >> log2(nc)), "c": ((p) & (nc - 1))}
 
     z_order = sorted(range(1, nz), key=lambda d: -min(d, nz - d))
-    z_peers = [lax.rem(z + d, nz) for d in z_order]
+    z_peers = [((z + d) & (nz - 1)) for d in z_order]
     x_order = sorted(range(1, ncol), key=lambda d: -min(d, ncol - d))
-    x_peers = [lax.rem(col + d, ncol) for d in x_order]
-    y_peers = [lax.rem(y + d, nt) for d in range(1, nt)]
+    x_peers = [((col + d) & (ncol - 1)) for d in x_order]
+    y_peers = [((y + d) & (nt - 1)) for d in range(1, nt)]
     plane_order = sorted(
         [(dx, dc, dy) for dx in range(nx) for dc in range(nc) for dy in range(nt) if dx or dc or dy],
         key=lambda t: -(min(t[0], nx - t[0]) + min(t[2], nt - t[2])),
     )
     plane_peers = [
-        {"x": lax.rem(x + dx, nx), "c": lax.rem(c + dc, nc), "y": lax.rem(y + dy, nt)} for dx, dc, dy in plane_order
+        {"x": ((x + dx) & (nx - 1)), "c": ((c + dc) & (nc - 1)), "y": ((y + dy) & (nt - 1))} for dx, dc, dy in plane_order
     ]
 
     bar = pltpu.get_barrier_semaphore()
@@ -108,30 +111,39 @@
         pl.semaphore_signal(sem, inc=1, device_id=dev, device_id_type=MESH)
 
     for d in range(nx - 1, 0, -1):
-        signal(bar, {"x": lax.rem(x + d, nx), "c": 0})
+        signal(bar, {"x": ((x + d) & (nx - 1)), "c": 0})
 
     @pl.when(c == 1)
     def _():
         signal(bar, {"c": 0})
 
+    def nbytes(ref):
+        return math.prod(ref.shape) * jnp.dtype(ref.dtype).itemsize
+
+    def rows_of(n):
+        assert n % UNIT == 0 and n // UNIT <= ruler.shape[0]
+        return ruler.at[pl.ds(0, n // UNIT)]
+
     def loads(sem, pairs):
-        copies = [pltpu.make_async_copy(s, d, lsem.at[sem + i]) for i, (s, d) in enumerate(pairs)]
-        for cp in copies:
-            cp.start()
-        return copies
+        for src, dst in pairs:
+            pltpu.make_async_copy(src, dst, lsem.at[sem]).start()
+        part = rows_of(sum(nbytes(dst) for _, dst in pairs))
+        return [(part, sem)]
 
     def done(copies):
-        for cp in copies:
-            cp.wait()
+        for part, sem in copies:
+            pltpu.make_async_copy(part, part, lsem.at[sem]).wait()
 
     own_lq = pl.ds(pl.multiple_of(y * lq, lq), lq)
     own_hv = pl.ds(pl.multiple_of(y * HV, HV), HV)
     own_pf = pl.ds(pl.multiple_of(z * pf, pf), pf)
     half = HEAD_ROT // 2
     l_crit = loads(0, [
-        (w_query, crit.at[col, :, pl.ds(0, QW)]),
-        (w_latent.at[:, own_lq], crit.at[col, :, pl.ds(QW, lq)]),
-        (hidden, crit.at[col, :, pl.ds(QW + lq, batch)]),
+        (w_query.at[:, pl.ds(0, wa)], pack.at[0, :, pl.ds(0, wa)]),
+        (w_query.at[:, pl.ds(wa, QW - wa)], pack.at[1, :, pl.ds(0, QW - wa)]),
+        (w_latent.at[:, own_lq], pack.at[1, :, pl.ds(QW - wa, lq)]),
+        (hidden, pack.at[0, :, pl.ds(wa, batch)]),
+        (hidden, pack.at[1, :, pl.ds(wb, batch)]),
     ])
 
     for p in z_peers:
@@ -141,7 +153,7 @@
 
     def send(src, dst, k, dev):
         cp = pltpu.make_async_remote_copy(
-            src_ref=src, dst_ref=dst, send_sem=ssem.at[k], recv_sem=rsem.at[k], device_id=dev, device_id_type=MESH
+            src_ref=src, dst_ref=dst, send_sem=ssem.at[0], recv_sem=rsem.at[slot[k]], device_id=dev, device_id_type=MESH
         )
         cp.start()
 
@@ -149,12 +161,16 @@
         pltpu.make_async_copy(part, part, sem).wait()
 
     def arrived(buf, n, k):
-        take(buf.at[pl.ds(0, n)], rsem.at[k])
-
-    pending, late = [], []
-
-    def sent(buf, n, k):
-        pending.append((buf, n, k))
+        take(buf.at[pl.ds(0, n)], rsem.at[slot[k]])
+
+    slot = {0: 0, 1: 1, 3: 1, 6: 1, 2: 2, 14: 2, 5: 3, 7: 4, 15: 5, 17: 5, 16: 6, 4: 6, 8: 7, 9: 8, 10: 9, 11: 10, 12: 11, 13: 12}
+    pending = []
+
+    def sent(buf, n):
+        pending.append(n * nbytes(buf) // buf.shape[0])
+
+    def take_bytes(n, sem):
+        take(rows_of(n), sem)
 
     done(l_crit)
 
@@ -168,36 +184,34 @@
         pl.semaphore_wait(ok.at[0], 1)
 
     for p in x_peers:
-        send(crit.at[col], crit.at[col], 0, xdev(p))
-    sent(crit, ncol - 1, 0)
-    l_rot = loads(3, [
+        send(pack.at[((p) & (nc - 1))], crit.at[col], 0, xdev(p))
+    sent(crit, ncol - 1)
+    crit[pl.ds(col, 1)] = pack[pl.ds(c, 1)]
+    l_rot = loads(1, [
         (w_rotkey.at[:, own_pf], rotw.at[pl.ds(0, HEAD_ROT)]),
         (w_rotkey.at[pl.ds(half, half), own_pf], rotw.at[pl.ds(64, half)]),
         (w_rotkey.at[pl.ds(0, half), own_pf], rotw.at[pl.ds(64 + half, half)]),
         (attn_gain, again),
         (ffn_gain, fgain),
         (latent_gain, lgain),
-        (freq, fr),
-        (lengths, lens),
+        (w_key_up, keyup), (cache_rotkey, crot), (trig, trg), (route_ids, ids), (route_scores, scores), (freq, fr),
     ])
-    l_tab = loads(11, [
-        (w_key_up, keyup), (cache_rotkey, crot), (trig, trg), (route_ids, ids), (route_scores, scores),
-    ])
-    l_att = loads(16, [(cache_latent, cache), (w_value_up, valup)])
-    l_bg = loads(18, [
+    l_len = pltpu.make_async_copy(lengths, lens, lsem.at[2])
+    l_len.start()
+    l_att = loads(3, [(cache_latent, cache), (w_value_up, valup)])
+    l_bg = loads(4, [
         (w_attn_out.at[:, own_hv], bgs.at[:, pl.ds(0, HV)]),
         (w_shared_gate, bgs.at[:, pl.ds(HV, HIDDEN)]),
         (w_shared_up, bgs.at[:, pl.ds(HV + HIDDEN, HIDDEN)]),
         (w_shared_out, so.at[col]),
     ])
-    l_exp = loads(22, [(w_exp_down.at[0], wd)])
-    for i in range(ncol):
-        pltpu.make_async_copy(w_exp_gate.at[:, i], wgu.at[i, :, :, pl.ds(0, HIDDEN)], lsem.at[23]).start()
-        pltpu.make_async_copy(w_exp_up.at[:, i], wgu.at[i, :, :, pl.ds(HIDDEN, HIDDEN)], lsem.at[23]).start()
-    l_gu = pltpu.make_async_copy(wgu, wgu, lsem.at[23])
+    l_exp = loads(5, [(w_exp_down.at[0], wd)] + [
+        (w.at[:, i], wgu.at[i, :, :, pl.ds(HIDDEN * j, HIDDEN)])
+        for i in range(ncol) for j, w in enumerate((w_exp_gate, w_exp_up))
+    ])
 
     done(l_rot)
-    done(l_tab)
+    l_len.wait()
     cos_t, sin_t = trg[0], trg[1]
     for s in range(SEQS):
         low = crot[s, pl.ds(0, half), :].astype(F32)
@@ -228,101 +242,85 @@
                 signal(ok.at[2], {"y": p, "c": core})
 
     arrived(crit, ncol - 1, 0)
-    r_i, b_i = iota((rows, batch), 0), iota((rows, batch), 1)
-    sel_a = ones_where(b_i == (r_i >> 1) * tok + col * SEQS + (r_i & 1))
-    hid = crit[:, :, pl.ds(QW + lq, batch)].reshape(pf, batch)
+    r_i, b_i = iota((nc * rows, batch), 0), iota((nc * rows, batch), 1)
+    owner = x * nc + (r_i >> log2(rows))
+    sel_a = ones_where(b_i == ((r_i & (rows - 1)) >> 1) * tok + owner * SEQS + (r_i & 1))
+    hid = crit[:, :, pl.ds(wa, batch)].reshape(pf, batch)
     h_t = dot(sel_a, hid, NT)
     scaled = (h_t * again[pl.ds(z, 1), :]).astype(BF16)
-    main = dot(scaled, crit[:, :, pl.ds(0, QW + lq)].reshape(pf, QW + lq))
+    pall[:, pl.ds(0, wa)] = dot(scaled, crit[:, :, pl.ds(0, wa)].reshape(pf, wa))
     rot = dot(scaled, rot_w, NT)
     square = jnp.sum(h_t * h_t, axis=1, keepdims=True)
-    rot = jnp.where(iota((rows, 128), 1) == HEAD_ROT, square, rot)
-    aw = QW + lq + 128
-    pall[:, pl.ds(0, QW + lq)] = main
-    pall[:, pl.ds(QW + lq, 128)] = rot
-    for i in range(nz):
+    pall[:, pl.ds(wa, 128)] = jnp.where(iota((nc * rows, 128), 1) == HEAD_ROT, square, rot)
+    for i in range(nc * nz):
         za_s[i] = pall[pl.ds(SEQS * i, SEQS), :]
 
     @pl.when(c == 0)
     def _():
         pl.semaphore_wait(ok.at[1], 1)
 
-    for p in z_peers:
-        send(za_s.at[p], za_r.at[z], 2, {"z": p})
-    sent(za_s, nz - 1, 2)
-    za_r[pl.ds(z, 1)] = za_s[pl.ds(z, 1)]
+    zc_peers = [(p, d) for p in z_peers for d in range(nc)] + [(z, 1)]
+    for core in range(nc):
+
+        @pl.when(c == core)
+        def _():
+            lanes = pl.ds(0, wa if core else wa + 128)
+            dst = (za_r, zb_r)[core]
+            for p, d in zc_peers:
+                e = (core + d) % nc
+                send(za_s.at[e * nz + p, :, lanes], dst.at[z], 2 + 12 * core, {"z": p, "c": e})
+            dst[pl.ds(z, 1)] = za_s[pl.ds(core * nz + z, 1), :, lanes]
+
+    size_a, size_b = nbytes(za_r) // nz, nbytes(zb_r) // nz
+
     pl.semaphore_wait(ok.at[2], nt - 1)
     done(l_bg)
 
-    def chunk_send(src, dst, k):
-        for p in z_peers:
-            send(src, dst.at[spot], k, {"z": p, "y": y_to})
-
-        @pl.when(y_to == y)
-        def _():
-            dst[pl.ds(spot, 1)] = src[...].reshape(1, FEATS, HV)
-
-        @pl.when(y_to != y)
-        def _():
-            send(src, dst.at[spot], k, {"y": y_to})
-
-        def wait(sems, _):
-            @pl.when(y_to == y)
-            def _():
-                take(dst.at[pl.ds(0, nz - 1)], sems.at[k])
-
-            @pl.when(y_to != y)
-            def _():
-                take(dst.at[pl.ds(0, nz)], sems.at[k])
-
-        late.append((k, wait))
-        return wait
-
-    wait_ao = chunk_send(bgs.at[:, pl.ds(0, HV)], aoc, 1)
-    hzs = nz // 2
+    groups = sorted(range(nt), key=lambda k: -min(k, nt - k))
+    for src, dst, k in ((bgs.at[:, pl.ds(0, HV)], aoc, 1), (bgs.at[:, pl.ds(HV, HV)], sgc, 6)):
+        for g in groups:
+            dev = {"z": ((z + zy * g) & (nz - 1)), "y": y_to}
+            if g:
+                send(src, dst.at[ring, y], k, dev)
+            else:
+
+                @pl.when(y_to != y)
+                def _():
+                    send(src, dst.at[ring, y], k, dev)
+
+                @pl.when(y_to == y)
+                def _():
+                    dst[pl.ds(ring, 1), pl.ds(y, 1)] = src[...].reshape(1, 1, FEATS, HV)
 
     @pl.when(y_to == y)
     def _():
-        for p in z_peers:
-            lanes = pl.ds(pl.multiple_of(QW + lq + lax.div(p, hzs) * hb, hb), hb)
-            send(crit.at[col, :, lanes], hc.at[lax.rem(z, zy)], 3, {"z": p})
-        own = pl.ds(pl.multiple_of(QW + lq + lax.div(z, hzs) * hb, hb), hb)
-        hc[pl.ds(lax.rem(z, zy), 1)] = crit[pl.ds(col, 1), :, own]
-
-    def wait_hc(sems, receive):
-        @pl.when(y_to == y)
-        def _():
-            if receive:
-                if zy > 1:
-                    take(hc.at[pl.ds(0, zy - 1)], sems.at[3])
-            else:
-                take(aoc.at[pl.ds(0, nz - 1), :, pl.ds(0, hb)], sems.at[3])
-
-        if receive:
-
-            @pl.when(y_to != y)
-            def _():
-                take(hc.at[pl.ds(0, zy)], sems.at[3])
-
-    late.append((3, wait_hc))
+        for g in groups[:-1]:
+            send(pack.at[0, :, pl.ds(wa, batch)], hc.at[ring], 3, {"z": ((z + zy * g) & (nz - 1))})
+        hc[pl.ds(ring, 1)] = pack[pl.ds(0, 1), :, pl.ds(wa, batch)]
+
     for p in x_peers:
         send(so.at[col], so.at[col], 4, xdev(p))
-    sent(so, ncol - 1, 4)
-
-    arrived(za_r, nz - 1, 2)
-    tot = za_r[0]
+    sent(so, ncol - 1)
+
+    for core in range(nc):
+
+        @pl.when(c == core)
+        def _():
+            take_bytes((nz - 1 + core) * size_a + (nz - core) * size_b, rsem.at[2])
+
+    tot, tot_b = za_r[0], zb_r[0]
     for i in range(1, nz):
         tot = tot + za_r[i]
+        tot_b = tot_b + zb_r[i]
     lane2 = iota((SEQS, 128), 1)
-    tail = tot[:, QW + lq : aw]
+    tail = tot[:, wa:]
     sq = jnp.sum(jnp.where(lane2 == HEAD_ROT, tail, 0.0), axis=1, keepdims=True)
     scale = lax.rsqrt(sq / width + EPSILON)
-    yb[pl.ds(y, 1)] = rounded(tot[:, QW : QW + lq] * scale).reshape(1, SEQS, lq)
+    yb[pl.ds(y, 1)] = rounded(tot_b[:, QW - wa :] * scale).reshape(1, SEQS, lq)
     for p in y_peers:
         send(yb.at[y], yb.at[y], 5, {"y": p})
-    sent(yb, nt - 1, 5)
-    wait_sg = chunk_send(bgs.at[:, pl.ds(HV, HV)], sgc, 6)
-    q = rounded(tot[:, :QW] * scale)
+    sent(yb, nt - 1)
+    q = rounded(jnp.concatenate([tot[:, :wa], tot_b[:, : QW - wa]], axis=1) * scale)
     nrows = SEQS * LOCAL_HEADS
     r8 = iota((nrows, 128), 0)
     first8 = r8 < LOCAL_HEADS
@@ -337,7 +335,7 @@
     qa = dot(q8, ka[...], NT)
     absorbed = qa[:, :LATENT].astype(BF16)
     len8 = jnp.where(first8, lens[0], lens[1])
-    angle = len8.astype(F32) * fr[...]
+    angle = len8.astype(F32) * fr[pl.ds(0, 1), :]
     cos8 = jnp.cos(angle)
     lane8 = iota((nrows, 128), 1)
     sin8 = jnp.where((lane8 & half) == 0, -jnp.sin(angle), jnp.sin(angle))
@@ -351,6 +349,11 @@
     live = iota((nrows, CACHE), 1) < jnp.where(top_rows, lens[0], lens[1])
     cache_score = jnp.where(live, score_scale * jnp.where(top_rows, per_seq[0], per_seq[1]), -1e30)
     best = jnp.max(cache_score, axis=1, keepdims=True)
+    cache_weight = jnp.exp(cache_score - best)
+    cache_total = jnp.sum(cache_weight, axis=1, keepdims=True)
+    cache_weight = cache_weight.astype(BF16)
+    ctx = [dot(cache_weight, cache[s]) for s in range(SEQS)]
+    ctx = jnp.where(iota((nrows, LATENT), 0) < LOCAL_HEADS, ctx[0], ctx[1])
 
     new_rot = rounded(tail * scale)
     o_rotkey[...] = new_rot[:, :HEAD_ROT].astype(BF16)
@@ -369,14 +372,10 @@
         + jnp.sum(q_rot * own_rot, axis=1, keepdims=True)
     )
     top_score = jnp.maximum(best, own_score)
-    cache_weight = jnp.exp(cache_score - top_score)
+    rescale = jnp.exp(best - top_score)
     own_weight = jnp.exp(own_score - top_score)
-    denominator = jnp.sum(cache_weight, axis=1, keepdims=True) + own_weight
-    prob = (cache_weight / denominator).astype(BF16)
-    own_prob = rounded(own_weight / denominator)
-    ctx = [dot(prob, cache[s]) for s in range(SEQS)]
-    top_rows = iota((nrows, LATENT), 0) < LOCAL_HEADS
-    context = jnp.where(top_rows, ctx[0], ctx[1]) + own_prob * lat8
+    denominator = rescale * cache_total + own_weight
+    context = (rescale / denominator) * ctx + rounded(own_weight / denominator) * lat8
     ho = dot(context.astype(BF16), valup[...])
     r_h = iota((nrows, HV), 0)
     ho = jnp.where((iota((nrows, HV), 1) >> log2(HEAD_VAL)) == (r_h & (LOCAL_HEADS - 1)), ho, 0.0)
@@ -386,13 +385,25 @@
     ha[pl.ds(place_of, 1)] = heads.reshape(1, SEQS, HV)
     for dev in plane_peers:
         send(ha.at[place_of], ha.at[place_of], 7, dev)
-    sent(ha, npl - 1, 7)
-
-    wait_hc(rsem, True)
-    t_i, l_i = iota((tok, hb), 0), iota((tok, hb), 1)
-    sel_h = ones_where(l_i == lax.rem(z, hzs) * tok + t_i)
-    hcv = hc[...].reshape(cf, hb)
-    hid_c = dot(sel_h, jnp.concatenate([hcv, hcv], axis=0), NT)
+    sent(ha, npl - 1)
+
+    size_bg, size_h = nbytes(bgs), nbytes(hc) // zy
+    for here in (True, False):
+
+        @pl.when((y_to == y) if here else (y_to != y))
+        def _():
+            take_bytes((nt - 1) * size_bg if here else nt * size_bg + size_h, rsem.at[1])
+
+    beside = [r if 2 * r <= zy else r - zy for r in range(1, zy)]
+    for r in sorted(beside, key=lambda r: -abs(r)):
+        dev = {"z": ((z + r + nz) & (nz - 1))}
+        send(hc.at[ring], hc.at[ring], 17, dev)
+        send(aoc.at[ring], aoc.at[ring], 15, dev)
+    for r in sorted(beside, key=lambda r: -abs(r)):
+        send(sgc.at[ring], sgc.at[ring], 16, {"z": ((z + r + nz) & (nz - 1))})
+    for buf in (hc, aoc, sgc):
+        sent(buf, zy - 1)
+
     rs = scores[...]
     rw = ROUTED_SCALE * rs / jnp.sum(rs, axis=0, keepdims=True)
     idv = ids[...]
@@ -426,34 +437,39 @@
             g = jnp.where(lane_z == i, tiled[2 * zy * k + i], g)
         gp[k] = g
 
-    wait_ao(rsem, True)
+    if beside:
+        take_bytes((zy - 1) * (nbytes(hc) + nbytes(aoc)) // zy, rsem.at[slot[15]])
+    t_i, l_i = iota((tok, batch), 0), iota((tok, batch), 1)
+    sel_h = ones_where(l_i == z * tok + t_i)
+    hcv = hc[...].reshape(cf, batch)
+    hid_c = dot(sel_h, jnp.concatenate([hcv, hcv], axis=0), NT)
     arrived(ha, npl - 1, 7)
     for i in range(ncol):
         for j in range(nt):
             h16[pl.ds(SEQS * i, SEQS), pl.ds(HV * j, HV)] = ha[i * nt + j]
     attn = jnp.zeros((tok, 2 * cf), F32)
     for j in range(nt):
-        w = jnp.concatenate([aoc[i * nt + j] for i in range(zy)] * 2, axis=0)
+        w = jnp.concatenate([aoc[i, j] for i in range(zy)] * 2, axis=0)
         attn = attn + dot(h16[:, pl.ds(HV * j, HV)].astype(BF16), w, NT)
     mine = (iota((tok, 2 * cf), 1) >> log2(cf)) == (y & 1)
     mid = jnp.where(mine, rounded(hid_c + rounded(attn)), 0.0)
     mz[pl.ds(z, 1)] = mid.astype(BF16).reshape(1, tok, 2 * cf)
     for p in z_peers:
         send(mz.at[z], mz.at[z], 8, {"z": p})
-    sent(mz, nz - 1, 8)
+    sent(mz, nz - 1)
 
     ffn = (mid * gp[pl.ds(y >> 1, 1), pl.ds(col, 1)].reshape(1, 2 * cf)).astype(BF16)
     square = jnp.broadcast_to(jnp.sum(mid * mid, axis=1, keepdims=True), (tok, 128))
-    wait_sg(rsem, True)
+    take_bytes((zy - 1) * nbytes(sgc) // zy + (ncol - 1) * nbytes(so) // ncol, rsem.at[slot[16]])
     for j in range(nt):
-        w = jnp.concatenate([sgc[i * nt + j] for i in range(zy)] * 2, axis=0)
+        w = jnp.concatenate([sgc[i, j] for i in range(zy)] * 2, axis=0)
         sp[:, pl.ds(0, 2 * HIDDEN)] = dot(ffn, w)
         sp[:, pl.ds(2 * HIDDEN, 128)] = square
         for i in range(ncol):
             sh_s[i * nt + j] = sp[pl.ds(SEQS * i, SEQS), :]
     for dev in plane_peers:
         send(sh_s.at[(dev["x"] * nc + dev["c"]) * nt + dev["y"]], sh_r.at[place_of], 9, dev)
-    sent(sh_s, npl - 1, 9)
+    sent(sh_s, npl - 1)
     sh_r[pl.ds(place_of, 1)] = sh_s[pl.ds(place_of, 1)]
 
     expand = ones_where(iota((nslot, nex), 1) == (iota((nslot, nex), 0) >> log2(SLOTS)))
@@ -468,7 +484,7 @@
     tk_s[...] = dot(sel_p[...], mid_all).astype(BF16).reshape(ncol, SLOTS, 2 * cf)
     for dev in plane_peers:
         send(tk_s.at[dev["x"] * nc + dev["c"]], tk_r.at[place_of], 10, dev)
-    sent(tk_r, npl - 1, 10)
+    sent(tk_r, npl - 1)
     tk_r[pl.ds(place_of, 1)] = tk_s[pl.ds(col, 1)]
     f_i, l_i = iota((pf, 2 * cf), 0), iota((pf, 2 * cf), 1)
     own_f = (f_i >> log2(FEATS) == col) & (l_i == (z & (2 * zy - 1)) * FEATS + (f_i & (FEATS - 1))) & (y_to == y)
@@ -484,10 +500,9 @@
     zs[pl.ds(z, 1)] = act.reshape(1, SEQS, HIDDEN)
     for p in z_peers:
         send(zs.at[z], zs.at[z], 11, {"z": p})
-    sent(zs, nz - 1, 11)
+    sent(zs, nz - 1)
 
     done(l_exp)
-    done([l_gu])
     arrived(tk_r, npl - 1, 10)
     pieces = []
     sq = jnp.zeros((SLOTS, 2 * cf), F32)
@@ -505,10 +520,9 @@
         zh_s[i] = out[:, pf * i : pf * (i + 1)].astype(BF16)
     for p in z_peers:
         send(zh_s.at[p], zh_r.at[z], 12, {"z": p})
-    sent(zh_s, nz - 1, 12)
+    sent(zh_s, nz - 1)
     zh_r[pl.ds(z, 1)] = zh_s[pl.ds(z, 1)]
 
-    arrived(so, ncol - 1, 4)
     arrived(zs, nz - 1, 11)
     for i in range(nz):
         s32[pl.ds(SEQS * i, SEQS), :] = zs[i]
@@ -531,7 +545,7 @@
         pd_s[:, 2 * k + 1] = jnp.where(low_lane, ra, tb)
     for dev in plane_peers:
         send(pd_s.at[dev["x"] * nc + dev["c"], dev["y"]], pd_r.at[place_of], 13, dev)
-    sent(pd_r, npl - 1, 13)
+    sent(pd_r, npl - 1)
     pd_r[pl.ds(place_of, 1)] = pd_s[pl.ds(col, 1), pl.ds(y, 1)].reshape(1, FEATS // 2, hl)
     arrived(pd_r, npl - 1, 13)
     tot = pd_r[0]
@@ -540,10 +554,14 @@
     both = jnp.concatenate([tot, pltpu.roll(tot, ob, 1)], axis=0)
     o_mixed[...] = both[:, :ob].astype(BF16)
 
-    for k, f in late:
-        f(ssem, False)
-    for buf, n, k in pending:
-        take(buf.at[pl.ds(0, n)], ssem.at[k])
+    for core in range(nc):
+        for here in (True, False):
+
+            @pl.when((c == core) & ((y_to == y) if here else (y_to != y)))
+            def _():
+                mine = (nc * nz - 1) * (size_b if core else size_a)
+                mine += (nt - 1) * (size_bg + size_h) if here else nt * size_bg
+                take_bytes(sum(pending) + mine, ssem.at[0])
 
 
 def finish(*refs):
@@ -563,7 +581,7 @@
     lq = LATENT // nt
     nslot = nz * SLOTS
     hl = 2 * (batch // nt)
-    aw = QW + lq + 128
+    wa = 2 * 128
     for i in (1, 12):
         args[i] = args[i].reshape(nz, pf)
     args[5] = args[5].reshape(1, LATENT)
@@ -574,26 +592,26 @@
     frequency = THETA_BASE ** (-np.arange(half, dtype=np.float64) / half)
     angles = frequency.astype(np.float32)[:, None] * np.arange(CACHE, dtype=np.float32)[None, :]
     trig = jnp.asarray(np.stack([np.cos(angles.astype(np.float64)), np.sin(angles.astype(np.float64))]).astype(np.float32))
-    freq = jnp.asarray(np.tile(frequency.astype(np.float32), 128 // half)[None, :])
+    freq = jnp.asarray(np.tile(frequency.astype(np.float32), (2, 128 // half)))
     vm = pltpu.VMEM
     tok = ncol * SEQS
     cf = FEATS * nz // nt
     npl = ncol * nt
     scratch = [
-        vm((ncol, FEATS, QW + lq + batch), BF16),
+        vm((nc, FEATS, wa + batch), BF16), vm((ncol, FEATS, wa + batch), BF16),
         vm((ncol, FEATS, HIDDEN), BF16),
         vm((FEATS, 2 * HV), BF16),
-        vm((nz, FEATS, HV), BF16), vm((nz, FEATS, HV), BF16),
-        vm((nz // nt, FEATS, batch // 2), BF16),
+        vm((nz // nt, nt, FEATS, HV), BF16), vm((nz // nt, nt, FEATS, HV), BF16),
+        vm((nz // nt, FEATS, batch), BF16),
         vm((128, pf), BF16),
-        vm((nz, pf), F32), vm((nz, pf), F32), vm((1, LATENT), F32), vm((1, 128), F32),
+        vm((nz, pf), F32), vm((nz, pf), F32), vm((1, LATENT), F32), vm((2, 128), F32),
         vm((LATENT, LOCAL_HEADS * HEAD_KEY), BF16), vm((LATENT, HV), BF16),
         vm((SEQS, CACHE, LATENT), BF16), vm((SEQS, HEAD_ROT, CACHE), BF16),
         pltpu.SMEM((SEQS,), jnp.int32),
         vm((4, batch), jnp.int32), vm((4, batch), F32),
         vm((ncol, nz, FEATS, 2 * HIDDEN), BF16), vm((HIDDEN, pf * nz), BF16),
         vm((2, half, CACHE), F32),
-        vm((nz, SEQS, aw), F32), vm((nz, SEQS, aw), F32),
+        vm((nc * nz, SEQS, wa + 128), F32), vm((nz, SEQS, wa + 128), F32), vm((nz, SEQS, wa), F32),
         vm((nt, SEQS, lq), F32),
         vm((npl, SEQS, HV), F32),
         vm((nz, tok, 2 * cf), BF16),
@@ -608,14 +626,15 @@
         vm((2 * nslot, batch), BF16),
         vm((tok, nt * HV), F32),
         vm((rows, HIDDEN), F32),
-        vm((rows, aw), F32),
+        vm((nc * rows, wa + 128), F32),
         vm((tok, 2 * HIDDEN + 128), F32),
         vm((nt // 2, ncol, 2 * cf), F32),
         vm((pf, batch), F32),
-        pltpu.SemaphoreType.DMA((24,)),
-        pltpu.SemaphoreType.DMA((14,)),
-        pltpu.SemaphoreType.DMA((14,)),
+        pltpu.SemaphoreType.DMA((6,)),
+        pltpu.SemaphoreType.DMA((1,)),
+        pltpu.SemaphoreType.DMA((13,)),
         pltpu.SemaphoreType.REGULAR((3,)),
+        vm((2560 * 1024 // UNIT, 2, UNIT // 8), F32),
     ]
     anywhere = pl.BlockSpec(memory_space=pltpu.HBM)
     results = pl.pallas_call(

time: 65.1 us -> 63.8 us (0.980)
  Pallas kernels: 64.2 us -> 63 us
    pallas_call x1, Pallas kernels: 63.6 us -> 62.4 us  [body(): pl.pallas_call(functools.partial(kernel, nz, nx, nc, nt), out_shape=(pltp...]
where the time goes in v5:
time: 63.8 us; the launch traced here: 63.6 us
  Pallas kernels  63 us (99%)
  between operations  0.65 us (1%)
    pallas_call x1, Pallas kernels, body(): pl.pallas_call(functools.partial(kernel, nz, nx, nc, nt), out_shape=(pltp...  62.4 us

profile of v5, /device:TPU:1, one launch (start us, length us, event | category | flops | bytes accessed | tf_op | source)
XLA Modules:
  0.0 63.6 jit_solution(17536204816864712084)
XLA Ops:
  0.6 62.4 %layer.1 = (bf16[16,64]{1,0:T(8,128)(2,1)S(1)}, bf16[2,512]{1,0:T(2,128)(2,1)S(1)}, bf16[2,32]{1,0:T(2,128)(2,1)S(1)}) custom-call(bf16[16,256]{1,0:T(8,128)(2,1)} %refs_0_.1, f32[16,128]{1,0:T(8,128)} %bitcast.9, bf16[16,384]{1,0:T(8,128)(2,1)} %refs_2_.1, bf16[16,512]{1,0:T(8,128)(2,1)} %refs_3_.1, bf16[32,2048]{1,0:T(8,128)(2,1)} %refs_4_.1, ...), custom_call_target="tpu_custom_call" | custom-call | tf_op jit(solution)/shard_map/layer/pallas_call | solution.py:640
  63.0 0.6 finish.1

commit v6 on v5

--- a/solution.py
+++ b/solution.py
@@ -63,7 +63,7 @@
         lengths, ffn_gain, route_ids, route_scores, w_exp_gate, w_exp_up, w_exp_down, w_shared_gate, w_shared_up, w_shared_out,
         trig, freq,
         o_mixed, o_latent, o_rotkey,
-        pack, crit, so, bgs, aoc, sgc, hc, rotw, again, fgain, lgain, fr, keyup, valup, cache, crot, lens, ids, scores, wgu, wd, trg,
+        pack, crit, hidn, hp_s, hp, so, bgs, aoc, sgc, hc, rotw, again, fgain, lgain, fr, keyup, valup, cache, crot, lens, ids, scores, wgu, wd, trg,
         za_s, za_r, zb_r, yb, ha, mz, sh_s, sh_r, tk_s, tk_r, zh_s, zh_r, zs, pd_s, pd_r,
         ka, krot, sel_p, wt, h16, s32, pall, sp, gp, tot0,
         lsem, ssem, rsem, ok, ruler,
@@ -78,11 +78,12 @@
     ob = batch // nt
     hl = 2 * ob
     wa = 2 * 128
-    wb = QW - wa + lq
+    hw = max(128, nc * rows)
     zy = nz // nt
     tok = ncol * SEQS
     cf = FEATS * zy
     npl = ncol * nt
+    th, sh = tok // 2, SLOTS // 2
     z, x, c, y = (lax.axis_index(a) for a in ("z", "x", "c", "y"))
     col = x * nc + c
     place_of = col * nt + y
@@ -117,6 +118,10 @@
     def _():
         signal(bar, {"c": 0})
 
+    sig_first = nz // 4
+    for p in z_peers[:sig_first]:
+        signal(bar, {"z": p, "c": 1})
+
     def nbytes(ref):
         return math.prod(ref.shape) * jnp.dtype(ref.dtype).itemsize
 
@@ -142,11 +147,10 @@
         (w_query.at[:, pl.ds(0, wa)], pack.at[0, :, pl.ds(0, wa)]),
         (w_query.at[:, pl.ds(wa, QW - wa)], pack.at[1, :, pl.ds(0, QW - wa)]),
         (w_latent.at[:, own_lq], pack.at[1, :, pl.ds(QW - wa, lq)]),
-        (hidden, pack.at[0, :, pl.ds(wa, batch)]),
-        (hidden, pack.at[1, :, pl.ds(wb, batch)]),
+        (hidden, hidn),
     ])
 
-    for p in z_peers:
+    for p in z_peers[sig_first:]:
         signal(bar, {"z": p, "c": 1})
     for p in y_peers:
         signal(bar, {"y": p, "c": 1})
@@ -172,7 +176,15 @@
     def take_bytes(n, sem):
         take(rows_of(n), sem)
 
+    chip = nc * rows
+    order = iota((batch, nx * hw), 1)
+    place = order & (hw - 1)
+    b_i = ((place & (rows - 1)) >> 1) * tok + ((order >> log2(hw)) * nc + (place >> log2(rows))) * SEQS + (place & 1)
+    chosen = ones_where((iota((batch, nx * hw), 0) == b_i) & (place < chip))
     done(l_crit)
+    cut = dot(hidn[...], chosen).astype(BF16)
+    for i in range(nx):
+        hp_s[i] = cut[:, hw * i : hw * (i + 1)]
 
     @pl.when(c == 0)
     def _():
@@ -184,9 +196,12 @@
         pl.semaphore_wait(ok.at[0], 1)
 
     for p in x_peers:
-        send(pack.at[((p) & (nc - 1))], crit.at[col], 0, xdev(p))
+        send(hp_s.at[p >> log2(nc)], hp.at[col], 0, xdev(p))
+        send(pack.at[p & (nc - 1)], crit.at[col], 0, xdev(p))
+    sent(hp, ncol - 1)
     sent(crit, ncol - 1)
     crit[pl.ds(col, 1)] = pack[pl.ds(c, 1)]
+    hp[pl.ds(col, 1)] = hp_s[pl.ds(x, 1)]
     l_rot = loads(1, [
         (w_rotkey.at[:, own_pf], rotw.at[pl.ds(0, HEAD_ROT)]),
         (w_rotkey.at[pl.ds(half, half), own_pf], rotw.at[pl.ds(64, half)]),
@@ -233,19 +248,20 @@
     rot_rows = iota((128, pf), 0)
     rot_w = jnp.where((rot_rows & 63) < HEAD_ROT, rotw[...].astype(F32), 0.0).astype(BF16)
 
-    @pl.when(c == 1)
-    def _():
-        pl.semaphore_wait(bar, nc * (nz - 1) + nc * (nt - 1))
-        signal(ok.at[1], {"c": 0})
-        for p in y_peers:
-            for core in range(nc):
-                signal(ok.at[2], {"y": p, "c": core})
-
-    arrived(crit, ncol - 1, 0)
-    r_i, b_i = iota((nc * rows, batch), 0), iota((nc * rows, batch), 1)
-    owner = x * nc + (r_i >> log2(rows))
-    sel_a = ones_where(b_i == ((r_i & (rows - 1)) >> 1) * tok + owner * SEQS + (r_i & 1))
-    hid = crit[:, :, pl.ds(wa, batch)].reshape(pf, batch)
+    def others_ready(when):
+        @pl.when((c == 1) & when)
+        def _():
+            pl.semaphore_wait(bar, nc * (nz - 1) + nc * (nt - 1))
+            signal(ok.at[1], {"c": 0})
+            for p in y_peers:
+                for core in range(nc):
+                    signal(ok.at[2], {"y": p, "c": core})
+
+    others_ready(z >= nz // 2)
+
+    take_bytes((ncol - 1) * (nbytes(crit) + nbytes(hp)) // ncol, rsem.at[slot[0]])
+    sel_a = ones_where(iota((nc * rows, hw), 0) == iota((nc * rows, hw), 1))
+    hid = hp[...].reshape(pf, hw)
     h_t = dot(sel_a, hid, NT)
     scaled = (h_t * again[pl.ds(z, 1), :]).astype(BF16)
     pall[:, pl.ds(0, wa)] = dot(scaled, crit[:, :, pl.ds(0, wa)].reshape(pf, wa))
@@ -255,6 +271,8 @@
     for i in range(nc * nz):
         za_s[i] = pall[pl.ds(SEQS * i, SEQS), :]
 
+    others_ready(z < nz // 2)
+
     @pl.when(c == 0)
     def _():
         pl.semaphore_wait(ok.at[1], 1)
@@ -295,8 +313,8 @@
     @pl.when(y_to == y)
     def _():
         for g in groups[:-1]:
-            send(pack.at[0, :, pl.ds(wa, batch)], hc.at[ring], 3, {"z": ((z + zy * g) & (nz - 1))})
-        hc[pl.ds(ring, 1)] = pack[pl.ds(0, 1), :, pl.ds(wa, batch)]
+            send(hidn, hc.at[ring], 3, {"z": ((z + zy * g) & (nz - 1))})
+        hc[pl.ds(ring, 1)] = hidn[...].reshape(1, FEATS, batch)
 
     for p in x_peers:
         send(so.at[col], so.at[col], 4, xdev(p))
@@ -382,7 +400,7 @@
     h0 = jnp.sum(jnp.where(r_h < LOCAL_HEADS, ho, 0.0), axis=0, keepdims=True)
     h1 = jnp.sum(jnp.where(r_h < LOCAL_HEADS, 0.0, ho), axis=0, keepdims=True)
     heads = rounded(jnp.where(iota((SEQS, HV), 0) == 0, h0, h1))
-    ha[pl.ds(place_of, 1)] = heads.reshape(1, SEQS, HV)
+    ha[pl.ds(place_of, 1)] = heads.astype(BF16).reshape(1, SEQS, HV)
     for dev in plane_peers:
         send(ha.at[place_of], ha.at[place_of], 7, dev)
     sent(ha, npl - 1)
@@ -420,8 +438,18 @@
     rank = dot(hit.astype(BF16), before)
     val = jnp.where(hit > 0.0, rank, -1.0).astype(BF16)
     pslot = ncol * SLOTS
+
+    def pick(upper, shape, token_axis):
+        t, p = iota(shape, token_axis), iota(shape, 1 - token_axis)
+        return ones_where((t >> log2(th)) == 2 * (p >> log2(th)) + upper, jnp.int32) * ones_where(
+            (t & (th - 1)) == (p & (th - 1)), jnp.int32
+        )
+
     expand_p = ones_where(iota((pslot, nex), 1) == nz + (iota((pslot, nex), 0) >> log2(SLOTS)))
-    sel_p[...] = ones_where(dot(expand_p, val) == (iota((pslot, batch), 0) & (SLOTS - 1)).astype(F32))
+    slot_p = (iota((pslot, nz * th), 0) & (SLOTS - 1)).astype(F32)
+    for i in range(2):
+        part = dot(val, pick(i, (batch, nz * th), 0).astype(F32).astype(BF16)).astype(BF16)
+        sel_p[i] = ones_where(dot(expand_p, part) == slot_p)
 
     gain_rows = jnp.broadcast_to(fgain[...][:, None, :], (nz, ncol, pf)).reshape(nz * ncol, pf)
     gr = iota((nz * ncol, pf), 0)
@@ -446,18 +474,20 @@
     arrived(ha, npl - 1, 7)
     for i in range(ncol):
         for j in range(nt):
-            h16[pl.ds(SEQS * i, SEQS), pl.ds(HV * j, HV)] = ha[i * nt + j]
+            h16[pl.ds(SEQS * i, SEQS), pl.ds(HV * j, HV)] = ha[i * nt + j].astype(F32)
     attn = jnp.zeros((tok, 2 * cf), F32)
     for j in range(nt):
         w = jnp.concatenate([aoc[i, j] for i in range(zy)] * 2, axis=0)
         attn = attn + dot(h16[:, pl.ds(HV * j, HV)].astype(BF16), w, NT)
-    mine = (iota((tok, 2 * cf), 1) >> log2(cf)) == (y & 1)
-    mid = jnp.where(mine, rounded(hid_c + rounded(attn)), 0.0)
-    mz[pl.ds(z, 1)] = mid.astype(BF16).reshape(1, tok, 2 * cf)
+    mid = rounded(hid_c + rounded(attn))
+    low8 = iota((th, 2 * cf), 1) < cf
+    mz[pl.ds(z, 1)] = jnp.where(low8, mid[:th], mid[th:]).astype(BF16).reshape(1, th, 2 * cf)
     for p in z_peers:
         send(mz.at[z], mz.at[z], 8, {"z": p})
     sent(mz, nz - 1)
 
+    mine = (iota((tok, 2 * cf), 1) >> log2(cf)) == (y & 1)
+    mid = jnp.where(mine, mid, 0.0)
     ffn = (mid * gp[pl.ds(y >> 1, 1), pl.ds(col, 1)].reshape(1, 2 * cf)).astype(BF16)
     square = jnp.broadcast_to(jnp.sum(mid * mid, axis=1, keepdims=True), (tok, 128))
     take_bytes((zy - 1) * nbytes(sgc) // zy + (ncol - 1) * nbytes(so) // ncol, rsem.at[slot[16]])
@@ -480,15 +510,22 @@
     wt[pl.ds(0, nslot), :] = jnp.where(in_slot, dot(expand, w_hi), 0.0).astype(BF16)
     wt[pl.ds(nslot, nslot), :] = jnp.where(in_slot, dot(expand, w_lo), 0.0).astype(BF16)
     arrived(mz, nz - 1, 8)
-    mid_all = mz[...].reshape(batch, 2 * cf)
-    tk_s[...] = dot(sel_p[...], mid_all).astype(BF16).reshape(ncol, SLOTS, 2 * cf)
+    mid_all = mz[...].reshape(nz * th, 2 * cf)
+    low = iota((pslot, 2 * cf), 1) < cf
+    tk = jnp.where(low, dot(sel_p[0], mid_all), dot(sel_p[1], mid_all))
+    tk = (tk + pltpu.roll(tk, cf, 1)).reshape(ncol, 2, sh, 2 * cf)
+    tk_s[...] = jnp.where(iota((ncol, sh, 2 * cf), 2) < cf, tk[:, 0], tk[:, 1]).astype(BF16)
     for dev in plane_peers:
         send(tk_s.at[dev["x"] * nc + dev["c"]], tk_r.at[place_of], 10, dev)
     sent(tk_r, npl - 1)
     tk_r[pl.ds(place_of, 1)] = tk_s[pl.ds(col, 1)]
     f_i, l_i = iota((pf, 2 * cf), 0), iota((pf, 2 * cf), 1)
-    own_f = (f_i >> log2(FEATS) == col) & (l_i == (z & (2 * zy - 1)) * FEATS + (f_i & (FEATS - 1))) & (y_to == y)
-    tot0[...] = dot(ones_where(own_f), mid_all, NT)
+    own_f = ((f_i >> log2(FEATS)) == col) & (y_to == y)
+    own_l = ring * FEATS + (f_i & (FEATS - 1))
+    tot0[...] = jnp.zeros((pf, batch), F32)
+    for i in range(2):
+        part = dot(ones_where(own_f & (l_i == own_l + cf * i)), mid_all, NT).astype(BF16)
+        tot0[...] += dot(part, pick(i, (nz * th, batch), 1).astype(F32).astype(BF16))
 
     arrived(sh_r, npl - 1, 9)
     tot = sh_r[0]
@@ -505,21 +542,25 @@
     done(l_exp)
     arrived(tk_r, npl - 1, 10)
     pieces = []
+    low_s = iota((sh, 2 * cf), 1) < cf
     sq = jnp.zeros((SLOTS, 2 * cf), F32)
     for i in range(ncol):
         for k in range(nt // 2):
-            v = tk_r[i * nt + 2 * k].astype(F32) + tk_r[i * nt + 2 * k + 1].astype(F32)
+            va = tk_r[i * nt + 2 * k].astype(F32)
+            vb = tk_r[i * nt + 2 * k + 1].astype(F32)
+            v = jnp.concatenate(
+                [jnp.where(low_s, va, pltpu.roll(vb, cf, 1)), jnp.where(low_s, pltpu.roll(va, cf, 1), vb)], axis=0
+            )
             sq = sq + v * v
             pieces.append((v * gp[k, pl.ds(i, 1), :]).astype(BF16))
     gu = dot(jnp.concatenate(pieces, axis=1), wgu[...].reshape(width, 2 * HIDDEN))
     scale = lax.rsqrt(jnp.sum(sq, axis=1, keepdims=True) / width + EPSILON)
     gate = scale * gu[:, :HIDDEN]
     act = (gate / (1.0 + jnp.exp(-gate)) * (scale * gu[:, HIDDEN:])).astype(BF16)
-    out = dot(act, wd[...])
-    for i in range(nz):
-        zh_s[i] = out[:, pf * i : pf * (i + 1)].astype(BF16)
-    for p in z_peers:
-        send(zh_s.at[p], zh_r.at[z], 12, {"z": p})
+    for p in z_peers + [z]:
+        zh_s[pl.ds(p, 1)] = dot(act, wd[:, pl.ds(pl.multiple_of(p * pf, pf), pf)]).astype(BF16).reshape(1, SLOTS, pf)
+        if p is not z:
+            send(zh_s.at[p], zh_r.at[z], 12, {"z": p})
     sent(zh_s, nz - 1)
     zh_r[pl.ds(z, 1)] = zh_s[pl.ds(z, 1)]
 
@@ -598,7 +639,8 @@
     cf = FEATS * nz // nt
     npl = ncol * nt
     scratch = [
-        vm((nc, FEATS, wa + batch), BF16), vm((ncol, FEATS, wa + batch), BF16),
+        vm((nc, FEATS, wa), BF16), vm((ncol, FEATS, wa), BF16),
+        vm((FEATS, batch), BF16), vm((nx, FEATS, max(128, nc * rows)), BF16), vm((ncol, FEATS, max(128, nc * rows)), BF16),
         vm((ncol, FEATS, HIDDEN), BF16),
         vm((FEATS, 2 * HV), BF16),
         vm((nz // nt, nt, FEATS, HV), BF16), vm((nz // nt, nt, FEATS, HV), BF16),
@@ -613,16 +655,16 @@
         vm((2, half, CACHE), F32),
         vm((nc * nz, SEQS, wa + 128), F32), vm((nz, SEQS, wa + 128), F32), vm((nz, SEQS, wa), F32),
         vm((nt, SEQS, lq), F32),
-        vm((npl, SEQS, HV), F32),
-        vm((nz, tok, 2 * cf), BF16),
+        vm((npl, SEQS, HV), BF16),
+        vm((nz, tok // 2, 2 * cf), BF16),
         vm((npl, SEQS, 2 * HIDDEN + 128), F32), vm((npl, SEQS, 2 * HIDDEN + 128), F32),
-        vm((ncol, SLOTS, 2 * cf), BF16), vm((npl, SLOTS, 2 * cf), BF16),
+        vm((ncol, SLOTS // 2, 2 * cf), BF16), vm((npl, SLOTS // 2, 2 * cf), BF16),
         vm((nz, SLOTS, pf), BF16), vm((nz, SLOTS, pf), BF16),
         vm((nz, SEQS, HIDDEN), F32),
         vm((ncol, nt, FEATS // 2, hl), F32), vm((npl, FEATS // 2, hl), F32),
         vm((LATENT + 256, QW), BF16),
         vm((SEQS, HEAD_ROT, CACHE), F32),
-        vm((ncol * SLOTS, batch), BF16),
+        vm((2, ncol * SLOTS, batch // 2), BF16),
         vm((2 * nslot, batch), BF16),
         vm((tok, nt * HV), F32),
         vm((rows, HIDDEN), F32),

time: 63.8 us -> 63.2 us (level)
  Pallas kernels: 63 us -> 62.3 us
where the time goes in v6:
time: 63.2 us; the launch traced here: 63 us
  Pallas kernels  62.3 us (99%)
  between operations  0.65 us (1%)
    pallas_call x1, Pallas kernels, body(): pl.pallas_call(functools.partial(kernel, nz, nx, nc, nt), out_shape=(pltp...  61.7 us

profile of v6, /device:TPU:1, one launch (start us, length us, event | category | flops | bytes accessed | tf_op | source)
XLA Modules:
  0.0 63.0 jit_solution(16211190661020354312)
XLA Ops:
  0.6 61.7 %layer.1 = (bf16[16,64]{1,0:T(8,128)(2,1)S(1)}, bf16[2,512]{1,0:T(2,128)(2,1)S(1)}, bf16[2,32]{1,0:T(2,128)(2,1)S(1)}) custom-call(bf16[16,256]{1,0:T(8,128)(2,1)} %refs_0_.1, f32[16,128]{1,0:T(8,128)} %bitcast.9, bf16[16,384]{1,0:T(8,128)(2,1)} %refs_2_.1, bf16[16,512]{1,0:T(8,128)(2,1)} %refs_3_.1, bf16[32,2048]{1,0:T(8,128)(2,1)} %refs_4_.1, ...), custom_call_target="tpu_custom_call" | custom-call | tf_op jit(solution)/shard_map/layer/pallas_call | solution.py:682
  62.4 0.6 finish.1

commit v7 on v6

--- a/solution.py
+++ b/solution.py
@@ -167,7 +167,7 @@
     def arrived(buf, n, k):
         take(buf.at[pl.ds(0, n)], rsem.at[slot[k]])
 
-    slot = {0: 0, 1: 1, 3: 1, 6: 1, 2: 2, 14: 2, 5: 3, 7: 4, 15: 5, 17: 5, 16: 6, 4: 6, 8: 7, 9: 8, 10: 9, 11: 10, 12: 11, 13: 12}
+    slot = {0: 0, 1: 1, 3: 1, 6: 13, 2: 2, 14: 2, 5: 3, 7: 4, 15: 5, 17: 5, 16: 6, 4: 6, 8: 7, 9: 8, 10: 9, 11: 10, 12: 11, 13: 12}
     pending = []
 
     def sent(buf, n):
@@ -295,9 +295,9 @@
     done(l_bg)
 
     groups = sorted(range(nt), key=lambda k: -min(k, nt - k))
-    for src, dst, k in ((bgs.at[:, pl.ds(0, HV)], aoc, 1), (bgs.at[:, pl.ds(HV, HV)], sgc, 6)):
+    def first_stage(src, dst, k):
         for g in groups:
-            dev = {"z": ((z + zy * g) & (nz - 1)), "y": y_to}
+            dev = {"z": (z + zy * g) & (nz - 1), "y": y_to}
             if g:
                 send(src, dst.at[ring, y], k, dev)
             else:
@@ -309,6 +309,8 @@
                 @pl.when(y_to == y)
                 def _():
                     dst[pl.ds(ring, 1), pl.ds(y, 1)] = src[...].reshape(1, 1, FEATS, HV)
+
+    first_stage(bgs.at[:, pl.ds(0, HV)], aoc, 1)
 
     @pl.when(y_to == y)
     def _():
@@ -338,6 +340,7 @@
     for p in y_peers:
         send(yb.at[y], yb.at[y], 5, {"y": p})
     sent(yb, nt - 1)
+    first_stage(bgs.at[:, pl.ds(HV, HV)], sgc, 6)
     q = rounded(jnp.concatenate([tot[:, :wa], tot_b[:, : QW - wa]], axis=1) * scale)
     nrows = SEQS * LOCAL_HEADS
     r8 = iota((nrows, 128), 0)
@@ -378,6 +381,37 @@
     new_swap = pltpu.roll(new_rot, 64, 1)
     own_rot = jnp.where(lane8 < HEAD_ROT, per_row(new_rot) * cos8 + per_row(new_swap) * sin8, 0.0)
 
+    size_bg, size_h = nbytes(bgs) // 2, nbytes(hc) // zy
+    beside = [r if 2 * r <= zy else r - zy for r in range(1, zy)]
+    far = ((y_to - y) & (nt - 1)) == nt // 2
+
+    def forward_rows(when):
+        for here in (True, False):
+
+            @pl.when(when & ((y_to == y) if here else (y_to != y)))
+            def _():
+                take_bytes((nt - 1) * size_bg if here else nt * size_bg + size_h, rsem.at[1])
+
+        @pl.when(when)
+        def _():
+            for r in sorted(beside, key=lambda r: -abs(r)):
+                dev = {"z": (z + r + nz) & (nz - 1)}
+                send(hc.at[ring], hc.at[ring], 17, dev)
+                send(aoc.at[ring], aoc.at[ring], 15, dev)
+
+    def forward_shared(when):
+        for here in (True, False):
+
+            @pl.when(when & ((y_to == y) if here else (y_to != y)))
+            def _():
+                take_bytes((nt - 1 if here else nt) * size_bg, rsem.at[slot[6]])
+
+        @pl.when(when)
+        def _():
+            for r in sorted(beside, key=lambda r: -abs(r)):
+                send(sgc.at[ring], sgc.at[ring], 16, {"z": (z + r + nz) & (nz - 1)})
+
+    forward_rows(jnp.logical_not(far))
     arrived(yb, nt - 1, 5)
     raw = jnp.concatenate([yb[i] for i in range(nt)], axis=1)
     new_latent = (
@@ -405,20 +439,7 @@
         send(ha.at[place_of], ha.at[place_of], 7, dev)
     sent(ha, npl - 1)
 
-    size_bg, size_h = nbytes(bgs), nbytes(hc) // zy
-    for here in (True, False):
-
-        @pl.when((y_to == y) if here else (y_to != y))
-        def _():
-            take_bytes((nt - 1) * size_bg if here else nt * size_bg + size_h, rsem.at[1])
-
-    beside = [r if 2 * r <= zy else r - zy for r in range(1, zy)]
-    for r in sorted(beside, key=lambda r: -abs(r)):
-        dev = {"z": ((z + r + nz) & (nz - 1))}
-        send(hc.at[ring], hc.at[ring], 17, dev)
-        send(aoc.at[ring], aoc.at[ring], 15, dev)
-    for r in sorted(beside, key=lambda r: -abs(r)):
-        send(sgc.at[ring], sgc.at[ring], 16, {"z": ((z + r + nz) & (nz - 1))})
+    forward_rows(far)
     for buf in (hc, aoc, sgc):
         sent(buf, zy - 1)
 
@@ -465,6 +486,7 @@
             g = jnp.where(lane_z == i, tiled[2 * zy * k + i], g)
         gp[k] = g
 
+    forward_shared(jnp.logical_not(far))
     if beside:
         take_bytes((zy - 1) * (nbytes(hc) + nbytes(aoc)) // zy, rsem.at[slot[15]])
     t_i, l_i = iota((tok, batch), 0), iota((tok, batch), 1)
@@ -485,6 +507,8 @@
     for p in z_peers:
         send(mz.at[z], mz.at[z], 8, {"z": p})
     sent(mz, nz - 1)
+
+    forward_shared(far)
 
     mine = (iota((tok, 2 * cf), 1) >> log2(cf)) == (y & 1)
     mid = jnp.where(mine, mid, 0.0)
@@ -601,7 +625,7 @@
             @pl.when((c == core) & ((y_to == y) if here else (y_to != y)))
             def _():
                 mine = (nc * nz - 1) * (size_b if core else size_a)
-                mine += (nt - 1) * (size_bg + size_h) if here else nt * size_bg
+                mine += (nt - 1) * (2 * size_bg + size_h) if here else nt * 2 * size_bg
                 take_bytes(sum(pending) + mine, ssem.at[0])
 
 
@@ -674,7 +698,7 @@
         vm((pf, batch), F32),
         pltpu.SemaphoreType.DMA((6,)),
         pltpu.SemaphoreType.DMA((1,)),
-        pltpu.SemaphoreType.DMA((13,)),
+        pltpu.SemaphoreType.DMA((14,)),
         pltpu.SemaphoreType.REGULAR((3,)),
         vm((2560 * 1024 // UNIT, 2, UNIT // 8), F32),
     ]

time: 63.2 us -> 62 us (0.981)
  Pallas kernels: 62.3 us -> 61.2 us
    pallas_call x1, Pallas kernels: 61.7 us -> 60.6 us  [body(): pl.pallas_call(functools.partial(kernel, nz, nx, nc, nt), out_shape=(pltp...]
where the time goes in v7:
time: 62 us; the launch traced here: 61.9 us
  Pallas kernels  61.2 us (99%)
  between operations  0.65 us (1%)
    pallas_call x1, Pallas kernels, body(): pl.pallas_call(functools.partial(kernel, nz, nx, nc, nt), out_shape=(pltp...  60.6 us

profile of v7, /device:TPU:1, one launch (start us, length us, event | category | flops | bytes accessed | tf_op | source)
XLA Modules:
  0.0 61.9 jit_solution(438781950057675375)
XLA Ops:
  0.6 60.6 %layer.1 = (bf16[16,64]{1,0:T(8,128)(2,1)S(1)}, bf16[2,512]{1,0:T(2,128)(2,1)S(1)}, bf16[2,32]{1,0:T(2,128)(2,1)S(1)}) custom-call(bf16[16,256]{1,0:T(8,128)(2,1)} %refs_0_.1, f32[16,128]{1,0:T(8,128)} %bitcast.9, bf16[16,384]{1,0:T(8,128)(2,1)} %refs_2_.1, bf16[16,512]{1,0:T(8,128)(2,1)} %refs_3_.1, bf16[32,2048]{1,0:T(8,128)(2,1)} %refs_4_.1, ...), custom_call_target="tpu_custom_call" | custom-call | tf_op jit(solution)/shard_map/layer/pallas_call | solution.py:706
  61.2 0.6 %finish.1 = (bf16[16,64]{1,0:T(8,128)(2,1)}, bf16[2,512]{1,0:T(2,128)(2,1)}, bf16[2,32]{1,0:T(2,128)(2,1)}) custom-call(bf16[16,64]{1,0:T(8,128)(2,1)S(1)} %get-tuple-element.6.refs_0_, bf16[2,512]{1,0:T(2,128)(2,1)S(1)} %get-tuple-element.7.refs_1_, bf16[2,32]{1,0:T(2,128)(2,1)S(1)} %get-tuple-element.8.refs_2_), custom_call_target="tpu_custom_call" | custom-call | tf_op jit(solution)/shard_map/finish/pallas_call | solution.py:720

commit v8 on v7

--- a/solution.py
+++ b/solution.py
@@ -535,12 +535,18 @@
     wt[pl.ds(nslot, nslot), :] = jnp.where(in_slot, dot(expand, w_lo), 0.0).astype(BF16)
     arrived(mz, nz - 1, 8)
     mid_all = mz[...].reshape(nz * th, 2 * cf)
-    low = iota((pslot, 2 * cf), 1) < cf
-    tk = jnp.where(low, dot(sel_p[0], mid_all), dot(sel_p[1], mid_all))
-    tk = (tk + pltpu.roll(tk, cf, 1)).reshape(ncol, 2, sh, 2 * cf)
-    tk_s[...] = jnp.where(iota((ncol, sh, 2 * cf), 2) < cf, tk[:, 0], tk[:, 1]).astype(BF16)
-    for dev in plane_peers:
-        send(tk_s.at[dev["x"] * nc + dev["c"]], tk_r.at[place_of], 10, dev)
+    group = nc * SLOTS
+    low = iota((group, 2 * cf), 1) < cf
+    for dx in sorted(range(nx), key=lambda d: -min(d, nx - d)):
+        chip_x = (x + dx) & (nx - 1)
+        mine_of = pl.ds(pl.multiple_of(chip_x * group, group), group)
+        tk = jnp.where(low, dot(sel_p[0, mine_of, :], mid_all), dot(sel_p[1, mine_of, :], mid_all))
+        tk = (tk + pltpu.roll(tk, cf, 1)).reshape(nc, 2, sh, 2 * cf)
+        tk = jnp.where(iota((nc, sh, 2 * cf), 2) < cf, tk[:, 0], tk[:, 1]).astype(BF16)
+        tk_s[pl.ds(chip_x * nc, nc)] = tk
+        for (ex, _, _), dev in zip(plane_order, plane_peers):
+            if ex == dx:
+                send(tk_s.at[chip_x * nc + dev["c"]], tk_r.at[place_of], 10, dev)
     sent(tk_r, npl - 1)
     tk_r[pl.ds(place_of, 1)] = tk_s[pl.ds(col, 1)]
     f_i, l_i = iota((pf, 2 * cf), 0), iota((pf, 2 * cf), 1)
@@ -594,22 +600,36 @@
     b_i, r_i = iota((batch, rows), 0), iota((batch, rows), 1)
     place = ones_where(b_i == (r_i >> 1) * tok + col * SEQS + (r_i & 1))
     spread_act = dot(place, s32[...].astype(BF16)).astype(BF16)
-    total = tot0[...] + dot(so[...].reshape(pf, HIDDEN), spread_act, NT)
+    tot0[...] += dot(so[...].reshape(pf, HIDDEN), spread_act, NT)
     arrived(zh_r, nz - 1, 12)
     parts = zh_r[...].reshape(nslot, pf)
-    total = total + dot(parts, wt[pl.ds(0, nslot), :], TN) + dot(parts, wt[pl.ds(nslot, nslot), :], TN)
-    total = total.reshape(ncol, 2, FEATS // 2, batch)
+    flat = (ncol * FEATS // 2, hl)
     low_lane = iota((ncol, FEATS // 2, hl), 2) < ob
-    for k in range(nt // 2):
-        ta = total[:, 0, :, hl * k : hl * (k + 1)]
-        tb = total[:, 1, :, hl * k : hl * (k + 1)]
-        flat = (ncol * FEATS // 2, hl)
+    far_first = sorted(
+        [(dx, dc) for dx in range(nx) for dc in range(nc)], key=lambda t: -(2 * min(t[0], nx - t[0]) + t[1])
+    )
+    for near in range(2):
+        side = (y >> 1) if near else 1 - (y >> 1)
+        lanes = pl.ds(pl.multiple_of(side * hl, hl), hl)
+        total = tot0[:, lanes] + dot(parts, wt[pl.ds(0, nslot), lanes], TN) + dot(parts, wt[pl.ds(nslot, nslot), lanes], TN)
+        total = total.reshape(ncol, 2, FEATS // 2, hl)
+        ta, tb = total[:, 0], total[:, 1]
         ra = pltpu.roll(ta.reshape(flat), ob, 1).reshape(ta.shape)
         rb = pltpu.roll(tb.reshape(flat), ob, 1).reshape(tb.shape)
-        pd_s[:, 2 * k] = jnp.where(low_lane, ta, rb)
-        pd_s[:, 2 * k + 1] = jnp.where(low_lane, ra, tb)
-    for dev in plane_peers:
-        send(pd_s.at[dev["x"] * nc + dev["c"], dev["y"]], pd_r.at[place_of], 13, dev)
+        pd_s[:, pl.ds(2 * side, 1)] = jnp.where(low_lane, ta, rb).reshape(ncol, 1, FEATS // 2, hl)
+        pd_s[:, pl.ds(2 * side + 1, 1)] = jnp.where(low_lane, ra, tb).reshape(ncol, 1, FEATS // 2, hl)
+        for dx, dc in far_first:
+            px, pc = (x + dx) & (nx - 1), (c + dc) & (nc - 1)
+            for e in range(2):
+                dev = {"x": px, "c": pc, "y": 2 * side + e}
+
+                def out():
+                    send(pd_s.at[px * nc + pc, 2 * side + e], pd_r.at[place_of], 13, dev)
+
+                if dx or dc or not near:
+                    out()
+                else:
+                    pl.when((y & 1) != e)(out)
     sent(pd_r, npl - 1)
     pd_r[pl.ds(place_of, 1)] = pd_s[pl.ds(col, 1), pl.ds(y, 1)].reshape(1, FEATS // 2, hl)
     arrived(pd_r, npl - 1, 13)

time: 62 us -> 61.9 us (level)
  no operation moved by 1% of the time
where the time goes in v8:
time: 61.9 us; the launch traced here: 61.7 us
  Pallas kernels  61 us (99%)
  between operations  0.65 us (1%)
    pallas_call x1, Pallas kernels, body(): pl.pallas_call(functools.partial(kernel, nz, nx, nc, nt), out_shape=(pltp...  60.4 us

profile of v8, /device:TPU:1, one launch (start us, length us, event | category | flops | bytes accessed | tf_op | source)
XLA Modules:
  0.0 61.7 jit_solution(913524919989194739)
XLA Ops:
  0.6 60.4 %layer.1 = (bf16[16,64]{1,0:T(8,128)(2,1)S(1)}, bf16[2,512]{1,0:T(2,128)(2,1)S(1)}, bf16[2,32]{1,0:T(2,128)(2,1)S(1)}) custom-call(bf16[16,256]{1,0:T(8,128)(2,1)} %refs_0_.1, f32[16,128]{1,0:T(8,128)} %bitcast.9, bf16[16,384]{1,0:T(8,128)(2,1)} %refs_2_.1, bf16[16,512]{1,0:T(8,128)(2,1)} %refs_3_.1, bf16[32,2048]{1,0:T(8,128)(2,1)} %refs_4_.1, ...), custom_call_target="tpu_custom_call" | custom-call | tf_op jit(solution)/shard_map/layer/pallas_call | solution.py:726
  61.1 0.6 %finish.1 = (bf16[16,64]{1,0:T(8,128)(2,1)}, bf16[2,512]{1,0:T(2,128)(2,1)}, bf16[2,32]{1,0:T(2,128)(2,1)}) custom-call(bf16[16,64]{1,0:T(8,128)(2,1)S(1)} %get-tuple-element.6.refs_0_, bf16[2,512]{1,0:T(2,128)(2,1)S(1)} %get-tuple-element.7.refs_1_, bf16[2,32]{1,0:T(2,128)(2,1)S(1)} %get-tuple-element.8.refs_2_), custom_call_target="tpu_custom_call" | custom-call | tf_op jit(solution)/shard_map/finish/pallas_call | solution.py:740
